TPU v7x, 128 devices: a whole 4x4x4 slice. The times are simulated.
128 devices in a mesh: sp: 16 (over z, x), tp: 8 (over y, core).
Axes of the slice: x: 4, y: 4, z: 4, core: 2. Of those that a mesh axis runs over, the one named last changes fastest.
Arguments:
- query_wide: bfloat16 [12288, 8, 256], P('sp', 'tp'), may hold values from -6 to 6
- key_wide: bfloat16 [12288, 8, 256], P('sp', 'tp'), may hold values from -6 to 6
- value_wide: bfloat16 [12288, 8, 256], P('sp', 'tp'), may hold values from -6 to 6
- query_narrow: bfloat16 [12288, 8, 128], P('sp', 'tp'), may hold values from -6 to 6
- key_narrow: bfloat16 [12288, 8, 128], P('sp', 'tp'), may hold values from -6 to 6
- value_narrow: bfloat16 [12288, 8, 128], P('sp', 'tp'), may hold values from -6 to 6
- mix_lambda: float32 [2, 8], P(None, 'tp'), may hold values from 0.3 to 0.8
- residual_in: bfloat16 [12288, 2048], P(('sp', 'tp')), may hold values from -6 to 6
- out_wide: bfloat16 [2048, 2048], P('tp'), may hold values from -0.109375 to 0.109375
- out_narrow: bfloat16 [1024, 2048], P('tp'), may hold values from -0.109375 to 0.109375
- ffn_gain: float32 [2048], replicated, may hold values from 0.1 to 1.9
- expert_ids: int32 [12288, 2], P(('sp', 'tp')), may hold values from 0 to 127, as said below
- expert_weights: float32 [12288, 2], P(('sp', 'tp')), may hold values from 0.1 to 1
- gate_weight: bfloat16 [128, 2048, 1024], P(('sp', 'tp')), may hold values from -0.125 to 0.125
- up_weight: bfloat16 [128, 2048, 1024], P(('sp', 'tp')), may hold values from -0.125 to 0.125
- down_weight: bfloat16 [128, 1024, 2048], P(('sp', 'tp')), may hold values from -0.1875 to 0.1875
Outputs:
- layer_out: bfloat16 [12288, 2048], P(('sp', 'tp'))
Inputs may be any that keep to these rules, and one draw needn't show every extreme that they name: `expert_ids`: A row's two experts differ and lie in the same group of 4 consecutive experts (32 groups). In each aligned block of 96 rows (the rows of one device) no expert is named by more than 3 rows, and in every block some expert is named by exactly 3 rows.
All inputs are finite; a program needn't handle non-finite values.
Results may differ from a plain program's by a relative error of at most 0.015.
Values may be sent and summed in bfloat16 or wider, within the bound.
No kernel may reach another device: no remote copies, remote signals or barrier semaphores. Data moves between devices by JAX's collectives and lax.ppermute only.
A program may use at most 192 MiB of HBM per device.

v0:
```python
import jax
import jax.numpy as jnp
from jax import lax
from jax.experimental import pallas as pl
from jax.experimental.pallas import tpu as pltpu
from jax.sharding import Mesh
from jax.sharding import PartitionSpec as P

TP = ("y", "c")
SP_TP = ("z", "x", "y", "c")
RING = 4
LOG2E = 1.4426950408889634
NEG_FILL = -1e30
STAT_ROWS = 16
LANES = 128
BLOCK = 256
SOME = 48
LEAST_TOTAL = 2.0**-60
MOST_TOTAL = 2.0**100


def pack_kernel(v_wide, k_narrow, v_narrow, v_out, kv_out):
    chunk, width = v_wide.shape
    half = chunk // 2
    width_narrow = v_narrow.shape[1]
    for j in range(chunk // BLOCK):
        rows = slice(j * BLOCK, (j + 1) * BLOCK)
        v_out[j * width : (j + 1) * width, :] = v_wide[rows, :].T
        begin = half + j * width_narrow
        kv_out[begin : begin + width_narrow, :] = v_narrow[rows, :].T
    for side in range(2):
        lanes = slice(side * LANES, (side + 1) * LANES)
        kv_out[:half, lanes] = k_narrow[side * half : (side + 1) * half, :]


def pack(v_wide, k_narrow, v_narrow):
    chunk, width = v_wide.shape
    rows = chunk // 2 + chunk // BLOCK * v_narrow.shape[1]
    return pl.pallas_call(
        pack_kernel,
        out_shape=(
            jax.ShapeDtypeStruct((chunk // BLOCK * width, BLOCK), jnp.bfloat16),
            jax.ShapeDtypeStruct((rows, BLOCK), jnp.bfloat16),
        ),
        name="pack",
    )(v_wide, k_narrow, v_narrow)


def attend_kernel(plan, q_ref, *refs, pieces, wide, diagonal, fill, size, width, chunk):
    slots = len(refs[: -7]) // pieces
    src_refs = refs[: slots * pieces]
    out_ref = refs[slots * pieces]
    q_scr, kv_scr, acc, out_scr, sems, q_sem = refs[slots * pieces + 1 :]
    active, count, offset = plan[0], plan[1], plan[2]
    scale = size ** (-0.5) * LOG2E
    key_rows = chunk if wide else chunk // 2
    halves = key_rows // LANES

    def slot_copies(slot):
        made = []
        begin = 0
        for k in range(pieces):
            source = src_refs[slot * pieces + k]
            rows = source.shape[0]
            made.append(
                pltpu.make_async_copy(
                    source, kv_scr.at[slot, pl.ds(begin, rows), :], sems.at[slot, k]
                )
            )
            begin += rows
        return made

    def wait_slot(slot):
        begin = 0
        for k in range(pieces):
            source = src_refs[k]
            rows = source.shape[0]
            pltpu.make_async_copy(
                source, kv_scr.at[slot, pl.ds(begin, rows), :], sems.at[slot, k]
            ).wait()
            begin += rows

    def only_map(rows, m):
        lane = lax.broadcasted_iota(jnp.int32, rows.shape, 1)
        return jnp.where((lane >= m * size) & (lane < (m + 1) * size), rows, 0)

    def dot_nt(left, right):
        return lax.dot_general(
            left, right, (((1,), (1,)), ((), ())), preferred_element_type=jnp.float32
        )

    def value_block(slot, j):
        return kv_scr[slot, pl.ds(key_rows + j * width, width), :]

    def store_result(m, columns, read, total, level):
        out_scr[pl.ds(m * width, width), columns] = (read * (1.0 / total)).astype(jnp.bfloat16)
        row = lax.broadcasted_iota(jnp.int32, (8, total.shape[1]), 0)
        packed = jnp.zeros((8, total.shape[1]), jnp.float32)
        for k in range(3):
            term = level.astype(jnp.bfloat16).astype(jnp.float32)
            packed = jnp.where(row == k, term, packed)
            level = level - term
        return packed

    @pl.when(active > 0)
    def _():
        got_q = pltpu.make_async_copy(q_ref, q_scr, q_sem)
        got_q.start()
        for slot in range(slots):

            @pl.when((slot >= offset) & (slot < offset + count))
            def _(slot=slot):
                for made in slot_copies(slot):
                    made.start()

        acc[...] = jnp.zeros_like(acc)
        got_q.wait()

        def add_slot(number, totals):
            slot = 0 if diagonal else number + offset
            wait_slot(slot)
            values = jnp.concatenate(
                [value_block(slot, j) for j in range(chunk // BLOCK)], axis=1
            )
            result = []
            for m in range(2):
                if wide:
                    lanes = slice(m * size, (m + 1) * size)
                    scores = dot_nt(kv_scr[slot, :key_rows, lanes], q_scr[:, lanes])
                else:
                    queries = only_map(q_scr[...], m)
                    scores = jnp.concatenate(
                        [
                            dot_nt(kv_scr[slot, :key_rows, side * LANES : (side + 1) * LANES], queries)
                            for side in range(2)
                        ],
                        axis=0,
                    )
                scores = scores * scale
                if diagonal:
                    key_pos = lax.broadcasted_iota(jnp.int32, scores.shape, 0)
                    query_pos = lax.broadcasted_iota(jnp.int32, scores.shape, 1)
                    scores = jnp.where(key_pos <= query_pos, scores, NEG_FILL)
                weights = jnp.exp2(scores)
                result.append(totals[m] + jnp.sum(weights.reshape(chunk // 8, 8, chunk), axis=0))
                acc[m] = acc[m] + jnp.dot(
                    values, weights.astype(jnp.bfloat16), preferred_element_type=jnp.float32
                )
            return tuple(result)

        none = jnp.zeros((8, chunk), jnp.float32)
        if diagonal:
            totals = add_slot(0, (none, none))
        else:
            totals = lax.fori_loop(0, count, add_slot, (none, none))
        outside = jnp.zeros((1, chunk), jnp.float32)
        stats = []
        for m in range(2):
            total = jnp.sum(totals[m], axis=0, keepdims=True)
            inside = (total >= LEAST_TOTAL) & (total <= MOST_TOTAL)
            outside = jnp.maximum(outside, jnp.where(inside, 0.0, 1.0))
            stats.append(store_result(m, slice(None), acc[m], total, jnp.log2(total)))
        out_scr[2 * width :, :] = jnp.concatenate(stats, axis=0).astype(jnp.bfloat16)

        @pl.when(jnp.max(outside) > 0)
        def _():
            def packed_rows(take, number):
                made = []
                for k in range(2):
                    piece = number * 2 + k
                    place = pl.ds(pl.multiple_of(lax.rem(piece, halves) * LANES, LANES), LANES)
                    first, second = take(place)
                    made.append(jnp.where(piece < halves, first, second))
                return jnp.concatenate(made, axis=0)

            def keys_at(slot, number):
                return packed_rows(
                    lambda place: (kv_scr[slot, place, :LANES], kv_scr[slot, place, LANES:]), number
                )

            def one_query_block(number, _):
                begin = pl.multiple_of(number * BLOCK, BLOCK)
                columns = pl.ds(begin, BLOCK)

                def one_map(m, packed):
                    acc[m, :, columns] = jnp.zeros((width, BLOCK), jnp.float32)

                    def careful(index, state):
                        peak, total = state
                        slot = index // (chunk // BLOCK) + offset
                        block = lax.rem(index, chunk // BLOCK)
                        place = pl.ds(pl.multiple_of(block * BLOCK, BLOCK), BLOCK)
                        if wide:
                            lanes = pl.ds(pl.multiple_of(m * size, size), size)
                            scores = dot_nt(kv_scr[slot, place, lanes], q_scr[columns, lanes])
                        else:
                            scores = dot_nt(keys_at(slot, block), only_map(q_scr[columns, :], m))
                        scores = scores * scale
                        if diagonal:
                            key_pos = block * BLOCK + lax.broadcasted_iota(
                                jnp.int32, scores.shape, 0
                            )
                            query_pos = begin + lax.broadcasted_iota(jnp.int32, scores.shape, 1)
                            scores = jnp.where(key_pos <= query_pos, scores, NEG_FILL)
                        new_peak = jnp.maximum(peak, jnp.max(scores, axis=0, keepdims=True))
                        factor = jnp.exp2(peak - new_peak)
                        weights = jnp.exp2(scores - new_peak)
                        acc[m, :, columns] = factor * acc[m, :, columns] + jnp.dot(
                            value_block(slot, block),
                            weights.astype(jnp.bfloat16),
                            preferred_element_type=jnp.float32,
                        )
                        return new_peak, factor * total + jnp.sum(weights, axis=0, keepdims=True)

                    peak, total = lax.fori_loop(
                        0,
                        count * (chunk // BLOCK),
                        careful,
                        (
                            jnp.full((1, BLOCK), NEG_FILL, jnp.float32),
                            jnp.zeros((1, BLOCK), jnp.float32),
                        ),
                    )
                    rows = store_result(
                        m, columns, acc[m, :, columns], total, peak + jnp.log2(total)
                    )
                    both = jnp.concatenate([rows, rows], axis=0)
                    row = lax.broadcasted_iota(jnp.int32, both.shape, 0)
                    return jnp.where((row >= 8 * m) & (row < 8 * m + 8), both, packed)

                packed = lax.fori_loop(
                    0, 2, one_map, jnp.zeros((STAT_ROWS, BLOCK), jnp.float32)
                )
                out_scr[2 * width :, columns] = packed.astype(jnp.bfloat16)
                return 0

            lax.fori_loop(0, chunk // BLOCK, one_query_block, 0)

    if fill:

        @pl.when(active == 0)
        def _():
            out_scr[...] = jnp.zeros_like(out_scr)

    @pl.when((active > 0) | fill)
    def _():
        sent = pltpu.make_async_copy(out_scr, out_ref, q_sem)
        sent.start()
        sent.wait()


def attend(plan, queries, sources, wide, diagonal, fill, size, width):
    chunk = queries.shape[0]
    pieces = len(sources[0])
    flat = [array for group in sources for array in group]
    kv_rows = sum(array.shape[0] for array in sources[0])
    body = lambda *refs: attend_kernel(
        *refs,
        pieces=pieces,
        wide=wide,
        diagonal=diagonal,
        fill=fill,
        size=size,
        width=width,
        chunk=chunk,
    )
    area = chunk * chunk * 2 * 2
    return pl.pallas_call(
        body,
        out_shape=jax.ShapeDtypeStruct((2 * width + STAT_ROWS, chunk), jnp.bfloat16),
        in_specs=[pl.BlockSpec(memory_space=pltpu.SMEM)]
        + [pl.BlockSpec(memory_space=pl.ANY)] * (1 + len(flat)),
        out_specs=pl.BlockSpec(memory_space=pl.ANY),
        scratch_shapes=[
            pltpu.VMEM(queries.shape, jnp.bfloat16),
            pltpu.VMEM((len(sources), kv_rows, BLOCK), jnp.bfloat16),
            pltpu.VMEM((2, width, chunk), jnp.float32),
            pltpu.VMEM((2 * width + STAT_ROWS, chunk), jnp.bfloat16),
            pltpu.SemaphoreType.DMA((len(sources), pieces)),
            pltpu.SemaphoreType.DMA,
        ],
        cost_estimate=pl.CostEstimate(
            flops=2 * area * (size + width),
            transcendentals=area,
            bytes_accessed=len(sources) * kv_rows * 512,
        ),
    )(plan, queries, *flat)


def merge_kernel(valid, lam, *refs, widths, counts):
    out_ref = refs[-1]
    guarded = (1, None)
    begin = 0
    column = 0
    for group, (width, count) in enumerate(zip(widths, counts)):
        parts = refs[begin : begin + count]
        begin += count
        reads = []
        for m in range(2):
            levels = []
            for k, part in enumerate(parts):
                stats = part[2 * width :, :].astype(jnp.float32)
                level = stats[8 * m : 8 * m + 1] + stats[8 * m + 1 : 8 * m + 2] + stats[
                    8 * m + 2 : 8 * m + 3
                ]
                levels.append(jnp.where(valid[group, k] > 0, level, NEG_FILL))
            top = levels[0]
            for level in levels[1:]:
                top = jnp.maximum(top, level)
            shares = [jnp.exp2(level - top) for level in levels]
            whole = shares[0]
            for share in shares[1:]:
                whole = whole + share
            read = None
            for k, (share, part) in enumerate(zip(shares, parts)):
                term = part[m * width : (m + 1) * width, :].astype(jnp.float32) * (share / whole)
                if read is None:
                    read = term
                elif guarded[group] == k:
                    read = read + jnp.where(valid[group, k] > 0, term, 0.0)
                else:
                    read = read + term
            reads.append(read)
        mixed = reads[0] - lam[group, 0] * reads[1]
        normed = mixed * lax.rsqrt(jnp.mean(mixed * mixed, axis=0, keepdims=True) + 1e-06)
        out_ref[:, column : column + width] = normed.T.astype(jnp.bfloat16)
        column += width


def merge(valid, lam, groups, widths):
    chunk = groups[0][0].shape[1]
    counts = [len(parts) for parts in groups]
    flat = [part for parts in groups for part in parts]
    body = lambda *refs: merge_kernel(*refs, widths=widths, counts=counts)
    return pl.pallas_call(
        body,
        grid=(chunk // BLOCK,),
        out_shape=jax.ShapeDtypeStruct((chunk, sum(widths)), jnp.bfloat16),
        in_specs=[pl.BlockSpec(memory_space=pltpu.SMEM)] * 2
        + [pl.BlockSpec((part.shape[0], BLOCK), lambda i: (0, i)) for part in flat],
        out_specs=pl.BlockSpec((BLOCK, sum(widths)), lambda i: (i, 0)),
        name="merge_reads",
    )(valid, lam, *flat)


def around(array, axis, by):
    return lax.ppermute(array, axis, [(k, (k + by) % RING) for k in range(RING)])


def onward(array, axis, by):
    return lax.ppermute(
        array, axis, [(k, k + by) for k in range(RING) if 0 <= k + by < RING]
    )


def after(array, *others):
    return lax.optimization_barrier((array,) + others)[0]


def attention(
    query_wide, key_wide, value_wide, query_narrow, key_narrow, value_narrow, mix_lambda
):
    z = lax.axis_index("z")
    x = lax.axis_index("x")
    size_wide = query_wide.shape[1] // 2
    size_narrow = query_narrow.shape[1] // 2
    width_wide, width_narrow = value_wide.shape[1], value_narrow.shape[1]

    xk_near = around(key_wide, "x", 1)
    q_later = {d: onward(query_wide, "z", -d) for d in (1, 2, 3)}
    values, kv_narrow = pack(value_wide, key_narrow, value_narrow)
    xv_back = around(values, "x", -1)
    xv_near = around(values, "x", 1)
    xk_back = around(key_wide, "x", -1)
    kv_below = {d: onward(kv_narrow, "z", d) for d in (1, 2, 3)}
    xk_far = around(xk_near, "x", 1)
    xv_far = around(xv_back, "x", -1)
    q_side = {s: around(query_narrow, "x", s) for s in (1, 2, 3)}

    wide_sources = [(key_wide, values), (xk_near, xv_near), (xk_far, xv_far), (xk_back, xv_back)]
    narrow_sources = [(kv_narrow,)] + [(kv_below[d],) for d in (1, 2, 3)]

    def plan(*numbers):
        return jnp.stack([jnp.asarray(n, jnp.int32) for n in numbers])

    def wide(numbers, queries, sources, diagonal):
        return attend(numbers, queries, sources, True, diagonal, False, size_wide, width_wide)

    def narrow(numbers, queries, sources, diagonal, fill):
        return attend(numbers, queries, sources, False, diagonal, fill, size_narrow, width_narrow)

    one = jnp.int32(1)
    diag_wide = wide(plan(1, 1, 0), query_wide, wide_sources[:1], True)
    diag_narrow = narrow(
        after(plan(1, 1, 0), diag_wide), query_narrow, narrow_sources[:1], True, False,
    )
    last = diag_narrow
    made = {}
    for d in (2, 1, 3):
        numbers = plan((z + d < RING), RING, 0)
        last = wide(after(numbers, last), q_later[d], wide_sources, False)
        made[d] = last
    relayed = lax.ppermute(made[2], "z", [(0, 3), (1, 2)])
    sent = {d: onward(made[d], "z", d) for d in (1, 3)}
    narrow_parts = []
    for s in (2, 1, 3):
        level = (lax.rem(x - s + RING, RING) > x).astype(jnp.int32)
        numbers = plan((z > 0) | (level > 0), z + level, 1 - level)
        last = narrow(after(numbers, last), q_side[s], narrow_sources, False, True)
        narrow_parts.append(around(last, "x", -s))
    sent[2] = lax.ppermute(after(relayed, last), "z", [(3, 2), (2, 3)])
    rest_narrow = narrow(
        after(plan((z > 0), z, 1), last), query_narrow, narrow_sources, False, True
    )
    rest_wide = wide(after(plan((x > 0), x, 1), rest_narrow), query_wide, wide_sources, False)
    valid = jnp.stack(
        [
            jnp.stack([one, x > 0] + [z >= d for d in (2, 1, 3)]).astype(jnp.int32),
            jnp.stack(
                [one, z > 0] + [(z > 0) | (lax.rem(x + s, RING) < x) for s in (2, 1, 3)]
            ).astype(jnp.int32),
        ]
    )
    return merge(
        valid,
        mix_lambda,
        (
            [diag_wide, rest_wide] + [sent[d] for d in (2, 1, 3)],
            [diag_narrow, rest_narrow] + narrow_parts,
        ),
        (width_wide, width_narrow),
    )


def project_kernel(
    token_of, mine, weight_wide, weight_narrow, residual, gain, stream_out, rows_out, stream_scr, squares, flat_scr, rows
):
    step = pl.program_id(0)
    heads, tokens, _ = mine.shape
    columns = weight_wide.shape[1]
    wide = weight_wide.shape[0] // heads
    model = stream_scr.shape[1]
    tiles = model // LANES
    made = residual[...].astype(jnp.float32)
    for h in range(heads):
        made = made + jnp.dot(
            mine[h, :, :wide],
            weight_wide[h * wide : (h + 1) * wide, :],
            preferred_element_type=jnp.float32,
        )
    stacked = jnp.concatenate([mine[h, :, wide:] for h in range(heads)], axis=1)
    made = made + jnp.dot(stacked, weight_narrow[...], preferred_element_type=jnp.float32)
    rounded = made.astype(jnp.bfloat16)
    stream_out[...] = rounded
    stream = rounded.astype(jnp.float32)
    stream_scr[:, pl.ds(pl.multiple_of(step * columns, columns), columns)] = stream
    square = jnp.sum(stream * stream, axis=1, keepdims=True)

    @pl.when(step == 0)
    def _():
        squares[...] = jnp.broadcast_to(square, squares.shape)

    @pl.when(step > 0)
    def _():
        squares[...] = squares[...] + square

    @pl.when(step == pl.num_programs(0) - 1)
    def _():
        inverse = lax.rsqrt(squares[...] / model + 1e-06)
        for j in range(tiles):
            lanes = slice(j * LANES, (j + 1) * LANES)
            flat_scr[pl.ds(j, tokens, stride=tiles), :] = (
                stream_scr[:, lanes] * inverse * gain[:, lanes]
            )
        rows[...] = flat_scr[...].reshape(tokens, tiles, LANES).astype(jnp.bfloat16)

        def copy_row(slot, _):
            rows_out[slot] = rows[token_of[slot]]
            return 0

        lax.fori_loop(0, rows_out.shape[0], copy_row, 0, unroll=16)


def project(token_of, mine, weight_wide, weight_narrow, residual, gain):
    heads, tokens, depth = mine.shape
    model = weight_wide.shape[1]
    slots = token_of.shape[0]
    tiles = model // LANES
    columns = 2 * BLOCK
    return pl.pallas_call(
        project_kernel,
        grid=(model // columns,),
        out_shape=(
            jax.ShapeDtypeStruct((tokens, model), jnp.bfloat16),
            jax.ShapeDtypeStruct((slots, tiles, LANES), jnp.bfloat16),
        ),
        in_specs=[
            pl.BlockSpec(memory_space=pltpu.SMEM),
            pl.BlockSpec((heads, tokens, depth), lambda i: (0, 0, 0)),
            pl.BlockSpec((weight_wide.shape[0], columns), lambda i: (0, i)),
            pl.BlockSpec((weight_narrow.shape[0], columns), lambda i: (0, i)),
            pl.BlockSpec((tokens, columns), lambda i: (0, i)),
            pl.BlockSpec((1, model), lambda i: (0, 0)),
        ],
        out_specs=(
            pl.BlockSpec((tokens, columns), lambda i: (0, i)),
            pl.BlockSpec((slots, tiles, LANES), lambda i: (0, 0, 0)),
        ),
        scratch_shapes=[
            pltpu.VMEM((tokens, model), jnp.float32),
            pltpu.VMEM((tokens, LANES), jnp.float32),
            pltpu.VMEM((tokens * tiles, LANES), jnp.float32),
            pltpu.VMEM((tokens, tiles, LANES), jnp.bfloat16),
        ],
        name="project",
    )(token_of, mine, weight_wide, weight_narrow, residual, gain)


def expert_kernel(
    arrived, gate, up, down, out, gate_scr, up_scr, down_scr, flat, rows, hidden, sems
):
    count, tiles, _ = arrived.shape
    model, inner = gate.shape
    steps = inner // BLOCK
    columns = model // steps

    def inner_part(k):
        return pl.ds(pl.multiple_of(k * BLOCK, BLOCK), BLOCK)

    def outer_part(k):
        return pl.ds(pl.multiple_of(k * columns, columns), columns)

    def in_copies(k):
        part = inner_part(k)
        return (
            pltpu.make_async_copy(gate.at[:, part], gate_scr.at[:, part], sems.at[0, k]),
            pltpu.make_async_copy(up.at[:, part], up_scr.at[:, part], sems.at[1, k]),
        )

    def out_copy(k):
        part = outer_part(k)
        return pltpu.make_async_copy(down.at[:, part], down_scr.at[:, part], sems.at[2, k])

    def spread(k, _):
        some = arrived[pl.ds(k * SOME, SOME)].astype(jnp.float32)
        flat[pl.ds(pl.multiple_of(k * SOME * tiles, LANES), SOME * tiles), :] = some.reshape(
            SOME * tiles, LANES
        )
        return 0

    def gathered(k, _):
        some = flat[pl.ds(pl.multiple_of(k * SOME * tiles, LANES), SOME * tiles), :]
        out[pl.ds(k * SOME, SOME)] = some.reshape(SOME, tiles, LANES).astype(jnp.bfloat16)
        return 0

    for k in range(steps):
        for made in in_copies(k):
            made.start()
    for k in range(steps):
        out_copy(k).start()
    lax.fori_loop(0, count // SOME, spread, 0)
    for j in range(tiles):
        rows[:, j * LANES : (j + 1) * LANES] = flat[pl.ds(j, count, stride=tiles), :].astype(
            jnp.bfloat16
        )

    def widen(k, _):
        for made in in_copies(k):
            made.wait()
        part = inner_part(k)
        gate_part = jnp.dot(rows[...], gate_scr[:, part], preferred_element_type=jnp.float32)
        up_part = jnp.dot(rows[...], up_scr[:, part], preferred_element_type=jnp.float32)
        hidden[:, part] = (gate_part * jax.nn.sigmoid(gate_part) * up_part).astype(jnp.bfloat16)
        return 0

    def narrow(k, _):
        out_copy(k).wait()
        result = jnp.dot(
            hidden[...], down_scr[:, outer_part(k)], preferred_element_type=jnp.float32
        )
        for j in range(columns // LANES):
            flat[pl.ds(k * (columns // LANES) + j, count, stride=tiles), :] = result[
                :, j * LANES : (j + 1) * LANES
            ]
        return 0

    lax.fori_loop(0, steps, widen, 0)
    lax.fori_loop(0, steps, narrow, 0)
    lax.fori_loop(0, count // SOME, gathered, 0)


def experts(arrived, gate, up, down):
    count, tiles, _ = arrived.shape
    model, inner = gate.shape
    steps = inner // BLOCK
    return pl.pallas_call(
        expert_kernel,
        out_shape=jax.ShapeDtypeStruct(arrived.shape, jnp.bfloat16),
        in_specs=[pl.BlockSpec(memory_space=pltpu.VMEM)]
        + [pl.BlockSpec(memory_space=pl.ANY)] * 3,
        out_specs=pl.BlockSpec(memory_space=pltpu.VMEM),
        scratch_shapes=[
            pltpu.VMEM((model, inner), jnp.bfloat16),
            pltpu.VMEM((model, inner), jnp.bfloat16),
            pltpu.VMEM((inner, model), jnp.bfloat16),
            pltpu.VMEM((count * tiles, LANES), jnp.float32),
            pltpu.VMEM((count, model), jnp.bfloat16),
            pltpu.VMEM((count, inner), jnp.bfloat16),
            pltpu.SemaphoreType.DMA((3, steps)),
        ],
        name="experts",
    )(arrived, gate, up, down)


def combine_kernel(slot_of, share_of, returned, stream, out, flat):
    tokens, model = stream.shape
    tiles = model // LANES

    def one_token(token, _):
        total = share_of[2 * token] * returned[slot_of[2 * token]].astype(jnp.float32)
        total = total + share_of[2 * token + 1] * returned[slot_of[2 * token + 1]].astype(
            jnp.float32
        )
        flat[pl.ds(pl.multiple_of(token * tiles, tiles), tiles), :] = total
        return 0

    lax.fori_loop(0, tokens, one_token, 0, unroll=8)
    for j in range(tiles):
        lanes = slice(j * LANES, (j + 1) * LANES)
        out[:, lanes] = (
            stream[:, lanes].astype(jnp.float32) + flat[pl.ds(j, tokens, stride=tiles), :]
        ).astype(jnp.bfloat16)


def combine(slot_of, share_of, returned, stream):
    tokens, model = stream.shape
    return pl.pallas_call(
        combine_kernel,
        out_shape=jax.ShapeDtypeStruct(stream.shape, jnp.bfloat16),
        in_specs=[pl.BlockSpec(memory_space=pltpu.SMEM)] * 2
        + [pl.BlockSpec(memory_space=pltpu.VMEM)] * 2,
        out_specs=pl.BlockSpec(memory_space=pltpu.VMEM),
        scratch_shapes=[pltpu.VMEM((tokens * (model // LANES), LANES), jnp.float32)],
        name="combine",
    )(slot_of, share_of, returned, stream)


def slot_tables(expert_ids, experts_all, capacity):
    flat_expert = expert_ids.reshape(-1)
    order = jnp.arange(flat_expert.shape[0], dtype=jnp.int32)
    earlier = (flat_expert[:, None] == flat_expert[None, :]) & (order[None, :] < order[:, None])
    slot_of = flat_expert * capacity + jnp.sum(earlier.astype(jnp.int32), axis=1)
    slot_ids = jnp.arange(experts_all * capacity, dtype=jnp.int32)
    placed = slot_ids[:, None] == slot_of[None, :]
    token_of = jnp.sum(jnp.where(placed, order[None, :] // 2, 0), axis=1)
    return slot_of, token_of


def shards(
    query_wide,
    key_wide,
    value_wide,
    query_narrow,
    key_narrow,
    value_narrow,
    mix_lambda,
    residual_in,
    out_wide,
    out_narrow,
    ffn_gain,
    expert_ids,
    expert_weights,
    gate_weight,
    up_weight,
    down_weight,
):
    heads = attention(
        query_wide[:, 0],
        key_wide[:, 0],
        value_wide[:, 0],
        query_narrow[:, 0],
        key_narrow[:, 0],
        value_narrow[:, 0],
        mix_lambda,
    )
    tp_size = lax.axis_size(TP)
    local_rows = heads.shape[0] // tp_size
    experts_all = lax.axis_size(SP_TP)
    capacity = max(2, 4 * local_rows // experts_all)
    slot_of, token_of = slot_tables(expert_ids, experts_all, capacity)
    whole_wide = lax.all_gather(out_wide, TP, axis=0, tiled=True)
    whole_narrow = lax.all_gather(out_narrow, TP, axis=0, tiled=True)
    mine = lax.all_to_all(
        heads.reshape(tp_size, local_rows, -1), TP, split_axis=0, concat_axis=0, tiled=True
    )
    stream, outgoing = project(
        token_of, mine, whole_wide, whole_narrow, residual_in, ffn_gain[None, :]
    )

    def exchanged(rows):
        shape = rows.shape
        moved = lax.all_to_all(
            rows.reshape(experts_all, -1, LANES), SP_TP, split_axis=0, concat_axis=0, tiled=True
        )
        return moved.reshape(shape)

    result = experts(exchanged(outgoing), gate_weight[0], up_weight[0], down_weight[0])
    return combine(slot_of, expert_weights.reshape(-1), exchanged(result), stream)


def solution(mesh):
    finer = Mesh(mesh.devices.reshape(4, 4, 4, 2), SP_TP)
    sp = ("z", "x")
    placed = (
        P(sp, TP, None),
        P(sp, TP, None),
        P(sp, TP, None),
        P(sp, TP, None),
        P(sp, TP, None),
        P(sp, TP, None),
        P(None, TP),
        P(SP_TP, None),
        P(TP, None),
        P(TP, None),
        P(),
        P(SP_TP, None),
        P(SP_TP, None),
        P(SP_TP, None, None),
        P(SP_TP, None, None),
        P(SP_TP, None, None),
    )
    return jax.shard_map(
        shards, mesh=finer, in_specs=placed, out_specs=P(SP_TP, None), check_vma=False
    )
```

profile of v0, /device:TPU:1, one launch (start us, length us, event | category | flops | bytes accessed | tf_op | source)
XLA Modules:
  0.0 349.0 jit_solution(8430741096512070780)
XLA Ops:
  10.2 3.3 collective-permute-start.4
  13.7 2.5 collective-permute-start.6
  17.6 4.3 %shard_map.154.refs_2_ = bf16[528,768]{1,0:T(8,128)(2,1)} custom-call(s32[3]{0:T(128)} %constant.55.clone.1.refs_0_, bf16[768,256]{1,0:T(8,128)(2,1)} %bitcast.54, bf16[768,256]{1,0:T(8,128)(2,1)} %bitcast.60, bf16[768,256]{1,0:T(8,128)(2,1)} %get-tuple-element.19.refs_3_), custom_call_target="tpu_custom_call" | custom-call | flops 1811939328 | bytes 786432 | tf_op jit(solution)/shard_map/pallas_call | solution.py:268
  25.0 3.7 %shard_map.155.refs_7_ = bf16[272,768]{1,0:T(8,128)(2,1)} custom-call(s32[3]{0:T(128)} %constant.55.clone.1.refs_0_, bf16[768,128]{1,0:T(8,128)(2,1)} %bitcast.65, bf16[768,256]{1,0:T(8,128)(2,1)} %get-tuple-element.21.refs_2_), custom_call_target="tpu_custom_call" | custom-call | flops 905969664 | bytes 393216 | tf_op jit(solution)/shard_map/pallas_call | solution.py:268
  29.9 3.3 collective-permute-done.2.refs_5_
  36.5 4.3 %collective-permute-start.10 = (bf16[768,256]{1,0:T(8,128)(2,1)S(1)}, bf16[768,256]{1,0:T(8,128)(2,1)S(1)}, u32[]{:S(2)}, u32[]{:S(2)}) collective-permute-start(bf16[768,256]{1,0:T(8,128)(2,1)S(1)} %copy-done.12), channel_id=1, source_target_pairs={{0,32},{32,64},{64,96},{1,33},{33,65},{65,97},{2,34},{34,66},{66,9... | collective-permute-start | bytes 1179656 | tf_op jit(solution)/shard_map/ppermute | solution.py:351
  42.4 43.6 %shard_map.156 = bf16[528,768]{1,0:T(8,128)(2,1)} custom-call(s32[3]{0:T(128)} %pad_add_fusion.1.refs_0_, bf16[768,256]{1,0:T(8,128)(2,1)} %collective-permute-done.refs_1_, bf16[768,256]{1,0:T(8,128)(2,1)} %bitcast.61, bf16[768,256]{1,0:T(8,128)(2,1)} %get-tuple-element.19.refs_3_, bf16[768,256]{1,0:T(8,128)(2,1)} %copy-done.13, ...), custom_call_target="tpu_custom_call" | custom-call | flops 1811939328 | bytes 3145728 | tf_op jit(solution)/shard_map/pallas_call | solution.py:268
  92.3 9.3 %shard_map.157 = bf16[528,768]{1,0:T(8,128)(2,1)} custom-call(s32[3]{0:T(128)} %pad_add_fusion.2.refs_0_, bf16[768,256]{1,0:T(8,128)(2,1)} %collective-permute-done.7.refs_1_, bf16[768,256]{1,0:T(8,128)(2,1)} %bitcast.62, bf16[768,256]{1,0:T(8,128)(2,1)} %get-tuple-element.19.refs_3_, bf16[768,256]{1,0:T(8,128)(2,1)} %copy-done.13, ...), custom_call_target="tpu_custom_call" | custom-call | flops 1811939328 | bytes 3145728 | tf_op jit(solution)/shard_map/pallas_call | solution.py:268
  101.6 2.6 collective-permute-start.14
  104.3 43.6 %shard_map.158 = bf16[528,768]{1,0:T(8,128)(2,1)} custom-call(s32[3]{0:T(128)} %pad_add_fusion.3.refs_0_, bf16[768,256]{1,0:T(8,128)(2,1)} %collective-permute-done.8.refs_1_, bf16[768,256]{1,0:T(8,128)(2,1)} %bitcast.63, bf16[768,256]{1,0:T(8,128)(2,1)} %get-tuple-element.19.refs_3_, bf16[768,256]{1,0:T(8,128)(2,1)} %copy-done.13, ...), custom_call_target="tpu_custom_call" | custom-call | flops 1811939328 | bytes 3145728 | tf_op jit(solution)/shard_map/pallas_call | solution.py:268
  149.4 3.9 %shard_map.159 = bf16[272,768]{1,0:T(8,128)(2,1)} custom-call(s32[3]{0:T(128)} %pad_add_fusion.11.refs_0_, bf16[768,128]{1,0:T(8,128)(2,1)} %collective-permute-done.9.refs_1_, bf16[768,256]{1,0:T(8,128)(2,1)} %get-tuple-element.21.refs_2_, bf16[768,256]{1,0:T(8,128)(2,1)} %copy-done.18, bf16[768,256]{1,0:T(8,128)(2,1)} %copy-done.19, ...), custom_call_target="tpu_custom_call" | custom-call | flops 905969664 | bytes 1572864 | tf_op jit(solution)/shard_map/pallas_call | solution.py:268
  154.0 3.8 %shard_map.160 = bf16[272,768]{1,0:T(8,128)(2,1)} custom-call(s32[3]{0:T(128)} %pad_add_fusion.10.refs_0_, bf16[768,128]{1,0:T(8,128)(2,1)} %copy-done.22, bf16[768,256]{1,0:T(8,128)(2,1)} %get-tuple-element.21.refs_2_, bf16[768,256]{1,0:T(8,128)(2,1)} %copy-done.18, bf16[768,256]{1,0:T(8,128)(2,1)} %copy-done.19, bf16[768,256]{1,0:T(8,128)(2,1)} %copy-done.20), custom_call_target="tpu_custom_call" | custom-call | flops 905969664 | bytes 1572864 | tf_op jit(solution)/shard_map/pallas_call | solution.py:268
  158.5 3.9 %shard_map.161 = bf16[272,768]{1,0:T(8,128)(2,1)} custom-call(s32[3]{0:T(128)} %pad_add_fusion.9.refs_0_, bf16[768,128]{1,0:T(8,128)(2,1)} %copy-done.23, bf16[768,256]{1,0:T(8,128)(2,1)} %get-tuple-element.21.refs_2_, bf16[768,256]{1,0:T(8,128)(2,1)} %copy-done.18, bf16[768,256]{1,0:T(8,128)(2,1)} %copy-done.19, bf16[768,256]{1,0:T(8,128)(2,1)} %copy-done.20), custom_call_target="tpu_custom_call" | custom-call | flops 905969664 | bytes 1572864 | tf_op jit(solution)/shard_map/pallas_call | solution.py:268
  166.5 22.8 %collective-permute-start.20 = (bf16[272,768]{1,0:T(8,128)(2,1)}, bf16[272,768]{1,0:T(8,128)(2,1)S(1)}, u32[]{:S(2)}, u32[]{:S(2)}) collective-permute-start(bf16[272,768]{1,0:T(8,128)(2,1)} %shard_map.160), channel_id=1, source_target_pairs={{0,24},{8,0},{16,8},{24,16},{1,25},{9,1},{17,9},{25,17},{2,26},{10... | collective-permute-start | bytes 1253384 | tf_op jit(solution)/shard_map/ppermute | solution.py:347
  194.9 11.3 %collective-permute-done.20.refs_10_ = bf16[272,768]{1,0:T(8,128)(2,1)S(1)} collective-permute-done((bf16[272,768]{1,0:T(8,128)(2,1)}, bf16[272,768]{1,0:T(8,128)(2,1)S(1)}, u32[]{:S(2)}, u32[]{:S(2)}) %collective-permute-start.20) | collective-permute-done | bytes 417824 | tf_op jit(solution)/shard_map/ppermute | solution.py:347
  208.4 5.4 %merge_reads.1 = bf16[768,384]{1,0:T(8,128)(2,1)} custom-call(s32[2,5]{1,0:T(2,128)} %pad_add_fusion.refs_0_, f32[2,1]{1,0:T(2,128)} %copy.23.refs_1_, bf16[528,768]{1,0:T(8,128)(2,1)} %shard_map.154.refs_2_, bf16[528,768]{1,0:T(8,128)(2,1)} %shard_map.163.refs_3_, bf16[528,768]{1,0:T(8,128)(2,1)} %copy-done.4, bf16[528,768]{1,0:T(8,128)(2,1)} %copy-done.3, ...), custom_call_target="tpu_custom_call" | custom-call | tf_op jit(solution)/shard_map/merge_reads/pallas_call | solution.py:335
  213.8 6.5 %all-to-all-start = ((bf16[8,96,384]{2,1,0:T(8,128)(2,1)}), bf16[8,96,384]{2,1,0:T(8,128)(2,1)S(1)}, u32[]{:S(2)}, u32[]{:S(2)}) async-start(bf16[8,96,384]{2,1,0:T(8,128)(2,1)} %bitcast.45), calls=%async_computation | async-start | bytes 1179648 | tf_op jit(solution)/shard_map/all_to_all | solution.py:693
  221.5 8.9 %all-to-all-done.mine = bf16[8,96,384]{2,1,0:T(8,128)(2,1)S(1)} async-done(((bf16[8,96,384]{2,1,0:T(8,128)(2,1)}), bf16[8,96,384]{2,1,0:T(8,128)(2,1)S(1)}, u32[]{:S(2)}, u32[]{:S(2)}) %all-to-all-start) | async-done | bytes 589856 | tf_op jit(solution)/shard_map/all_to_all | solution.py:693
  231.2 9.2 %project.1 = (bf16[96,2048]{1,0:T(8,128)(2,1)}, bf16[384,16,128]{2,1,0:T(8,128)(2,1)}) custom-call(s32[384]{0:T(512)} %select_reduce_fusion.token_of, bf16[8,96,384]{2,1,0:T(8,128)(2,1)} %copy-done.1, bf16[2048,2048]{1,0:T(8,128)(2,1)} %all-gather.3.cloned.1.call-done.weight_wide, bf16[1024,2048]{1,0:T(8,128)(2,1)} %all-gather.5.cloned.1.call-done.weight_narrow, ...), custom_call_target="tpu_custom_call" | custom-call | tf_op jit(solution)/shard_map/project/pallas_call | solution.py:490
  240.4 56.8 %all_to_all.15 = bf16[128,48,128]{2,1,0:T(8,128)(2,1)} all-to-all(bf16[128,48,128]{2,1,0:T(8,128)(2,1)} %bitcast.46), channel_id=1, replica_groups=mesh['z'=4,'x'=4,'y'=4,'c'=2] {'z','x','y','c'}, dimensions={0} | all-to-all | bytes 3145728 | tf_op jit(solution)/shard_map/all_to_all | solution.py:702
  297.3 11.5 %experts.1 = bf16[384,16,128]{2,1,0:T(8,128)(2,1)} custom-call(bf16[384,16,128]{2,1,0:T(8,128)(2,1)} %bitcast.41, bf16[2048,1024]{1,0:T(8,128)(2,1)} %bitcast.42, bf16[2048,1024]{1,0:T(8,128)(2,1)} %bitcast.43, bf16[1024,2048]{1,0:T(8,128)(2,1)} %bitcast.44), custom_call_target="tpu_custom_call" | custom-call | tf_op jit(solution)/shard_map/experts/pallas_call | solution.py:596
  308.8 4.9 %all-to-all-start.2 = ((bf16[128,48,128]{2,1,0:T(8,128)(2,1)}), bf16[128,48,128]{2,1,0:T(8,128)(2,1)S(1)}, u32[]{:S(2)}, u32[]{:S(2)}) async-start(bf16[128,48,128]{2,1,0:T(8,128)(2,1)} %bitcast.40), calls=%async_computation.2 | async-start | bytes 3145728 | tf_op jit(solution)/shard_map/all_to_all | solution.py:702
  314.5 23.7 %all-to-all-done.2 = bf16[128,48,128]{2,1,0:T(8,128)(2,1)S(1)} async-done(((bf16[128,48,128]{2,1,0:T(8,128)(2,1)}), bf16[128,48,128]{2,1,0:T(8,128)(2,1)S(1)}, u32[]{:S(2)}, u32[]{:S(2)}) %all-to-all-start.2) | async-done | bytes 1572896 | tf_op jit(solution)/shard_map/all_to_all | solution.py:702
  339.3 2.9 combine.1
  (116 shorter events, 39.1 us)
Async XLA Ops:
  6.5 223.9 %all-gather.5.cloned.1.call-start = ((), (), s32[]{:S(2)}) async-start(), calls=%async_computation.4 | async-start | bytes 4718592 | tf_op jit(solution)/shard_map/all_gather | solution.py:692
  7.3 223.2 %all-gather.3.cloned.1.call-start = ((), (), s32[]{:S(2)}) async-start(), calls=%async_computation.3 | async-start | bytes 9437184 | tf_op jit(solution)/shard_map/all_gather | solution.py:691
  13.5 19.7 %collective-permute-start.2 = (bf16[768,256]{1,0:T(8,128)(2,1)}, bf16[768,256]{1,0:T(8,128)(2,1)S(1)}, u32[]{:S(2)}, u32[]{:S(2)}) collective-permute-start(bf16[768,256]{1,0:T(8,128)(2,1)} %get-tuple-element.19.refs_3_), channel_id=1, source_target_pairs={{0,8},{8,16},{16,24},{24,0},{1,9},{9,17},{17,25},{25,1},{2,10},{10... | collective-permute-start | bytes 1179656 | tf_op jit(solution)/shard_map/ppermute | solution.py:347
  13.7 21.4 %collective-permute-start.6 = (bf16[768,256]{1,0:T(8,128)(2,1)}, bf16[768,256]{1,0:T(8,128)(2,1)S(1)}, u32[]{:S(2)}, u32[]{:S(2)}) collective-permute-start(bf16[768,256]{1,0:T(8,128)(2,1)} %bitcast.59), channel_id=1, source_target_pairs={{0,24},{8,0},{16,8},{24,16},{1,25},{9,1},{17,9},{25,17},{2,26},{10... | collective-permute-start | bytes 1179656 | tf_op jit(solution)/shard_map/ppermute | solution.py:347
  16.2 20.2 %collective-permute-start = (bf16[768,256]{1,0:T(8,128)(2,1)}, bf16[768,256]{1,0:T(8,128)(2,1)}, u32[]{:S(2)}, u32[]{:S(2)}) collective-permute-start(bf16[768,256]{1,0:T(8,128)(2,1)} %bitcast.53), channel_id=1, source_target_pairs={{64,0},{96,32},{65,1},{97,33},{66,2},{98,34},{67,3},{99,35},{68,4}... | collective-permute-start | bytes 1179656 | tf_op jit(solution)/shard_map/ppermute | solution.py:351
  22.5 18.3 %collective-permute-start.5 = (bf16[768,256]{1,0:T(8,128)(2,1)S(1)}, bf16[768,256]{1,0:T(8,128)(2,1)S(1)}, u32[]{:S(2)}, u32[]{:S(2)}) collective-permute-start(bf16[768,256]{1,0:T(8,128)(2,1)S(1)} %collective-permute-done.4.refs_9_), channel_id=1, source_target_pairs={{0,24},{8,0},{16,8},{24,16},{1,25},{9,1},{17,9},{25,17},{2,26},{10... | collective-permute-start | bytes 1179656 | tf_op jit(solution)/shard_map/ppermute | solution.py:347
  25.0 16.7 %collective-permute-start.3 = (bf16[768,256]{1,0:T(8,128)(2,1)S(1)}, bf16[768,256]{1,0:T(8,128)(2,1)S(1)}, u32[]{:S(2)}, u32[]{:S(2)}) collective-permute-start(bf16[768,256]{1,0:T(8,128)(2,1)S(1)} %collective-permute-done.1.refs_4_), channel_id=1, source_target_pairs={{0,8},{8,16},{16,24},{24,0},{1,9},{9,17},{17,25},{25,1},{2,10},{10... | collective-permute-start | bytes 1179656 | tf_op jit(solution)/shard_map/ppermute | solution.py:347
  33.2 57.1 %collective-permute-start.7 = (bf16[768,256]{1,0:T(8,128)(2,1)S(1)}, bf16[768,256]{1,0:T(8,128)(2,1)}, u32[]{:S(2)}, u32[]{:S(2)}) collective-permute-start(bf16[768,256]{1,0:T(8,128)(2,1)S(1)} %bitcast.56), channel_id=1, source_target_pairs={{32,0},{64,32},{96,64},{33,1},{65,33},{97,65},{34,2},{66,34},{98,6... | collective-permute-start | bytes 1179656 | tf_op jit(solution)/shard_map/ppermute | solution.py:351
  35.2 66.4 %collective-permute-start.8 = (bf16[768,256]{1,0:T(8,128)(2,1)S(1)}, bf16[768,256]{1,0:T(8,128)(2,1)}, u32[]{:S(2)}, u32[]{:S(2)}) collective-permute-start(bf16[768,256]{1,0:T(8,128)(2,1)S(1)} %bitcast.57), channel_id=1, source_target_pairs={{96,0},{97,1},{98,2},{99,3},{100,4},{101,5},{102,6},{103,7},{104,8... | collective-permute-start | bytes 1179656 | tf_op jit(solution)/shard_map/ppermute | solution.py:351
  36.5 65.2 %collective-permute-start.10 = (bf16[768,256]{1,0:T(8,128)(2,1)S(1)}, bf16[768,256]{1,0:T(8,128)(2,1)S(1)}, u32[]{:S(2)}, u32[]{:S(2)}) collective-permute-start(bf16[768,256]{1,0:T(8,128)(2,1)S(1)} %copy-done.12), channel_id=1, source_target_pairs={{0,32},{32,64},{64,96},{1,33},{33,65},{65,97},{2,34},{34,66},{66,9... | collective-permute-start | bytes 1179656 | tf_op jit(solution)/shard_map/ppermute | solution.py:351
  40.8 48.2 %collective-permute-start.9 = (bf16[768,128]{1,0:T(8,128)(2,1)}, bf16[768,128]{1,0:T(8,128)(2,1)}, u32[]{:S(2)}, u32[]{:S(2)}) collective-permute-start(bf16[768,128]{1,0:T(8,128)(2,1)} %bitcast.66), channel_id=1, source_target_pairs={{0,16},{8,24},{16,0},{24,8},{1,17},{9,25},{17,1},{25,9},{2,18},{10... | collective-permute-start | bytes 589832 | tf_op jit(solution)/shard_map/ppermute | solution.py:347
  86.0 79.1 %collective-permute-start.15 = (bf16[528,768]{1,0:T(8,128)(2,1)}, bf16[528,768]{1,0:T(8,128)(2,1)}, u32[]{:S(2)}, u32[]{:S(2)}) collective-permute-start(bf16[528,768]{1,0:T(8,128)(2,1)} %shard_map.156), channel_id=1, source_target_pairs={{0,96},{32,64},{1,97},{33,65},{2,98},{34,66},{3,99},{35,67},{4,100... | collective-permute-start | bytes 2433032 | tf_op jit(solution)/shard_map/ppermute | solution.py:403
  89.0 58.8 %collective-permute-start.11 = (bf16[768,256]{1,0:T(8,128)(2,1)S(1)}, bf16[768,256]{1,0:T(8,128)(2,1)S(1)}, u32[]{:S(2)}, u32[]{:S(2)}) collective-permute-start(bf16[768,256]{1,0:T(8,128)(2,1)S(1)} %copy-done.12), channel_id=1, source_target_pairs={{0,64},{32,96},{1,65},{33,97},{2,66},{34,98},{3,67},{35,99},{4,68}... | collective-permute-start | bytes 1179656 | tf_op jit(solution)/shard_map/ppermute | solution.py:351
  90.3 57.5 %collective-permute-start.12 = (bf16[768,256]{1,0:T(8,128)(2,1)S(1)}, bf16[768,256]{1,0:T(8,128)(2,1)S(1)}, u32[]{:S(2)}, u32[]{:S(2)}) collective-permute-start(bf16[768,256]{1,0:T(8,128)(2,1)S(1)} %copy-done.12), channel_id=1, source_target_pairs={{0,96},{1,97},{2,98},{3,99},{4,100},{5,101},{6,102},{7,103},{8,104... | collective-permute-start | bytes 1179656 | tf_op jit(solution)/shard_map/ppermute | solution.py:351
  101.5 51.7 %collective-permute-start.13 = (bf16[768,128]{1,0:T(8,128)(2,1)S(1)}, bf16[768,128]{1,0:T(8,128)(2,1)S(1)}, u32[]{:S(2)}, u32[]{:S(2)}) collective-permute-start(bf16[768,128]{1,0:T(8,128)(2,1)S(1)} %bitcast.68), channel_id=1, source_target_pairs={{0,8},{8,16},{16,24},{24,0},{1,9},{9,17},{17,25},{25,1},{2,10},{10... | collective-permute-start | bytes 589832 | tf_op jit(solution)/shard_map/ppermute | solution.py:347
  101.6 56.2 %collective-permute-start.14 = (bf16[768,128]{1,0:T(8,128)(2,1)S(1)}, bf16[768,128]{1,0:T(8,128)(2,1)S(1)}, u32[]{:S(2)}, u32[]{:S(2)}) collective-permute-start(bf16[768,128]{1,0:T(8,128)(2,1)S(1)} %bitcast.69), channel_id=1, source_target_pairs={{0,24},{8,0},{16,8},{24,16},{1,25},{9,1},{17,9},{25,17},{2,26},{10... | collective-permute-start | bytes 589832 | tf_op jit(solution)/shard_map/ppermute | solution.py:347
  162.4 26.9 %collective-permute-start.21 = (bf16[272,768]{1,0:T(8,128)(2,1)}, bf16[272,768]{1,0:T(8,128)(2,1)S(1)}, u32[]{:S(2)}, u32[]{:S(2)}) collective-permute-start(bf16[272,768]{1,0:T(8,128)(2,1)} %shard_map.161), channel_id=1, source_target_pairs={{0,8},{8,16},{16,24},{24,0},{1,9},{9,17},{17,25},{25,1},{2,10},{10... | collective-permute-start | bytes 1253384 | tf_op jit(solution)/shard_map/ppermute | solution.py:347
  162.5 43.7 %collective-permute-start.18 = (bf16[528,768]{1,0:T(8,128)(2,1)}, bf16[528,768]{1,0:T(8,128)(2,1)S(1)}, u32[]{:S(2)}, u32[]{:S(2)}) collective-permute-start(bf16[528,768]{1,0:T(8,128)(2,1)} %shard_map.158), channel_id=1, source_target_pairs={{0,96},{1,97},{2,98},{3,99},{4,100},{5,101},{6,102},{7,103},{8,104... | collective-permute-start | bytes 2433032 | tf_op jit(solution)/shard_map/ppermute | solution.py:351
  163.8 42.4 %collective-permute-start.17 = (bf16[528,768]{1,0:T(8,128)(2,1)}, bf16[528,768]{1,0:T(8,128)(2,1)S(1)}, u32[]{:S(2)}, u32[]{:S(2)}) collective-permute-start(bf16[528,768]{1,0:T(8,128)(2,1)} %shard_map.157), channel_id=1, source_target_pairs={{0,32},{32,64},{64,96},{1,33},{33,65},{65,97},{2,34},{34,66},{66,9... | collective-permute-start | bytes 2433032 | tf_op jit(solution)/shard_map/ppermute | solution.py:351
  165.2 41.0 %collective-permute-start.16 = (bf16[528,768]{1,0:T(8,128)(2,1)}, bf16[528,768]{1,0:T(8,128)(2,1)S(1)}, u32[]{:S(2)}, u32[]{:S(2)}) collective-permute-start(bf16[528,768]{1,0:T(8,128)(2,1)} %collective-permute-done.15), channel_id=1, source_target_pairs={{96,64},{64,96},{97,65},{65,97},{98,66},{66,98},{99,67},{67,99},{1... | collective-permute-start | bytes 2433032 | tf_op jit(solution)/shard_map/ppermute | solution.py:411
  166.5 39.7 %collective-permute-start.20 = (bf16[272,768]{1,0:T(8,128)(2,1)}, bf16[272,768]{1,0:T(8,128)(2,1)S(1)}, u32[]{:S(2)}, u32[]{:S(2)}) collective-permute-start(bf16[272,768]{1,0:T(8,128)(2,1)} %shard_map.160), channel_id=1, source_target_pairs={{0,24},{8,0},{16,8},{24,16},{1,25},{9,1},{17,9},{25,17},{2,26},{10... | collective-permute-start | bytes 1253384 | tf_op jit(solution)/shard_map/ppermute | solution.py:347
  189.3 16.9 %collective-permute-start.19 = (bf16[272,768]{1,0:T(8,128)(2,1)}, bf16[272,768]{1,0:T(8,128)(2,1)}, u32[]{:S(2)}, u32[]{:S(2)}) collective-permute-start(bf16[272,768]{1,0:T(8,128)(2,1)} %shard_map.159), channel_id=1, source_target_pairs={{0,16},{8,24},{16,0},{24,8},{1,17},{9,25},{17,1},{25,9},{2,18},{10... | collective-permute-start | bytes 1253384 | tf_op jit(solution)/shard_map/ppermute | solution.py:347
  213.8 16.6 %all-to-all-start = ((bf16[8,96,384]{2,1,0:T(8,128)(2,1)}), bf16[8,96,384]{2,1,0:T(8,128)(2,1)S(1)}, u32[]{:S(2)}, u32[]{:S(2)}) async-start(bf16[8,96,384]{2,1,0:T(8,128)(2,1)} %bitcast.45), calls=%async_computation | async-start | bytes 1179648 | tf_op jit(solution)/shard_map/all_to_all | solution.py:693
  308.8 29.4 %all-to-all-start.2 = ((bf16[128,48,128]{2,1,0:T(8,128)(2,1)}), bf16[128,48,128]{2,1,0:T(8,128)(2,1)S(1)}, u32[]{:S(2)}, u32[]{:S(2)}) async-start(bf16[128,48,128]{2,1,0:T(8,128)(2,1)} %bitcast.40), calls=%async_computation.2 | async-start | bytes 3145728 | tf_op jit(solution)/shard_map/all_to_all | solution.py:702
  (27 other events, 286.2 us)
Sparse Core Ops, SparseCore 0:
  9.0 35.6 all-gather.4
  46.5 49.6 all-gather.2
where the time goes:
time: 350 us; the launch traced here: 349 us
  Pallas kernels  149 us (43%)
  starting transfers between devices  63.4 us (18%)
  blocking collectives  56.8 us (16%)
  waiting for transfers between devices  49.3 us (14%)
  between operations  14 us (4%)
  local copies, waits for them, and re-layouts  9.67 us (3%)
  other arithmetic  6.39 us (2%)
    pallas_call x10, Pallas kernels, attend(): pl.pallas_call(body, out_shape=jax.ShapeDtypeStruct((2 * width + STAT_ROW...  118 us
    all_to_all x1, blocking collectives, exchanged(): lax.all_to_all(rows.reshape(experts_all, -1, LANES), SP_TP, split_axis=0,...  56.8 us
    ppermute x12, starting transfers between devices, around(): lax.ppermute(array, axis, [(k, (k + by) % RING) for k in range(RING)])  35.4 us
    all_to_all x1, waiting for transfers between devices, exchanged(): lax.all_to_all(rows.reshape(experts_all, -1, LANES), SP_TP, split_axis=0,...  23.7 us
    ppermute x12, waiting for transfers between devices, around(): lax.ppermute(array, axis, [(k, (k + by) % RING) for k in range(RING)])  15.3 us
    ppermute x8, starting transfers between devices, onward(): lax.ppermute(array, axis, [(k, k + by) for k in range(RING) if 0 <= k + b...  13.4 us
    pallas_call x1, Pallas kernels, experts(): pl.pallas_call(expert_kernel, out_shape=jax.ShapeDtypeStruct(arrived.shap...  11.5 us
    pallas_call x1, Pallas kernels, project(): pl.pallas_call(project_kernel, grid=(model // columns,), out_shape=(jax.S...  9.18 us
  transfers between devices with their start and end apart: 26, of which 5 were waited for; matrix products, arithmetic and copies ran while one was open for 2% of the time, Pallas kernels for 36%

commit v1 on v0

--- a/solution.py
+++ b/solution.py
@@ -15,6 +15,7 @@
 LANES = 128
 BLOCK = 256
 SOME = 48
+VALID_ROW = 8
 LEAST_TOTAL = 2.0**-60
 MOST_TOTAL = 2.0**100
 
@@ -46,12 +47,13 @@
     )(v_wide, k_narrow, v_narrow)
 
 
-def attend_kernel(plan, q_ref, *refs, pieces, wide, diagonal, fill, size, width, chunk):
-    slots = len(refs[: -7]) // pieces
-    src_refs = refs[: slots * pieces]
-    out_ref = refs[slots * pieces]
-    q_scr, kv_scr, acc, out_scr, sems, q_sem = refs[slots * pieces + 1 :]
-    active, count, offset = plan[0], plan[1], plan[2]
+def attend_kernel(table, *refs, rows, slots, pieces, wide, diagonal, fill, size, width, chunk):
+    chunks = len(rows)
+    q_refs = refs[:chunks]
+    src_refs = refs[chunks : chunks + slots * pieces]
+    out_refs = refs[chunks + slots * pieces : 2 * chunks + slots * pieces]
+    q_scr, kv_scr, acc, out_scr, sems, q_sems, out_sems = refs[2 * chunks + slots * pieces :]
+    plans = [(table[row, 0], table[row, 1], table[row, 2]) for row in rows]
     scale = size ** (-0.5) * LOG2E
     key_rows = chunk if wide else chunk // 2
     halves = key_rows // LANES
@@ -92,8 +94,8 @@
     def value_block(slot, j):
         return kv_scr[slot, pl.ds(key_rows + j * width, width), :]
 
-    def store_result(m, columns, read, total, level):
-        out_scr[pl.ds(m * width, width), columns] = (read * (1.0 / total)).astype(jnp.bfloat16)
+    def store_result(n, m, columns, read, total, level):
+        out_scr[n, pl.ds(m * width, width), columns] = (read * (1.0 / total)).astype(jnp.bfloat16)
         row = lax.broadcasted_iota(jnp.int32, (8, total.shape[1]), 0)
         packed = jnp.zeros((8, total.shape[1]), jnp.float32)
         for k in range(3):
@@ -102,23 +104,56 @@
             level = level - term
         return packed
 
-    @pl.when(active > 0)
-    def _():
-        got_q = pltpu.make_async_copy(q_ref, q_scr, q_sem)
-        got_q.start()
-        for slot in range(slots):
-
-            @pl.when((slot >= offset) & (slot < offset + count))
-            def _(slot=slot):
-                for made in slot_copies(slot):
-                    made.start()
-
+    def within(slot, plan):
+        active, count, offset = plan
+        return (active > 0) & (slot >= offset) & (slot < offset + count)
+
+    for n in range(chunks):
+
+        @pl.when(plans[n][0] > 0)
+        def _(n=n):
+            pltpu.make_async_copy(q_refs[n], q_scr.at[n], q_sems.at[n]).start()
+
+    for slot in range(slots):
+        used = within(slot, plans[0])
+        for plan in plans[1:]:
+            used = used | within(slot, plan)
+
+        @pl.when(used)
+        def _(slot=slot):
+            for made in slot_copies(slot):
+                made.start()
+
+    def one_chunk(n, _):
+        row = rows[0] + n
+        active, count, offset = table[row, 0], table[row, 1], table[row, 2]
+        pl.when(active > 0)(lambda: attend_chunk(n, count, offset))
+        if fill:
+
+            @pl.when(active == 0)
+            def _():
+                out_scr[n] = jnp.zeros(out_scr.shape[1:], out_scr.dtype)
+
+        for k in range(chunks):
+
+            @pl.when((n == k) & ((active > 0) | fill))
+            def _(k=k):
+                pltpu.make_async_copy(out_scr.at[k], out_refs[k], out_sems.at[k]).start()
+
+        return 0
+
+    def attend_chunk(n, count, offset):
         acc[...] = jnp.zeros_like(acc)
-        got_q.wait()
+        pltpu.make_async_copy(q_refs[0], q_scr.at[n], q_sems.at[n]).wait()
 
         def add_slot(number, totals):
             slot = 0 if diagonal else number + offset
-            wait_slot(slot)
+            if chunks > 1:
+                pl.when((n == 0) | jnp.logical_not(within(slot, plans[0])))(
+                    lambda: wait_slot(slot)
+                )
+            else:
+                wait_slot(slot)
             values = jnp.concatenate(
                 [value_block(slot, j) for j in range(chunk // BLOCK)], axis=1
             )
@@ -126,9 +161,9 @@
             for m in range(2):
                 if wide:
                     lanes = slice(m * size, (m + 1) * size)
-                    scores = dot_nt(kv_scr[slot, :key_rows, lanes], q_scr[:, lanes])
+                    scores = dot_nt(kv_scr[slot, :key_rows, lanes], q_scr[n, :, lanes])
                 else:
-                    queries = only_map(q_scr[...], m)
+                    queries = only_map(q_scr[n], m)
                     scores = jnp.concatenate(
                         [
                             dot_nt(kv_scr[slot, :key_rows, side * LANES : (side + 1) * LANES], queries)
@@ -159,8 +194,8 @@
             total = jnp.sum(totals[m], axis=0, keepdims=True)
             inside = (total >= LEAST_TOTAL) & (total <= MOST_TOTAL)
             outside = jnp.maximum(outside, jnp.where(inside, 0.0, 1.0))
-            stats.append(store_result(m, slice(None), acc[m], total, jnp.log2(total)))
-        out_scr[2 * width :, :] = jnp.concatenate(stats, axis=0).astype(jnp.bfloat16)
+            stats.append(store_result(n, m, slice(None), acc[m], total, jnp.log2(total)))
+        out_scr[n, 2 * width :, :] = jnp.concatenate(stats, axis=0).astype(jnp.bfloat16)
 
         @pl.when(jnp.max(outside) > 0)
         def _():
@@ -192,9 +227,9 @@
                         place = pl.ds(pl.multiple_of(block * BLOCK, BLOCK), BLOCK)
                         if wide:
                             lanes = pl.ds(pl.multiple_of(m * size, size), size)
-                            scores = dot_nt(kv_scr[slot, place, lanes], q_scr[columns, lanes])
+                            scores = dot_nt(kv_scr[slot, place, lanes], q_scr[n, columns, lanes])
                         else:
-                            scores = dot_nt(keys_at(slot, block), only_map(q_scr[columns, :], m))
+                            scores = dot_nt(keys_at(slot, block), only_map(q_scr[n, columns, :], m))
                         scores = scores * scale
                         if diagonal:
                             key_pos = block * BLOCK + lax.broadcasted_iota(
@@ -222,7 +257,7 @@
                         ),
                     )
                     rows = store_result(
-                        m, columns, acc[m, :, columns], total, peak + jnp.log2(total)
+                        n, m, columns, acc[m, :, columns], total, peak + jnp.log2(total)
                     )
                     both = jnp.concatenate([rows, rows], axis=0)
                     row = lax.broadcasted_iota(jnp.int32, both.shape, 0)
@@ -231,31 +266,32 @@
                 packed = lax.fori_loop(
                     0, 2, one_map, jnp.zeros((STAT_ROWS, BLOCK), jnp.float32)
                 )
-                out_scr[2 * width :, columns] = packed.astype(jnp.bfloat16)
+                out_scr[n, 2 * width :, columns] = packed.astype(jnp.bfloat16)
                 return 0
 
             lax.fori_loop(0, chunk // BLOCK, one_query_block, 0)
 
-    if fill:
-
-        @pl.when(active == 0)
-        def _():
-            out_scr[...] = jnp.zeros_like(out_scr)
-
-    @pl.when((active > 0) | fill)
-    def _():
-        sent = pltpu.make_async_copy(out_scr, out_ref, q_sem)
-        sent.start()
-        sent.wait()
-
-
-def attend(plan, queries, sources, wide, diagonal, fill, size, width):
-    chunk = queries.shape[0]
+    if chunks > 1:
+        lax.fori_loop(0, chunks, one_chunk, 0)
+    else:
+        one_chunk(0, 0)
+    for n in range(chunks):
+
+        @pl.when((plans[n][0] > 0) | fill)
+        def _(n=n):
+            pltpu.make_async_copy(out_scr.at[n], out_refs[n], out_sems.at[n]).wait()
+
+
+def attend(table, rows, queries, sources, wide, diagonal, fill, size, width):
+    chunk = queries[0].shape[0]
     pieces = len(sources[0])
     flat = [array for group in sources for array in group]
     kv_rows = sum(array.shape[0] for array in sources[0])
+    chunks = len(rows)
     body = lambda *refs: attend_kernel(
         *refs,
+        rows=rows,
+        slots=len(sources),
         pieces=pieces,
         wide=wide,
         diagonal=diagonal,
@@ -264,30 +300,32 @@
         width=width,
         chunk=chunk,
     )
-    area = chunk * chunk * 2 * 2
+    area = chunk * chunk * 2 * 2 * chunks
+    out = jax.ShapeDtypeStruct((2 * width + STAT_ROWS, chunk), jnp.bfloat16)
     return pl.pallas_call(
         body,
-        out_shape=jax.ShapeDtypeStruct((2 * width + STAT_ROWS, chunk), jnp.bfloat16),
+        out_shape=[out] * chunks,
         in_specs=[pl.BlockSpec(memory_space=pltpu.SMEM)]
-        + [pl.BlockSpec(memory_space=pl.ANY)] * (1 + len(flat)),
-        out_specs=pl.BlockSpec(memory_space=pl.ANY),
+        + [pl.BlockSpec(memory_space=pl.ANY)] * (chunks + len(flat)),
+        out_specs=[pl.BlockSpec(memory_space=pl.ANY)] * chunks,
         scratch_shapes=[
-            pltpu.VMEM(queries.shape, jnp.bfloat16),
+            pltpu.VMEM((chunks,) + queries[0].shape, jnp.bfloat16),
             pltpu.VMEM((len(sources), kv_rows, BLOCK), jnp.bfloat16),
             pltpu.VMEM((2, width, chunk), jnp.float32),
-            pltpu.VMEM((2 * width + STAT_ROWS, chunk), jnp.bfloat16),
+            pltpu.VMEM((chunks,) + out.shape, jnp.bfloat16),
             pltpu.SemaphoreType.DMA((len(sources), pieces)),
-            pltpu.SemaphoreType.DMA,
+            pltpu.SemaphoreType.DMA((chunks,)),
+            pltpu.SemaphoreType.DMA((chunks,)),
         ],
         cost_estimate=pl.CostEstimate(
             flops=2 * area * (size + width),
             transcendentals=area,
             bytes_accessed=len(sources) * kv_rows * 512,
         ),
-    )(plan, queries, *flat)
-
-
-def merge_kernel(valid, lam, *refs, widths, counts):
+    )(table, *queries, *flat)
+
+
+def merge_kernel(table, lam, *refs, widths, counts):
     out_ref = refs[-1]
     guarded = (1, None)
     begin = 0
@@ -303,7 +341,7 @@
                 level = stats[8 * m : 8 * m + 1] + stats[8 * m + 1 : 8 * m + 2] + stats[
                     8 * m + 2 : 8 * m + 3
                 ]
-                levels.append(jnp.where(valid[group, k] > 0, level, NEG_FILL))
+                levels.append(jnp.where(table[VALID_ROW + group, k] > 0, level, NEG_FILL))
             top = levels[0]
             for level in levels[1:]:
                 top = jnp.maximum(top, level)
@@ -317,7 +355,7 @@
                 if read is None:
                     read = term
                 elif guarded[group] == k:
-                    read = read + jnp.where(valid[group, k] > 0, term, 0.0)
+                    read = read + jnp.where(table[VALID_ROW + group, k] > 0, term, 0.0)
                 else:
                     read = read + term
             reads.append(read)
@@ -327,7 +365,7 @@
         column += width
 
 
-def merge(valid, lam, groups, widths):
+def merge(table, lam, groups, widths):
     chunk = groups[0][0].shape[1]
     counts = [len(parts) for parts in groups]
     flat = [part for parts in groups for part in parts]
@@ -340,7 +378,7 @@
         + [pl.BlockSpec((part.shape[0], BLOCK), lambda i: (0, i)) for part in flat],
         out_specs=pl.BlockSpec((BLOCK, sum(widths)), lambda i: (i, 0)),
         name="merge_reads",
-    )(valid, lam, *flat)
+    )(table, lam, *flat)
 
 
 def around(array, axis, by):
@@ -355,6 +393,10 @@
 
 def after(array, *others):
     return lax.optimization_barrier((array,) + others)[0]
+
+
+WIDE_ORDER = (2, 1, 3)
+NARROW_ORDER = (3, 1, 2)
 
 
 def attention(
@@ -367,7 +409,8 @@
     width_wide, width_narrow = value_wide.shape[1], value_narrow.shape[1]
 
     xk_near = around(key_wide, "x", 1)
-    q_later = {d: onward(query_wide, "z", -d) for d in (1, 2, 3)}
+    q_side = {3: around(query_narrow, "x", 3)}
+    q_later = {d: onward(query_wide, "z", -d) for d in WIDE_ORDER}
     values, kv_narrow = pack(value_wide, key_narrow, value_narrow)
     xv_back = around(values, "x", -1)
     xv_near = around(values, "x", 1)
@@ -375,110 +418,110 @@
     kv_below = {d: onward(kv_narrow, "z", d) for d in (1, 2, 3)}
     xk_far = around(xk_near, "x", 1)
     xv_far = around(xv_back, "x", -1)
-    q_side = {s: around(query_narrow, "x", s) for s in (1, 2, 3)}
+    for s in (1, 2):
+        q_side[s] = around(query_narrow, "x", s)
 
     wide_sources = [(key_wide, values), (xk_near, xv_near), (xk_far, xv_far), (xk_back, xv_back)]
     narrow_sources = [(kv_narrow,)] + [(kv_below[d],) for d in (1, 2, 3)]
 
-    def plan(*numbers):
-        return jnp.stack([jnp.asarray(n, jnp.int32) for n in numbers])
-
-    def wide(numbers, queries, sources, diagonal):
-        return attend(numbers, queries, sources, True, diagonal, False, size_wide, width_wide)
-
-    def narrow(numbers, queries, sources, diagonal, fill):
-        return attend(numbers, queries, sources, False, diagonal, fill, size_narrow, width_narrow)
-
-    one = jnp.int32(1)
-    diag_wide = wide(plan(1, 1, 0), query_wide, wide_sources[:1], True)
-    diag_narrow = narrow(
-        after(plan(1, 1, 0), diag_wide), query_narrow, narrow_sources[:1], True, False,
-    )
-    last = diag_narrow
-    made = {}
-    for d in (2, 1, 3):
-        numbers = plan((z + d < RING), RING, 0)
-        last = wide(after(numbers, last), q_later[d], wide_sources, False)
-        made[d] = last
-    relayed = lax.ppermute(made[2], "z", [(0, 3), (1, 2)])
-    sent = {d: onward(made[d], "z", d) for d in (1, 3)}
-    narrow_parts = []
-    for s in (2, 1, 3):
-        level = (lax.rem(x - s + RING, RING) > x).astype(jnp.int32)
-        numbers = plan((z > 0) | (level > 0), z + level, 1 - level)
-        last = narrow(after(numbers, last), q_side[s], narrow_sources, False, True)
-        narrow_parts.append(around(last, "x", -s))
-    sent[2] = lax.ppermute(after(relayed, last), "z", [(3, 2), (2, 3)])
-    rest_narrow = narrow(
-        after(plan((z > 0), z, 1), last), query_narrow, narrow_sources, False, True
-    )
-    rest_wide = wide(after(plan((x > 0), x, 1), rest_narrow), query_wide, wide_sources, False)
-    valid = jnp.stack(
+    one, zero = jnp.int32(1), jnp.int32(0)
+    level = {s: (lax.rem(x - s + RING, RING) > x).astype(jnp.int32) for s in NARROW_ORDER}
+    lines = [(one, one, zero)]
+    lines += [((z + d < RING), RING, 0) for d in WIDE_ORDER]
+    lines += [((z > 0) | (level[s] > 0), z + level[s], 1 - level[s]) for s in NARROW_ORDER]
+    lines += [((x > 0), x, 1)]
+    lines += [[one, x > 0] + [z >= d for d in WIDE_ORDER]]
+    lines += [[one, z > 0] + [(z > 0) | (lax.rem(x + s, RING) < x) for s in NARROW_ORDER]]
+    lines += [((z > 0), z, 1)]
+    table = jnp.stack(
         [
-            jnp.stack([one, x > 0] + [z >= d for d in (2, 1, 3)]).astype(jnp.int32),
-            jnp.stack(
-                [one, z > 0] + [(z > 0) | (lax.rem(x + s, RING) < x) for s in (2, 1, 3)]
-            ).astype(jnp.int32),
+            jnp.stack([jnp.asarray(n, jnp.int32) for n in (tuple(line) + (0, 0))[:5]])
+            for line in lines
         ]
     )
+
+    def wide(last, rows, queries, sources, diagonal):
+        given = after(table, last) if last is not None else table
+        return attend(given, rows, queries, sources, True, diagonal, False, size_wide, width_wide)
+
+    def narrow(last, rows, queries, sources, diagonal):
+        return attend(
+            after(table, last), rows, queries, sources, False, diagonal, not diagonal, size_narrow,
+            width_narrow,
+        )
+
+    diag_wide = wide(None, (0,), [query_wide], wide_sources[:1], True)[0]
+    diag_narrow = narrow(diag_wide, (0,), [query_narrow], narrow_sources[:1], True)[0]
+    side, sent = {}, {}
+    side[3] = narrow(diag_narrow, (4,), [q_side[3]], narrow_sources, False)[0]
+    sent[2] = wide(side[3], (1,), [q_later[2]], wide_sources, False)[0]
+    relayed = lax.ppermute(sent[2], "z", [(0, 3), (1, 2)])
+    sent[1], sent[3] = wide(sent[2], (2, 3), [q_later[1], q_later[3]], wide_sources, False)
+    side[1], side[2] = narrow(sent[1], (5, 6), [q_side[1], q_side[2]], narrow_sources, False)
+    for d in (1, 3):
+        sent[d] = onward(sent[d], "z", d)
+    sent[2] = lax.ppermute(after(relayed, side[1]), "z", [(3, 2), (2, 3)])
+    rest_narrow = narrow(side[1], (10,), [query_narrow], narrow_sources, False)[0]
+    rest_wide = wide(rest_narrow, (7,), [query_wide], wide_sources, False)[0]
+    side = {s: around(side[s], "x", -s) for s in NARROW_ORDER}
     return merge(
-        valid,
+        table,
         mix_lambda,
         (
-            [diag_wide, rest_wide] + [sent[d] for d in (2, 1, 3)],
-            [diag_narrow, rest_narrow] + narrow_parts,
+            [diag_wide, rest_wide] + [sent[d] for d in WIDE_ORDER],
+            [diag_narrow, rest_narrow] + [side[s] for s in NARROW_ORDER],
         ),
         (width_wide, width_narrow),
     )
 
 
 def project_kernel(
-    token_of, mine, weight_wide, weight_narrow, residual, gain, stream_out, rows_out, stream_scr, squares, flat_scr, rows
+    token_of, mine, weight_wide, weight_narrow, residual, gain, stream_out, rows_out,
+    weights, left, total, flat_scr, rows, sems,
 ):
-    step = pl.program_id(0)
     heads, tokens, _ = mine.shape
-    columns = weight_wide.shape[1]
-    wide = weight_wide.shape[0] // heads
-    model = stream_scr.shape[1]
+    depth, model = weight_wide.shape
+    wide = depth // heads
     tiles = model // LANES
-    made = residual[...].astype(jnp.float32)
-    for h in range(heads):
-        made = made + jnp.dot(
-            mine[h, :, :wide],
-            weight_wide[h * wide : (h + 1) * wide, :],
-            preferred_element_type=jnp.float32,
+    part = weights.shape[1]
+    parts = weights.shape[0]
+    for k in range(parts):
+        if k * part < depth:
+            source = weight_wide.at[pl.ds(k * part, part), :]
+        else:
+            source = weight_narrow.at[pl.ds(k * part - depth, part), :]
+        pltpu.make_async_copy(source, weights.at[k], sems.at[k]).start()
+    joined = jnp.concatenate(
+        [mine[h, :, :wide] for h in range(heads)] + [mine[h, :, wide:] for h in range(heads)], axis=1
+    )
+    for k in range(parts):
+        left[k] = joined[:, k * part : (k + 1) * part]
+    total[...] = residual[...].astype(jnp.float32)
+
+    def add_part(k, _):
+        pltpu.make_async_copy(
+            weight_wide.at[pl.ds(0, part), :], weights.at[k], sems.at[k]
+        ).wait()
+        total[...] = total[...] + jnp.dot(
+            left[k], weights[k], preferred_element_type=jnp.float32
         )
-    stacked = jnp.concatenate([mine[h, :, wide:] for h in range(heads)], axis=1)
-    made = made + jnp.dot(stacked, weight_narrow[...], preferred_element_type=jnp.float32)
-    rounded = made.astype(jnp.bfloat16)
+        return 0
+
+    lax.fori_loop(0, parts, add_part, 0)
+    rounded = total[...].astype(jnp.bfloat16)
     stream_out[...] = rounded
     stream = rounded.astype(jnp.float32)
-    stream_scr[:, pl.ds(pl.multiple_of(step * columns, columns), columns)] = stream
-    square = jnp.sum(stream * stream, axis=1, keepdims=True)
-
-    @pl.when(step == 0)
-    def _():
-        squares[...] = jnp.broadcast_to(square, squares.shape)
-
-    @pl.when(step > 0)
-    def _():
-        squares[...] = squares[...] + square
-
-    @pl.when(step == pl.num_programs(0) - 1)
-    def _():
-        inverse = lax.rsqrt(squares[...] / model + 1e-06)
-        for j in range(tiles):
-            lanes = slice(j * LANES, (j + 1) * LANES)
-            flat_scr[pl.ds(j, tokens, stride=tiles), :] = (
-                stream_scr[:, lanes] * inverse * gain[:, lanes]
-            )
-        rows[...] = flat_scr[...].reshape(tokens, tiles, LANES).astype(jnp.bfloat16)
-
-        def copy_row(slot, _):
-            rows_out[slot] = rows[token_of[slot]]
-            return 0
-
-        lax.fori_loop(0, rows_out.shape[0], copy_row, 0, unroll=16)
+    inverse = lax.rsqrt(jnp.mean(stream * stream, axis=1, keepdims=True) + 1e-06)
+    for j in range(tiles):
+        lanes = slice(j * LANES, (j + 1) * LANES)
+        flat_scr[pl.ds(j, tokens, stride=tiles), :] = stream[:, lanes] * inverse * gain[:, lanes]
+    rows[...] = flat_scr[...].reshape(tokens, tiles, LANES).astype(jnp.bfloat16)
+
+    def copy_row(slot, _):
+        rows_out[slot] = rows[token_of[slot]]
+        return 0
+
+    lax.fori_loop(0, rows_out.shape[0], copy_row, 0, unroll=16)
 
 
 def project(token_of, mine, weight_wide, weight_narrow, residual, gain):
@@ -486,60 +529,41 @@
     model = weight_wide.shape[1]
     slots = token_of.shape[0]
     tiles = model // LANES
-    columns = 2 * BLOCK
+    part = 2 * BLOCK
+    parts = heads * depth // part
     return pl.pallas_call(
         project_kernel,
-        grid=(model // columns,),
         out_shape=(
             jax.ShapeDtypeStruct((tokens, model), jnp.bfloat16),
             jax.ShapeDtypeStruct((slots, tiles, LANES), jnp.bfloat16),
         ),
         in_specs=[
             pl.BlockSpec(memory_space=pltpu.SMEM),
-            pl.BlockSpec((heads, tokens, depth), lambda i: (0, 0, 0)),
-            pl.BlockSpec((weight_wide.shape[0], columns), lambda i: (0, i)),
-            pl.BlockSpec((weight_narrow.shape[0], columns), lambda i: (0, i)),
-            pl.BlockSpec((tokens, columns), lambda i: (0, i)),
-            pl.BlockSpec((1, model), lambda i: (0, 0)),
+            pl.BlockSpec(memory_space=pltpu.VMEM),
+            pl.BlockSpec(memory_space=pltpu.HBM),
+            pl.BlockSpec(memory_space=pltpu.HBM),
+            pl.BlockSpec(memory_space=pltpu.VMEM),
+            pl.BlockSpec(memory_space=pltpu.VMEM),
         ],
-        out_specs=(
-            pl.BlockSpec((tokens, columns), lambda i: (0, i)),
-            pl.BlockSpec((slots, tiles, LANES), lambda i: (0, 0, 0)),
-        ),
+        out_specs=(pl.BlockSpec(memory_space=pltpu.VMEM),) * 2,
         scratch_shapes=[
+            pltpu.VMEM((parts, part, model), jnp.bfloat16),
+            pltpu.VMEM((parts, tokens, part), jnp.bfloat16),
             pltpu.VMEM((tokens, model), jnp.float32),
-            pltpu.VMEM((tokens, LANES), jnp.float32),
             pltpu.VMEM((tokens * tiles, LANES), jnp.float32),
             pltpu.VMEM((tokens, tiles, LANES), jnp.bfloat16),
+            pltpu.SemaphoreType.DMA((parts,)),
         ],
+        compiler_params=pltpu.CompilerParams(vmem_limit_bytes=49 * 1024 * 1024),
         name="project",
     )(token_of, mine, weight_wide, weight_narrow, residual, gain)
 
 
-def expert_kernel(
-    arrived, gate, up, down, out, gate_scr, up_scr, down_scr, flat, rows, hidden, sems
-):
+def expert_kernel(arrived, gate, up, down, out, flat, rows, hidden):
     count, tiles, _ = arrived.shape
     model, inner = gate.shape
     steps = inner // BLOCK
     columns = model // steps
-
-    def inner_part(k):
-        return pl.ds(pl.multiple_of(k * BLOCK, BLOCK), BLOCK)
-
-    def outer_part(k):
-        return pl.ds(pl.multiple_of(k * columns, columns), columns)
-
-    def in_copies(k):
-        part = inner_part(k)
-        return (
-            pltpu.make_async_copy(gate.at[:, part], gate_scr.at[:, part], sems.at[0, k]),
-            pltpu.make_async_copy(up.at[:, part], up_scr.at[:, part], sems.at[1, k]),
-        )
-
-    def out_copy(k):
-        part = outer_part(k)
-        return pltpu.make_async_copy(down.at[:, part], down_scr.at[:, part], sems.at[2, k])
 
     def spread(k, _):
         some = arrived[pl.ds(k * SOME, SOME)].astype(jnp.float32)
@@ -553,11 +577,6 @@
         out[pl.ds(k * SOME, SOME)] = some.reshape(SOME, tiles, LANES).astype(jnp.bfloat16)
         return 0
 
-    for k in range(steps):
-        for made in in_copies(k):
-            made.start()
-    for k in range(steps):
-        out_copy(k).start()
     lax.fori_loop(0, count // SOME, spread, 0)
     for j in range(tiles):
         rows[:, j * LANES : (j + 1) * LANES] = flat[pl.ds(j, count, stride=tiles), :].astype(
@@ -565,18 +584,17 @@
         )
 
     def widen(k, _):
-        for made in in_copies(k):
-            made.wait()
-        part = inner_part(k)
-        gate_part = jnp.dot(rows[...], gate_scr[:, part], preferred_element_type=jnp.float32)
-        up_part = jnp.dot(rows[...], up_scr[:, part], preferred_element_type=jnp.float32)
+        part = pl.ds(pl.multiple_of(k * BLOCK, BLOCK), BLOCK)
+        gate_part = jnp.dot(rows[...], gate[:, part], preferred_element_type=jnp.float32)
+        up_part = jnp.dot(rows[...], up[:, part], preferred_element_type=jnp.float32)
         hidden[:, part] = (gate_part * jax.nn.sigmoid(gate_part) * up_part).astype(jnp.bfloat16)
         return 0
 
     def narrow(k, _):
-        out_copy(k).wait()
         result = jnp.dot(
-            hidden[...], down_scr[:, outer_part(k)], preferred_element_type=jnp.float32
+            hidden[...],
+            down[:, pl.ds(pl.multiple_of(k * columns, columns), columns)],
+            preferred_element_type=jnp.float32,
         )
         for j in range(columns // LANES):
             flat[pl.ds(k * (columns // LANES) + j, count, stride=tiles), :] = result[
@@ -592,22 +610,17 @@
 def experts(arrived, gate, up, down):
     count, tiles, _ = arrived.shape
     model, inner = gate.shape
-    steps = inner // BLOCK
     return pl.pallas_call(
         expert_kernel,
         out_shape=jax.ShapeDtypeStruct(arrived.shape, jnp.bfloat16),
-        in_specs=[pl.BlockSpec(memory_space=pltpu.VMEM)]
-        + [pl.BlockSpec(memory_space=pl.ANY)] * 3,
+        in_specs=[pl.BlockSpec(memory_space=pltpu.VMEM)] * 4,
         out_specs=pl.BlockSpec(memory_space=pltpu.VMEM),
         scratch_shapes=[
-            pltpu.VMEM((model, inner), jnp.bfloat16),
-            pltpu.VMEM((model, inner), jnp.bfloat16),
-            pltpu.VMEM((inner, model), jnp.bfloat16),
             pltpu.VMEM((count * tiles, LANES), jnp.float32),
             pltpu.VMEM((count, model), jnp.bfloat16),
             pltpu.VMEM((count, inner), jnp.bfloat16),
-            pltpu.SemaphoreType.DMA((3, steps)),
         ],
+        compiler_params=pltpu.CompilerParams(vmem_limit_bytes=28*1024*1024),
         name="experts",
     )(arrived, gate, up, down)
 

time: 350 us -> 302 us (0.86)
  blocking collectives: 56.8 us -> 35.9 us
  starting transfers between devices: 63.4 us -> 44.3 us
  Pallas kernels: 149 us -> 141 us
  other arithmetic: 6.39 us -> 0.49 us
  waiting for transfers between devices: 49.3 us -> 53.7 us
    ppermute x12, starting transfers between devices: 35.4 us -> 11.7 us  [around(): lax.ppermute(array, axis, [(k, (k + by) % RING) for k in range(RING)])]
    all_to_all x1, blocking collectives: 56.8 us -> 35.9 us  [exchanged(): lax.all_to_all(rows.reshape(experts_all, -1, LANES), SP_TP, split_axis=0,...]
    ppermute x8, waiting for transfers between devices: 0.02 us -> 12.4 us  [onward(): lax.ppermute(array, axis, [(k, k + by) for k in range(RING) if 0 <= k + b...]
    ppermute x12, waiting for transfers between devices: 15.3 us -> 6.73 us  [around(): lax.ppermute(array, axis, [(k, (k + by) % RING) for k in range(RING)])]
    pallas_call x11 -> x9, Pallas kernels: 127 us -> 120 us  [the longest x8 113 us: attend(): pl.pallas_call(body, out_shape=[out] * chunks, in_specs=[pl.BlockSpec(mem...]
    another operation x9 -> x2, other arithmetic: 5.48 us -> 0.16 us  [attention(): jnp.stack([jnp.stack([jnp.asarray(n, jnp.int32) for n in (tuple(line) + (...]
    unnamed x53 -> x67, local copies, waits for them, and re-layouts: 8.65 us -> 8.47 us
  transfers between devices with their start and end apart: 26 -> 26, of which waited for: 5 -> 6; matrix products, arithmetic and copies ran while one was open for 2% -> 1% of each run, Pallas kernels for 36% -> 40%
where the time goes in v1:
time: 302 us; the launch traced here: 300 us
  Pallas kernels  141 us (47%)
  waiting for transfers between devices  53.7 us (18%)
  starting transfers between devices  44.3 us (15%)
  blocking collectives  35.9 us (12%)
  between operations  13.9 us (5%)
  local copies, waits for them, and re-layouts  11.4 us (4%)
    pallas_call x8, Pallas kernels, attend(): pl.pallas_call(body, out_shape=[out] * chunks, in_specs=[pl.BlockSpec(mem...  113 us
    all_to_all x1, blocking collectives, exchanged(): lax.all_to_all(rows.reshape(experts_all, -1, LANES), SP_TP, split_axis=0,...  35.9 us
    all_to_all x1, waiting for transfers between devices, exchanged(): lax.all_to_all(rows.reshape(experts_all, -1, LANES), SP_TP, split_axis=0,...  23.7 us
    ppermute x8, starting transfers between devices, onward(): lax.ppermute(array, axis, [(k, k + by) for k in range(RING) if 0 <= k + b...  16.9 us
    ppermute x8, waiting for transfers between devices, onward(): lax.ppermute(array, axis, [(k, k + by) for k in range(RING) if 0 <= k + b...  12.4 us
    ppermute x12, starting transfers between devices, around(): lax.ppermute(array, axis, [(k, (k + by) % RING) for k in range(RING)])  11.7 us
    pallas_call x1, Pallas kernels, experts(): pl.pallas_call(expert_kernel, out_shape=jax.ShapeDtypeStruct(arrived.shap...  9.91 us
    all_to_all x1, waiting for transfers between devices, shards(): lax.all_to_all(heads.reshape(tp_size, local_rows, -1), TP, split_axis=0,...  9.46 us
  transfers between devices with their start and end apart: 26, of which 6 were waited for; matrix products, arithmetic and copies ran while one was open for 1% of the time, Pallas kernels for 40%

profile of v1, /device:TPU:1, one launch (start us, length us, event | category | flops | bytes accessed | tf_op | source)
XLA Modules:
  0.0 300.4 jit_solution(11473725382629191611)
XLA Ops:
  8.0 3.4 %collective-permute-start = (bf16[768,128]{1,0:T(8,128)(2,1)}, bf16[768,128]{1,0:T(8,128)(2,1)S(1)}, u32[]{:S(2)}, u32[]{:S(2)}) collective-permute-start(bf16[768,128]{1,0:T(8,128)(2,1)} %bitcast.79), channel_id=1, source_target_pairs={{0,24},{8,0},{16,8},{24,16},{1,25},{9,1},{17,9},{25,17},{2,26},{10... | collective-permute-start | bytes 589832 | tf_op jit(solution)/shard_map/ppermute | solution.py:385
  11.4 2.2 pack.1
  13.6 3.6 %collective-permute-start.1 = (bf16[768,256]{1,0:T(8,128)(2,1)}, bf16[768,256]{1,0:T(8,128)(2,1)S(1)}, u32[]{:S(2)}, u32[]{:S(2)}) collective-permute-start(bf16[768,256]{1,0:T(8,128)(2,1)} %get-tuple-element.23.refs_2_.refs_3_), channel_id=1, source_target_pairs={{0,32},{32,64},{64,96},{1,33},{33,65},{65,97},{2,34},{34,66},{66,9... | collective-permute-start | bytes 1179656 | tf_op jit(solution)/shard_map/ppermute | solution.py:389
  17.1 5.2 %collective-permute-start.2 = (bf16[768,256]{1,0:T(8,128)(2,1)}, bf16[768,256]{1,0:T(8,128)(2,1)S(1)}, u32[]{:S(2)}, u32[]{:S(2)}) collective-permute-start(bf16[768,256]{1,0:T(8,128)(2,1)} %get-tuple-element.23.refs_2_.refs_3_), channel_id=1, source_target_pairs={{0,64},{32,96},{1,65},{33,97},{2,66},{34,98},{3,67},{35,99},{4,68}... | collective-permute-start | bytes 1179656 | tf_op jit(solution)/shard_map/ppermute | solution.py:389
  25.5 8.0 %collective-permute-done.2.refs_4_.refs_5_ = bf16[768,256]{1,0:T(8,128)(2,1)S(1)} collective-permute-done((bf16[768,256]{1,0:T(8,128)(2,1)}, bf16[768,256]{1,0:T(8,128)(2,1)S(1)}, u32[]{:S(2)}, u32[]{:S(2)}) %collective-permute-start.2) | collective-permute-done | bytes 393248 | tf_op jit(solution)/shard_map/ppermute | solution.py:389
  34.0 4.4 %collective-permute-done.3.refs_5_.refs_6_ = bf16[768,256]{1,0:T(8,128)(2,1)S(1)} collective-permute-done((bf16[768,256]{1,0:T(8,128)(2,1)}, bf16[768,256]{1,0:T(8,128)(2,1)S(1)}, u32[]{:S(2)}, u32[]{:S(2)}) %collective-permute-start.3) | collective-permute-done | bytes 393248 | tf_op jit(solution)/shard_map/ppermute | solution.py:389
  43.4 4.4 %shard_map.154.refs_2_ = bf16[528,768]{1,0:T(8,128)(2,1)} custom-call(s32[11,5]{1,0:T(8,128)} %stack.229.refs_0_, bf16[768,256]{1,0:T(8,128)(2,1)} %bitcast.69, bf16[768,256]{1,0:T(8,128)(2,1)} %bitcast.75, bf16[768,256]{1,0:T(8,128)(2,1)} %get-tuple-element.21.refs_3_.refs_4_), custom_call_target="tpu_custom_call" | custom-call | flops 1811939328 | bytes 786432 | tf_op jit(solution)/shard_map/pallas_call | solution.py:305
  47.8 4.0 %shard_map.155.refs_7_ = bf16[272,768]{1,0:T(8,128)(2,1)} custom-call(s32[11,5]{1,0:T(8,128)} %stack.229.refs_0_, bf16[768,128]{1,0:T(8,128)(2,1)} %bitcast.80, bf16[768,256]{1,0:T(8,128)(2,1)} %get-tuple-element.23.refs_2_.refs_3_), custom_call_target="tpu_custom_call" | custom-call | flops 905969664 | bytes 393216 | tf_op jit(solution)/shard_map/pallas_call | solution.py:305
  51.8 4.0 %shard_map.156 = bf16[272,768]{1,0:T(8,128)(2,1)} custom-call(s32[11,5]{1,0:T(8,128)} %stack.229.refs_0_, bf16[768,128]{1,0:T(8,128)(2,1)} %copy-done.28, bf16[768,256]{1,0:T(8,128)(2,1)} %get-tuple-element.23.refs_2_.refs_3_, bf16[768,256]{1,0:T(8,128)(2,1)} %copy-done.18, bf16[768,256]{1,0:T(8,128)(2,1)} %copy-done.19, bf16[768,256]{1,0:T(8,128)(2,1)} %copy-done.20), custom_call_target="tpu_custom_call" | custom-call | flops 905969664 | bytes 1572864 | tf_op jit(solution)/shard_map/pallas_call | solution.py:305
  58.7 43.6 %shard_map.157 = bf16[528,768]{1,0:T(8,128)(2,1)} custom-call(s32[11,5]{1,0:T(8,128)} %stack.229.refs_0_, bf16[768,256]{1,0:T(8,128)(2,1)} %collective-permute-done.4.refs_1_, bf16[768,256]{1,0:T(8,128)(2,1)} %bitcast.76, bf16[768,256]{1,0:T(8,128)(2,1)} %get-tuple-element.21.refs_3_.refs_4_, bf16[768,256]{1,0:T(8,128)(2,1)} %copy-done.22, ...), custom_call_target="tpu_custom_call" | custom-call | flops 1811939328 | bytes 3145728 | tf_op jit(solution)/shard_map/pallas_call | solution.py:305
  102.3 2.2 collective-permute-start.15
  105.6 2.1 collective-permute-start.19
  108.5 49.5 %shard_map.158 = (bf16[528,768]{1,0:T(8,128)(2,1)}, bf16[528,768]{1,0:T(8,128)(2,1)}) custom-call(s32[11,5]{1,0:T(8,128)} %stack.229.refs_0_, bf16[768,256]{1,0:T(8,128)(2,1)} %copy-done.25, bf16[768,256]{1,0:T(8,128)(2,1)} %copy-done.26, bf16[768,256]{1,0:T(8,128)(2,1)} %bitcast.77, bf16[768,256]{1,0:T(8,128)(2,1)} %get-tuple-element.21.refs_3_.refs_4_, ...), custom_call_target="tpu_custom_call" | custom-call | flops 3623878656 | bytes 3145728 | tf_op jit(solution)/shard_map/pallas_call | solution.py:305
  161.6 5.4 %shard_map.159 = (bf16[272,768]{1,0:T(8,128)(2,1)}, bf16[272,768]{1,0:T(8,128)(2,1)}) custom-call(s32[11,5]{1,0:T(8,128)} %stack.229.refs_0_, bf16[768,128]{1,0:T(8,128)(2,1)} %copy-done.29, bf16[768,128]{1,0:T(8,128)(2,1)} %copy-done.30, bf16[768,256]{1,0:T(8,128)(2,1)} %get-tuple-element.23.refs_2_.refs_3_, bf16[768,256]{1,0:T(8,128)(2,1)} %copy-done.18, ...), custom_call_target="tpu_custom_call" | custom-call | flops 1811939328 | bytes 1572864 | tf_op jit(solution)/shard_map/pallas_call | solution.py:305
  172.3 5.1 %collective-permute-done.20.refs_10_ = bf16[272,768]{1,0:T(8,128)(2,1)S(1)} collective-permute-done((bf16[272,768]{1,0:T(8,128)(2,1)}, bf16[272,768]{1,0:T(8,128)(2,1)S(1)}, u32[]{:S(2)}, u32[]{:S(2)}) %collective-permute-start.20) | collective-permute-done | bytes 417824 | tf_op jit(solution)/shard_map/ppermute | solution.py:385
  181.1 5.4 %merge_reads.1 = bf16[768,384]{1,0:T(8,128)(2,1)} custom-call(s32[11,5]{1,0:T(8,128)} %stack.229.refs_0_, f32[2,1]{1,0:T(2,128)} %copy.23.refs_1_, bf16[528,768]{1,0:T(8,128)(2,1)} %shard_map.154.refs_2_, bf16[528,768]{1,0:T(8,128)(2,1)} %shard_map.161.refs_3_, bf16[528,768]{1,0:T(8,128)(2,1)} %copy-done.11, bf16[528,768]{1,0:T(8,128)(2,1)} %copy-done.9, ...), custom_call_target="tpu_custom_call" | custom-call | tf_op jit(solution)/shard_map/merge_reads/pallas_call | solution.py:373
  186.6 8.0 %all-to-all-start = ((bf16[8,96,384]{2,1,0:T(8,128)(2,1)}), bf16[8,96,384]{2,1,0:T(8,128)(2,1)S(1)}, u32[]{:S(2)}, u32[]{:S(2)}) async-start(bf16[8,96,384]{2,1,0:T(8,128)(2,1)} %bitcast.62), calls=%async_computation | async-start | bytes 1179648 | tf_op jit(solution)/shard_map/all_to_all | solution.py:706
  195.1 9.5 %all-to-all-done.mine = bf16[8,96,384]{2,1,0:T(8,128)(2,1)S(1)} async-done(((bf16[8,96,384]{2,1,0:T(8,128)(2,1)}), bf16[8,96,384]{2,1,0:T(8,128)(2,1)S(1)}, u32[]{:S(2)}, u32[]{:S(2)}) %all-to-all-start) | async-done | bytes 589856 | tf_op jit(solution)/shard_map/all_to_all | solution.py:706
  207.5 6.9 %project.1 = (bf16[96,2048]{1,0:T(8,128)(2,1)S(1)}, bf16[384,16,128]{2,1,0:T(8,128)(2,1)S(1)}) custom-call(s32[384]{0:T(512)S(1)} %select_reduce_fusion.token_of, bf16[8,96,384]{2,1,0:T(8,128)(2,1)S(1)} %copy-done.4, bf16[2048,2048]{1,0:T(8,128)(2,1)} %all-gather.3.cloned.1.call-done.weight_wide, ...), custom_call_target="tpu_custom_call" | custom-call | tf_op jit(solution)/shard_map/project/pallas_call | solution.py:534
  214.4 35.9 %all_to_all.15 = bf16[128,48,128]{2,1,0:T(8,128)(2,1)S(1)} all-to-all(bf16[128,48,128]{2,1,0:T(8,128)(2,1)S(1)} %bitcast.59), channel_id=1, replica_groups=mesh['z'=4,'x'=4,'y'=4,'c'=2] {'z','x','y','c'}, dimensions={0} | all-to-all | bytes 3145728 | tf_op jit(solution)/shard_map/all_to_all | solution.py:715
  250.3 9.9 %experts.1 = bf16[384,16,128]{2,1,0:T(8,128)(2,1)} custom-call(bf16[384,16,128]{2,1,0:T(8,128)(2,1)S(1)} %bitcast.55, bf16[2048,1024]{1,0:T(8,128)(2,1)S(1)} %bitcast.56, bf16[2048,1024]{1,0:T(8,128)(2,1)S(1)} %bitcast.57, bf16[1024,2048]{1,0:T(8,128)(2,1)S(1)} %bitcast.58), custom_call_target="tpu_custom_call" | custom-call | tf_op jit(solution)/shard_map/experts/pallas_call | solution.py:613
  260.2 4.8 %all-to-all-start.2 = ((bf16[128,48,128]{2,1,0:T(8,128)(2,1)}), bf16[128,48,128]{2,1,0:T(8,128)(2,1)S(1)}, u32[]{:S(2)}, u32[]{:S(2)}) async-start(bf16[128,48,128]{2,1,0:T(8,128)(2,1)} %bitcast.45), calls=%async_computation.2 | async-start | bytes 3145728 | tf_op jit(solution)/shard_map/all_to_all | solution.py:715
  265.9 23.7 %all-to-all-done.2 = bf16[128,48,128]{2,1,0:T(8,128)(2,1)S(1)} async-done(((bf16[128,48,128]{2,1,0:T(8,128)(2,1)}), bf16[128,48,128]{2,1,0:T(8,128)(2,1)S(1)}, u32[]{:S(2)}, u32[]{:S(2)}) %all-to-all-start.2) | async-done | bytes 1572896 | tf_op jit(solution)/shard_map/all_to_all | solution.py:715
  290.7 2.9 combine.1
  (123 shorter events, 32.5 us)
Async XLA Ops:
  6.5 198.9 %all-gather.5.cloned.1.call-start = ((), (), s32[]{:S(2)}) async-start(), calls=%async_computation.4 | async-start | bytes 4718592 | tf_op jit(solution)/shard_map/all_gather | solution.py:705
  7.3 198.1 %all-gather.3.cloned.1.call-start = ((), (), s32[]{:S(2)}) async-start(), calls=%async_computation.3 | async-start | bytes 9437184 | tf_op jit(solution)/shard_map/all_gather | solution.py:704
  8.0 16.3 %collective-permute-start = (bf16[768,128]{1,0:T(8,128)(2,1)}, bf16[768,128]{1,0:T(8,128)(2,1)S(1)}, u32[]{:S(2)}, u32[]{:S(2)}) collective-permute-start(bf16[768,128]{1,0:T(8,128)(2,1)} %bitcast.79), channel_id=1, source_target_pairs={{0,24},{8,0},{16,8},{24,16},{1,25},{9,1},{17,9},{25,17},{2,26},{10... | collective-permute-start | bytes 589832 | tf_op jit(solution)/shard_map/ppermute | solution.py:385
  13.6 11.7 %collective-permute-start.1 = (bf16[768,256]{1,0:T(8,128)(2,1)}, bf16[768,256]{1,0:T(8,128)(2,1)S(1)}, u32[]{:S(2)}, u32[]{:S(2)}) collective-permute-start(bf16[768,256]{1,0:T(8,128)(2,1)} %get-tuple-element.23.refs_2_.refs_3_), channel_id=1, source_target_pairs={{0,32},{32,64},{64,96},{1,33},{33,65},{65,97},{2,34},{34,66},{66,9... | collective-permute-start | bytes 1179656 | tf_op jit(solution)/shard_map/ppermute | solution.py:389
  17.1 16.3 %collective-permute-start.2 = (bf16[768,256]{1,0:T(8,128)(2,1)}, bf16[768,256]{1,0:T(8,128)(2,1)S(1)}, u32[]{:S(2)}, u32[]{:S(2)}) collective-permute-start(bf16[768,256]{1,0:T(8,128)(2,1)} %get-tuple-element.23.refs_2_.refs_3_), channel_id=1, source_target_pairs={{0,64},{32,96},{1,65},{33,97},{2,66},{34,98},{3,67},{35,99},{4,68}... | collective-permute-start | bytes 1179656 | tf_op jit(solution)/shard_map/ppermute | solution.py:389
  22.4 16.0 %collective-permute-start.3 = (bf16[768,256]{1,0:T(8,128)(2,1)}, bf16[768,256]{1,0:T(8,128)(2,1)S(1)}, u32[]{:S(2)}, u32[]{:S(2)}) collective-permute-start(bf16[768,256]{1,0:T(8,128)(2,1)} %get-tuple-element.23.refs_2_.refs_3_), channel_id=1, source_target_pairs={{0,96},{1,97},{2,98},{3,99},{4,100},{5,101},{6,102},{7,103},{8,104... | collective-permute-start | bytes 1179656 | tf_op jit(solution)/shard_map/ppermute | solution.py:389
  23.7 16.0 %collective-permute-start.8 = (bf16[768,256]{1,0:T(8,128)(2,1)}, bf16[768,256]{1,0:T(8,128)(2,1)S(1)}, u32[]{:S(2)}, u32[]{:S(2)}) collective-permute-start(bf16[768,256]{1,0:T(8,128)(2,1)} %get-tuple-element.21.refs_3_.refs_4_), channel_id=1, source_target_pairs={{0,24},{8,0},{16,8},{24,16},{1,25},{9,1},{17,9},{25,17},{2,26},{10... | collective-permute-start | bytes 1179656 | tf_op jit(solution)/shard_map/ppermute | solution.py:385
  24.3 16.0 %collective-permute-start.5 = (bf16[768,256]{1,0:T(8,128)(2,1)}, bf16[768,256]{1,0:T(8,128)(2,1)S(1)}, u32[]{:S(2)}, u32[]{:S(2)}) collective-permute-start(bf16[768,256]{1,0:T(8,128)(2,1)} %bitcast.73), channel_id=1, source_target_pairs={{0,8},{8,16},{16,24},{24,0},{1,9},{9,17},{17,25},{25,1},{2,10},{10... | collective-permute-start | bytes 1179656 | tf_op jit(solution)/shard_map/ppermute | solution.py:385
  25.3 30.5 %collective-permute-start.6 = (bf16[768,256]{1,0:T(8,128)(2,1)}, bf16[768,256]{1,0:T(8,128)(2,1)S(1)}, u32[]{:S(2)}, u32[]{:S(2)}) collective-permute-start(bf16[768,256]{1,0:T(8,128)(2,1)} %get-tuple-element.21.refs_3_.refs_4_), channel_id=1, source_target_pairs={{0,8},{8,16},{16,24},{24,0},{1,9},{9,17},{17,25},{25,1},{2,10},{10... | collective-permute-start | bytes 1179656 | tf_op jit(solution)/shard_map/ppermute | solution.py:385
  33.4 23.9 %collective-permute-start.10 = (bf16[768,256]{1,0:T(8,128)(2,1)}, bf16[768,256]{1,0:T(8,128)(2,1)S(1)}, u32[]{:S(2)}, u32[]{:S(2)}) collective-permute-start(bf16[768,256]{1,0:T(8,128)(2,1)} %bitcast.74), channel_id=1, source_target_pairs={{0,24},{8,0},{16,8},{24,16},{1,25},{9,1},{17,9},{25,17},{2,26},{10... | collective-permute-start | bytes 1179656 | tf_op jit(solution)/shard_map/ppermute | solution.py:385
  38.4 20.2 %collective-permute-start.4 = (bf16[768,256]{1,0:T(8,128)(2,1)}, bf16[768,256]{1,0:T(8,128)(2,1)}, u32[]{:S(2)}, u32[]{:S(2)}) collective-permute-start(bf16[768,256]{1,0:T(8,128)(2,1)} %bitcast.68), channel_id=1, source_target_pairs={{64,0},{96,32},{65,1},{97,33},{66,2},{98,34},{67,3},{99,35},{68,4}... | collective-permute-start | bytes 1179656 | tf_op jit(solution)/shard_map/ppermute | solution.py:389
  39.7 18.9 %collective-permute-start.9 = (bf16[768,256]{1,0:T(8,128)(2,1)S(1)}, bf16[768,256]{1,0:T(8,128)(2,1)}, u32[]{:S(2)}, u32[]{:S(2)}) collective-permute-start(bf16[768,256]{1,0:T(8,128)(2,1)S(1)} %collective-permute-done.8.refs_9_.refs_10_), channel_id=1, source_target_pairs={{0,24},{8,0},{16,8},{24,16},{1,25},{9,1},{17,9},{25,17},{2,26},{10... | collective-permute-start | bytes 1179656 | tf_op jit(solution)/shard_map/ppermute | solution.py:385
  40.3 18.3 %collective-permute-start.7 = (bf16[768,256]{1,0:T(8,128)(2,1)S(1)}, bf16[768,256]{1,0:T(8,128)(2,1)}, u32[]{:S(2)}, u32[]{:S(2)}) collective-permute-start(bf16[768,256]{1,0:T(8,128)(2,1)S(1)} %collective-permute-done.5.refs_4_.refs_5_), channel_id=1, source_target_pairs={{0,8},{8,16},{16,24},{24,0},{1,9},{9,17},{17,25},{25,1},{2,10},{10... | collective-permute-start | bytes 1179656 | tf_op jit(solution)/shard_map/ppermute | solution.py:385
  55.9 49.7 %collective-permute-start.11 = (bf16[768,256]{1,0:T(8,128)(2,1)S(1)}, bf16[768,256]{1,0:T(8,128)(2,1)S(1)}, u32[]{:S(2)}, u32[]{:S(2)}) collective-permute-start(bf16[768,256]{1,0:T(8,128)(2,1)S(1)} %bitcast.71), channel_id=1, source_target_pairs={{32,0},{64,32},{96,64},{33,1},{65,33},{97,65},{34,2},{66,34},{98,6... | collective-permute-start | bytes 1179656 | tf_op jit(solution)/shard_map/ppermute | solution.py:389
  57.3 50.4 %collective-permute-start.12 = (bf16[768,256]{1,0:T(8,128)(2,1)S(1)}, bf16[768,256]{1,0:T(8,128)(2,1)S(1)}, u32[]{:S(2)}, u32[]{:S(2)}) collective-permute-start(bf16[768,256]{1,0:T(8,128)(2,1)S(1)} %bitcast.72), channel_id=1, source_target_pairs={{96,0},{97,1},{98,2},{99,3},{100,4},{101,5},{102,6},{103,7},{104,8... | collective-permute-start | bytes 1179656 | tf_op jit(solution)/shard_map/ppermute | solution.py:389
  102.3 64.7 %collective-permute-start.15 = (bf16[528,768]{1,0:T(8,128)(2,1)}, bf16[528,768]{1,0:T(8,128)(2,1)}, u32[]{:S(2)}, u32[]{:S(2)}) collective-permute-start(bf16[528,768]{1,0:T(8,128)(2,1)} %shard_map.157), channel_id=1, source_target_pairs={{0,96},{32,64},{1,97},{33,65},{2,98},{34,66},{3,99},{35,67},{4,100... | collective-permute-start | bytes 2433032 | tf_op jit(solution)/shard_map/ppermute | solution.py:458
  104.5 54.9 %collective-permute-start.13 = (bf16[768,128]{1,0:T(8,128)(2,1)S(1)}, bf16[768,128]{1,0:T(8,128)(2,1)S(1)}, u32[]{:S(2)}, u32[]{:S(2)}) collective-permute-start(bf16[768,128]{1,0:T(8,128)(2,1)S(1)} %bitcast.82), channel_id=1, source_target_pairs={{0,8},{8,16},{16,24},{24,0},{1,9},{9,17},{17,25},{25,1},{2,10},{10... | collective-permute-start | bytes 589832 | tf_op jit(solution)/shard_map/ppermute | solution.py:385
  104.5 56.4 %collective-permute-start.14 = (bf16[768,128]{1,0:T(8,128)(2,1)S(1)}, bf16[768,128]{1,0:T(8,128)(2,1)S(1)}, u32[]{:S(2)}, u32[]{:S(2)}) collective-permute-start(bf16[768,128]{1,0:T(8,128)(2,1)S(1)} %bitcast.83), channel_id=1, source_target_pairs={{0,16},{8,24},{16,0},{24,8},{1,17},{9,25},{17,1},{25,9},{2,18},{10... | collective-permute-start | bytes 589832 | tf_op jit(solution)/shard_map/ppermute | solution.py:385
  105.6 62.2 %collective-permute-start.19 = (bf16[272,768]{1,0:T(8,128)(2,1)}, bf16[272,768]{1,0:T(8,128)(2,1)S(1)}, u32[]{:S(2)}, u32[]{:S(2)}) collective-permute-start(bf16[272,768]{1,0:T(8,128)(2,1)} %shard_map.156), channel_id=1, source_target_pairs={{0,8},{8,16},{16,24},{24,0},{1,9},{9,17},{17,25},{25,1},{2,10},{10... | collective-permute-start | bytes 1253384 | tf_op jit(solution)/shard_map/ppermute | solution.py:385
  158.0 21.1 %collective-permute-start.17 = (bf16[528,768]{1,0:T(8,128)(2,1)}, bf16[528,768]{1,0:T(8,128)(2,1)S(1)}, u32[]{:S(2)}, u32[]{:S(2)}) collective-permute-start(bf16[528,768]{1,0:T(8,128)(2,1)} %get-tuple-element.27), channel_id=1, source_target_pairs={{0,32},{32,64},{64,96},{1,33},{33,65},{65,97},{2,34},{34,66},{66,9... | collective-permute-start | bytes 2433032 | tf_op jit(solution)/shard_map/ppermute | solution.py:389
  159.4 19.7 %collective-permute-start.18 = (bf16[528,768]{1,0:T(8,128)(2,1)}, bf16[528,768]{1,0:T(8,128)(2,1)S(1)}, u32[]{:S(2)}, u32[]{:S(2)}) collective-permute-start(bf16[528,768]{1,0:T(8,128)(2,1)} %get-tuple-element.33), channel_id=1, source_target_pairs={{0,96},{1,97},{2,98},{3,99},{4,100},{5,101},{6,102},{7,103},{8,104... | collective-permute-start | bytes 2433032 | tf_op jit(solution)/shard_map/ppermute | solution.py:389
  167.0 12.1 %collective-permute-start.16 = (bf16[528,768]{1,0:T(8,128)(2,1)}, bf16[528,768]{1,0:T(8,128)(2,1)S(1)}, u32[]{:S(2)}, u32[]{:S(2)}) collective-permute-start(bf16[528,768]{1,0:T(8,128)(2,1)} %collective-permute-done.15), channel_id=1, source_target_pairs={{96,64},{64,96},{97,65},{65,97},{98,66},{66,98},{99,67},{67,99},{1... | collective-permute-start | bytes 2433032 | tf_op jit(solution)/shard_map/ppermute | solution.py:463
  186.6 18.0 %all-to-all-start = ((bf16[8,96,384]{2,1,0:T(8,128)(2,1)}), bf16[8,96,384]{2,1,0:T(8,128)(2,1)S(1)}, u32[]{:S(2)}, u32[]{:S(2)}) async-start(bf16[8,96,384]{2,1,0:T(8,128)(2,1)} %bitcast.62), calls=%async_computation | async-start | bytes 1179648 | tf_op jit(solution)/shard_map/all_to_all | solution.py:706
  260.2 29.4 %all-to-all-start.2 = ((bf16[128,48,128]{2,1,0:T(8,128)(2,1)}), bf16[128,48,128]{2,1,0:T(8,128)(2,1)S(1)}, u32[]{:S(2)}, u32[]{:S(2)}) async-start(bf16[128,48,128]{2,1,0:T(8,128)(2,1)} %bitcast.45), calls=%async_computation.2 | async-start | bytes 3145728 | tf_op jit(solution)/shard_map/all_to_all | solution.py:715
  (34 other events, 482.7 us)
Sparse Core Ops, SparseCore 0:
  9.0 35.6 all-gather.4
  46.5 49.6 all-gather.2

commit v2 on v1

--- a/solution.py
+++ b/solution.py
@@ -15,15 +15,20 @@
 LANES = 128
 BLOCK = 256
 SOME = 48
-VALID_ROW = 8
+WIDE_ORDER = (2, 1, 3)
+NARROW_ORDER = (3, 1, 2)
 LEAST_TOTAL = 2.0**-60
 MOST_TOTAL = 2.0**100
 
 
-def pack_kernel(v_wide, k_narrow, v_narrow, v_out, kv_out):
+def pack_kernel(
+    place, q_wide, v_wide, q_narrow, k_narrow, v_narrow, v_out, kv_out, plus_out, minus_out, two_out
+):
+    z = place[0]
     chunk, width = v_wide.shape
     half = chunk // 2
     width_narrow = v_narrow.shape[1]
+    behind = chunk // BLOCK * width
     for j in range(chunk // BLOCK):
         rows = slice(j * BLOCK, (j + 1) * BLOCK)
         v_out[j * width : (j + 1) * width, :] = v_wide[rows, :].T
@@ -31,29 +36,51 @@
         kv_out[begin : begin + width_narrow, :] = v_narrow[rows, :].T
     for side in range(2):
         lanes = slice(side * LANES, (side + 1) * LANES)
-        kv_out[:half, lanes] = k_narrow[side * half : (side + 1) * half, :]
-
-
-def pack(v_wide, k_narrow, v_narrow):
+        rows = slice(side * half, (side + 1) * half)
+        kv_out[:half, lanes] = k_narrow[rows, :]
+        v_out[behind : behind + half, lanes] = q_narrow[rows, :]
+    for out, gives_queries in (
+        (plus_out, z == RING - 1),
+        (minus_out, z > 0),
+        (two_out, z >= RING // 2),
+    ):
+
+        @pl.when(gives_queries)
+        def _(out=out):
+            out[...] = q_wide[...]
+
+        @pl.when(jnp.logical_not(gives_queries))
+        def _(out=out):
+            out[...] = kv_out[...]
+
+
+def pack(place, q_wide, v_wide, q_narrow, k_narrow, v_narrow):
     chunk, width = v_wide.shape
-    rows = chunk // 2 + chunk // BLOCK * v_narrow.shape[1]
+    half = chunk // 2
+    both = jax.ShapeDtypeStruct(q_wide.shape, jnp.bfloat16)
+    assert half + chunk // BLOCK * v_narrow.shape[1] == chunk
     return pl.pallas_call(
         pack_kernel,
         out_shape=(
-            jax.ShapeDtypeStruct((chunk // BLOCK * width, BLOCK), jnp.bfloat16),
-            jax.ShapeDtypeStruct((rows, BLOCK), jnp.bfloat16),
+            jax.ShapeDtypeStruct((chunk // BLOCK * width + half, BLOCK), jnp.bfloat16),
+            both,
+            both,
+            both,
+            both,
         ),
+        in_specs=[pl.BlockSpec(memory_space=pltpu.SMEM)]
+        + [pl.BlockSpec(memory_space=pltpu.VMEM)] * 5,
         name="pack",
-    )(v_wide, k_narrow, v_narrow)
-
-
-def attend_kernel(table, *refs, rows, slots, pieces, wide, diagonal, fill, size, width, chunk):
-    chunks = len(rows)
+    )(place, q_wide, v_wide, q_narrow, k_narrow, v_narrow)
+
+
+def attend_kernel(place, *refs, plans, slots, pieces, wide, diagonal, fill, size, width, chunk):
+    chunks = len(plans)
     q_refs = refs[:chunks]
     src_refs = refs[chunks : chunks + slots * pieces]
     out_refs = refs[chunks + slots * pieces : 2 * chunks + slots * pieces]
     q_scr, kv_scr, acc, out_scr, sems, q_sems, out_sems = refs[2 * chunks + slots * pieces :]
-    plans = [(table[row, 0], table[row, 1], table[row, 2]) for row in rows]
+    plans = [plan(place[0], place[1]) for plan in plans]
     scale = size ** (-0.5) * LOG2E
     key_rows = chunk if wide else chunk // 2
     halves = key_rows // LANES
@@ -62,8 +89,8 @@
         made = []
         begin = 0
         for k in range(pieces):
-            source = src_refs[slot * pieces + k]
-            rows = source.shape[0]
+            rows = kv_scr.shape[1] // pieces
+            source = src_refs[slot * pieces + k].at[pl.ds(0, rows), :]
             made.append(
                 pltpu.make_async_copy(
                     source, kv_scr.at[slot, pl.ds(begin, rows), :], sems.at[slot, k]
@@ -75,8 +102,8 @@
     def wait_slot(slot):
         begin = 0
         for k in range(pieces):
-            source = src_refs[k]
-            rows = source.shape[0]
+            rows = kv_scr.shape[1] // pieces
+            source = src_refs[k].at[pl.ds(0, rows), :]
             pltpu.make_async_copy(
                 source, kv_scr.at[slot, pl.ds(begin, rows), :], sems.at[slot, k]
             ).wait()
@@ -104,6 +131,13 @@
             level = level - term
         return packed
 
+    def query_copy(source, n):
+        rows = q_scr.shape[1]
+        begin = 0 if wide else q_refs[source].shape[0] - rows
+        return pltpu.make_async_copy(
+            q_refs[source].at[pl.ds(begin, rows), :], q_scr.at[n], q_sems.at[n]
+        )
+
     def within(slot, plan):
         active, count, offset = plan
         return (active > 0) & (slot >= offset) & (slot < offset + count)
@@ -112,7 +146,7 @@
 
         @pl.when(plans[n][0] > 0)
         def _(n=n):
-            pltpu.make_async_copy(q_refs[n], q_scr.at[n], q_sems.at[n]).start()
+            query_copy(n, n).start()
 
     for slot in range(slots):
         used = within(slot, plans[0])
@@ -125,8 +159,11 @@
                 made.start()
 
     def one_chunk(n, _):
-        row = rows[0] + n
-        active, count, offset = table[row, 0], table[row, 1], table[row, 2]
+        active, count, offset = plans[0]
+        for k in range(1, chunks):
+            active, count, offset = (
+                jnp.where(n == k, new, old) for new, old in zip(plans[k], (active, count, offset))
+            )
         pl.when(active > 0)(lambda: attend_chunk(n, count, offset))
         if fill:
 
@@ -144,7 +181,7 @@
 
     def attend_chunk(n, count, offset):
         acc[...] = jnp.zeros_like(acc)
-        pltpu.make_async_copy(q_refs[0], q_scr.at[n], q_sems.at[n]).wait()
+        query_copy(0, n).wait()
 
         def add_slot(number, totals):
             slot = 0 if diagonal else number + offset
@@ -163,7 +200,9 @@
                     lanes = slice(m * size, (m + 1) * size)
                     scores = dot_nt(kv_scr[slot, :key_rows, lanes], q_scr[n, :, lanes])
                 else:
-                    queries = only_map(q_scr[n], m)
+                    queries = only_map(
+                        jnp.concatenate([q_scr[n, :, :LANES], q_scr[n, :, LANES:]], axis=0), m
+                    )
                     scores = jnp.concatenate(
                         [
                             dot_nt(kv_scr[slot, :key_rows, side * LANES : (side + 1) * LANES], queries)
@@ -213,6 +252,11 @@
                     lambda place: (kv_scr[slot, place, :LANES], kv_scr[slot, place, LANES:]), number
                 )
 
+            def queries_at(number):
+                return packed_rows(
+                    lambda place: (q_scr[n, place, :LANES], q_scr[n, place, LANES:]), number
+                )
+
             def one_query_block(number, _):
                 begin = pl.multiple_of(number * BLOCK, BLOCK)
                 columns = pl.ds(begin, BLOCK)
@@ -229,7 +273,7 @@
                             lanes = pl.ds(pl.multiple_of(m * size, size), size)
                             scores = dot_nt(kv_scr[slot, place, lanes], q_scr[n, columns, lanes])
                         else:
-                            scores = dot_nt(keys_at(slot, block), only_map(q_scr[n, columns, :], m))
+                            scores = dot_nt(keys_at(slot, block), only_map(queries_at(number), m))
                         scores = scores * scale
                         if diagonal:
                             key_pos = block * BLOCK + lax.broadcasted_iota(
@@ -282,15 +326,15 @@
             pltpu.make_async_copy(out_scr.at[n], out_refs[n], out_sems.at[n]).wait()
 
 
-def attend(table, rows, queries, sources, wide, diagonal, fill, size, width):
-    chunk = queries[0].shape[0]
+def attend(place, plans, queries, sources, wide, diagonal, fill, size, width, chunk):
     pieces = len(sources[0])
     flat = [array for group in sources for array in group]
-    kv_rows = sum(array.shape[0] for array in sources[0])
-    chunks = len(rows)
+    kv_rows = pieces * chunk
+    chunks = len(plans)
+    q_rows = chunk if wide else chunk // 2
     body = lambda *refs: attend_kernel(
         *refs,
-        rows=rows,
+        plans=plans,
         slots=len(sources),
         pieces=pieces,
         wide=wide,
@@ -309,7 +353,7 @@
         + [pl.BlockSpec(memory_space=pl.ANY)] * (chunks + len(flat)),
         out_specs=[pl.BlockSpec(memory_space=pl.ANY)] * chunks,
         scratch_shapes=[
-            pltpu.VMEM((chunks,) + queries[0].shape, jnp.bfloat16),
+            pltpu.VMEM((chunks, q_rows, BLOCK), jnp.bfloat16),
             pltpu.VMEM((len(sources), kv_rows, BLOCK), jnp.bfloat16),
             pltpu.VMEM((2, width, chunk), jnp.float32),
             pltpu.VMEM((chunks,) + out.shape, jnp.bfloat16),
@@ -322,10 +366,16 @@
             transcendentals=area,
             bytes_accessed=len(sources) * kv_rows * 512,
         ),
-    )(table, *queries, *flat)
-
-
-def merge_kernel(table, lam, *refs, widths, counts):
+    )(place, *queries, *flat)
+
+
+def merge_kernel(place, lam, *refs, widths, counts):
+    z, x = place[0], place[1]
+    wide_valid = [z >= 0, x > 0] + [z >= d for d in WIDE_ORDER]
+    narrow_valid = [z >= 0, z > 0] + [
+        (z > 0) | (lax.rem(x + s, RING) < x) for s in NARROW_ORDER
+    ]
+    valid = (wide_valid, narrow_valid)
     out_ref = refs[-1]
     guarded = (1, None)
     begin = 0
@@ -341,7 +391,7 @@
                 level = stats[8 * m : 8 * m + 1] + stats[8 * m + 1 : 8 * m + 2] + stats[
                     8 * m + 2 : 8 * m + 3
                 ]
-                levels.append(jnp.where(table[VALID_ROW + group, k] > 0, level, NEG_FILL))
+                levels.append(jnp.where(valid[group][k], level, NEG_FILL))
             top = levels[0]
             for level in levels[1:]:
                 top = jnp.maximum(top, level)
@@ -355,7 +405,7 @@
                 if read is None:
                     read = term
                 elif guarded[group] == k:
-                    read = read + jnp.where(table[VALID_ROW + group, k] > 0, term, 0.0)
+                    read = read + jnp.where(valid[group][k], term, 0.0)
                 else:
                     read = read + term
             reads.append(read)
@@ -365,7 +415,7 @@
         column += width
 
 
-def merge(table, lam, groups, widths):
+def merge(place, lam, groups, widths):
     chunk = groups[0][0].shape[1]
     counts = [len(parts) for parts in groups]
     flat = [part for parts in groups for part in parts]
@@ -378,7 +428,7 @@
         + [pl.BlockSpec((part.shape[0], BLOCK), lambda i: (0, i)) for part in flat],
         out_specs=pl.BlockSpec((BLOCK, sum(widths)), lambda i: (i, 0)),
         name="merge_reads",
-    )(table, lam, *flat)
+    )(place, lam, *flat)
 
 
 def around(array, axis, by):
@@ -393,10 +443,6 @@
 
 def after(array, *others):
     return lax.optimization_barrier((array,) + others)[0]
-
-
-WIDE_ORDER = (2, 1, 3)
-NARROW_ORDER = (3, 1, 2)
 
 
 def attention(
@@ -404,68 +450,82 @@
 ):
     z = lax.axis_index("z")
     x = lax.axis_index("x")
+    place = jnp.stack([z, x]).astype(jnp.int32)
+    chunk = query_wide.shape[0]
     size_wide = query_wide.shape[1] // 2
     size_narrow = query_narrow.shape[1] // 2
     width_wide, width_narrow = value_wide.shape[1], value_narrow.shape[1]
 
     xk_near = around(key_wide, "x", 1)
-    q_side = {3: around(query_narrow, "x", 3)}
-    q_later = {d: onward(query_wide, "z", -d) for d in WIDE_ORDER}
-    values, kv_narrow = pack(value_wide, key_narrow, value_narrow)
+    xk_back = around(key_wide, "x", -1)
+    values, kv_narrow, plus, minus, two = pack(
+        place, query_wide, value_wide, query_narrow, key_narrow, value_narrow
+    )
     xv_back = around(values, "x", -1)
     xv_near = around(values, "x", 1)
-    xk_back = around(key_wide, "x", -1)
-    kv_below = {d: onward(kv_narrow, "z", d) for d in (1, 2, 3)}
+    z_two = around(two, "z", 2)
+    z_plus = around(plus, "z", 1)
+    z_minus = around(minus, "z", -1)
+    xv_far = around(xv_back[:chunk], "x", -1)
     xk_far = around(xk_near, "x", 1)
-    xv_far = around(xv_back, "x", -1)
-    for s in (1, 2):
-        q_side[s] = around(query_narrow, "x", s)
+    xq_far = around(xv_near[chunk:], "x", 1)
 
     wide_sources = [(key_wide, values), (xk_near, xv_near), (xk_far, xv_far), (xk_back, xv_back)]
-    narrow_sources = [(kv_narrow,)] + [(kv_below[d],) for d in (1, 2, 3)]
-
-    one, zero = jnp.int32(1), jnp.int32(0)
-    level = {s: (lax.rem(x - s + RING, RING) > x).astype(jnp.int32) for s in NARROW_ORDER}
-    lines = [(one, one, zero)]
-    lines += [((z + d < RING), RING, 0) for d in WIDE_ORDER]
-    lines += [((z > 0) | (level[s] > 0), z + level[s], 1 - level[s]) for s in NARROW_ORDER]
-    lines += [((x > 0), x, 1)]
-    lines += [[one, x > 0] + [z >= d for d in WIDE_ORDER]]
-    lines += [[one, z > 0] + [(z > 0) | (lax.rem(x + s, RING) < x) for s in NARROW_ORDER]]
-    lines += [((z > 0), z, 1)]
-    table = jnp.stack(
-        [
-            jnp.stack([jnp.asarray(n, jnp.int32) for n in (tuple(line) + (0, 0))[:5]])
-            for line in lines
-        ]
-    )
-
-    def wide(last, rows, queries, sources, diagonal):
-        given = after(table, last) if last is not None else table
-        return attend(given, rows, queries, sources, True, diagonal, False, size_wide, width_wide)
-
-    def narrow(last, rows, queries, sources, diagonal):
+    narrow_sources = [(kv_narrow,), (z_plus,), (z_two,), (z_minus,)]
+    q_later = {1: z_minus, 2: z_two, 3: z_plus}
+    q_side = {1: xv_near, 2: xq_far, 3: xv_back}
+
+    def wide_plan(d):
+        return lambda z, x: ((z + d < RING).astype(jnp.int32), jnp.int32(RING), jnp.int32(0))
+
+    def narrow_plan(s):
+        def plan(z, x):
+            level = (lax.rem(x - s + RING, RING) > x).astype(jnp.int32)
+            return ((z > 0) | (level > 0)).astype(jnp.int32), z + level, 1 - level
+
+        return plan
+
+    def diag_plan(z, x):
+        return jnp.int32(1), jnp.int32(1), jnp.int32(0)
+
+    def wide_rest_plan(z, x):
+        return (x > 0).astype(jnp.int32), x, jnp.int32(1)
+
+    def narrow_rest_plan(z, x):
+        return (z > 0).astype(jnp.int32), z, jnp.int32(1)
+
+    def wide(last, plans, queries, sources, diagonal):
+        given = after(place, last) if last is not None else place
         return attend(
-            after(table, last), rows, queries, sources, False, diagonal, not diagonal, size_narrow,
-            width_narrow,
-        )
-
-    diag_wide = wide(None, (0,), [query_wide], wide_sources[:1], True)[0]
-    diag_narrow = narrow(diag_wide, (0,), [query_narrow], narrow_sources[:1], True)[0]
+            given, plans, queries, sources, True, diagonal, False, size_wide, width_wide, chunk
+        )
+
+    def narrow(last, plans, queries, sources, diagonal):
+        return attend(
+            after(place, last), plans, queries, sources, False, diagonal, not diagonal, size_narrow,
+            width_narrow, chunk,
+        )
+
+    diag_wide = wide(None, (diag_plan,), [query_wide], wide_sources[:1], True)[0]
+    diag_narrow = narrow(diag_wide, (diag_plan,), [values], narrow_sources[:1], True)[0]
     side, sent = {}, {}
-    side[3] = narrow(diag_narrow, (4,), [q_side[3]], narrow_sources, False)[0]
-    sent[2] = wide(side[3], (1,), [q_later[2]], wide_sources, False)[0]
+    side[3] = narrow(diag_narrow, (narrow_plan(3),), [q_side[3]], narrow_sources, False)[0]
+    sent[2] = wide(side[3], (wide_plan(2),), [q_later[2]], wide_sources, False)[0]
     relayed = lax.ppermute(sent[2], "z", [(0, 3), (1, 2)])
-    sent[1], sent[3] = wide(sent[2], (2, 3), [q_later[1], q_later[3]], wide_sources, False)
-    side[1], side[2] = narrow(sent[1], (5, 6), [q_side[1], q_side[2]], narrow_sources, False)
+    sent[1], sent[3] = wide(
+        sent[2], (wide_plan(1), wide_plan(3)), [q_later[1], q_later[3]], wide_sources, False,
+    )
+    side[1], side[2] = narrow(
+        sent[1], (narrow_plan(1), narrow_plan(2)), [q_side[1], q_side[2]], narrow_sources, False,
+    )
     for d in (1, 3):
         sent[d] = onward(sent[d], "z", d)
     sent[2] = lax.ppermute(after(relayed, side[1]), "z", [(3, 2), (2, 3)])
-    rest_narrow = narrow(side[1], (10,), [query_narrow], narrow_sources, False)[0]
-    rest_wide = wide(rest_narrow, (7,), [query_wide], wide_sources, False)[0]
+    rest_narrow = narrow(side[1], (narrow_rest_plan,), [values], narrow_sources, False)[0]
+    rest_wide = wide(rest_narrow, (wide_rest_plan,), [query_wide], wide_sources, False)[0]
     side = {s: around(side[s], "x", -s) for s in NARROW_ORDER}
     return merge(
-        table,
+        place,
         mix_lambda,
         (
             [diag_wide, rest_wide] + [sent[d] for d in WIDE_ORDER],
@@ -654,6 +714,7 @@
         + [pl.BlockSpec(memory_space=pltpu.VMEM)] * 2,
         out_specs=pl.BlockSpec(memory_space=pltpu.VMEM),
         scratch_shapes=[pltpu.VMEM((tokens * (model // LANES), LANES), jnp.float32)],
+        compiler_params=pltpu.CompilerParams(vmem_limit_bytes=16 * 1024 * 1024),
         name="combine",
     )(slot_of, share_of, returned, stream)
 

time: 302 us -> 290 us (0.960)
  waiting for transfers between devices: 53.7 us -> 48.6 us
  starting transfers between devices: 44.3 us -> 41.1 us
    ppermute x8 -> x2, starting transfers between devices: 16.9 us -> 2.68 us  [onward(): lax.ppermute(array, axis, [(k, k + by) for k in range(RING) if 0 <= k + b...]
    ppermute x8 -> x2, waiting for transfers between devices: 12.4 us -> 0.01 us  [onward(): lax.ppermute(array, axis, [(k, k + by) for k in range(RING) if 0 <= k + b...]
    ppermute x12 -> x13, starting transfers between devices: 11.7 us -> 20.5 us  [around(): lax.ppermute(array, axis, [(k, (k + by) % RING) for k in range(RING)])]
    ppermute x12 -> x13, waiting for transfers between devices: 6.73 us -> 13.5 us  [around(): lax.ppermute(array, axis, [(k, (k + by) % RING) for k in range(RING)])]
    unnamed x67 -> x51, local copies, waits for them, and re-layouts: 8.47 us -> 9.06 us
  transfers between devices with their start and end apart: 26 -> 21, of which waited for: 6 -> 6; matrix products, arithmetic and copies ran while one was open for 1% -> 1% of each run, Pallas kernels for 40% -> 42%
where the time goes in v2:
time: 290 us; the launch traced here: 289 us
  Pallas kernels  139 us (48%)
  waiting for transfers between devices  48.6 us (17%)
  starting transfers between devices  41.1 us (14%)
  blocking collectives  34.9 us (12%)
  between operations  13.8 us (5%)
  local copies, waits for them, and re-layouts  10.3 us (4%)
    pallas_call x8, Pallas kernels, attend(): pl.pallas_call(body, out_shape=[out] * chunks, in_specs=[pl.BlockSpec(mem...  112 us
    all_to_all x1, blocking collectives, exchanged(): lax.all_to_all(rows.reshape(experts_all, -1, LANES), SP_TP, split_axis=0,...  34.9 us
    all_to_all x1, waiting for transfers between devices, exchanged(): lax.all_to_all(rows.reshape(experts_all, -1, LANES), SP_TP, split_axis=0,...  24.3 us
    ppermute x13, starting transfers between devices, around(): lax.ppermute(array, axis, [(k, (k + by) % RING) for k in range(RING)])  20.5 us
    ppermute x13, waiting for transfers between devices, around(): lax.ppermute(array, axis, [(k, (k + by) % RING) for k in range(RING)])  13.5 us
    all_to_all x1, starting transfers between devices, shards(): lax.all_to_all(heads.reshape(tp_size, local_rows, -1), TP, split_axis=0,...  10.1 us
    pallas_call x1, Pallas kernels, experts(): pl.pallas_call(expert_kernel, out_shape=jax.ShapeDtypeStruct(arrived.shap...  9.96 us
    all_to_all x1, waiting for transfers between devices, shards(): lax.all_to_all(heads.reshape(tp_size, local_rows, -1), TP, split_axis=0,...  9.46 us
  transfers between devices with their start and end apart: 21, of which 6 were waited for; matrix products, arithmetic and copies ran while one was open for 1% of the time, Pallas kernels for 42%

profile of v2, /device:TPU:1, one launch (start us, length us, event | category | flops | bytes accessed | tf_op | source)
XLA Modules:
  0.0 289.1 jit_solution(4743682381513297566)
XLA Ops:
  8.7 3.0 %pack.1 = (bf16[1152,256]{1,0:T(8,128)(2,1)}, bf16[768,256]{1,0:T(8,128)(2,1)}, bf16[768,256]{1,0:T(8,128)(2,1)}, bf16[768,256]{1,0:T(8,128)(2,1)}, bf16[768,256]{1,0:T(8,128)(2,1)}) custom-call(s32[2]{0:T(128)} %pad_add_fusion.place.refs_0_, bf16[768,256]{1,0:T(8,128)(2,1)} %bitcast.26, bf16[768,256]{1,0:T(8,128)(2,1)} %bitcast.25, ...), custom_call_target="tpu_custom_call" | custom-call | tf_op jit(solution)/shard_map/pack/pallas_call | solution.py:62
  11.6 3.3 %collective-permute-start = (bf16[1152,256]{1,0:T(8,128)(2,1)}, bf16[1152,256]{1,0:T(8,128)(2,1)S(1)}, u32[]{:S(2)}, u32[]{:S(2)}) collective-permute-start(bf16[1152,256]{1,0:T(8,128)(2,1)} %get-tuple-element.24.refs_3_.refs_1_.refs_4_), channel_id=1, source_target_pairs={{0,24},{8,0},{16,8},{24,16},{1,25},{9,1},{17,9},{25,17},{2,26},{10... | collective-permute-start | bytes 1769480 | tf_op jit(solution)/shard_map/ppermute | solution.py:435
  16.6 3.3 %collective-permute-start.2 = (bf16[768,256]{1,0:T(8,128)(2,1)}, bf16[768,256]{1,0:T(8,128)(2,1)S(1)}, u32[]{:S(2)}, u32[]{:S(2)}) collective-permute-start(bf16[768,256]{1,0:T(8,128)(2,1)} %get-tuple-element.29), channel_id=1, source_target_pairs={{0,64},{32,96},{64,0},{96,32},{1,65},{33,97},{65,1},{97,33},{2,66}... | collective-permute-start | bytes 1179656 | tf_op jit(solution)/shard_map/ppermute | solution.py:435
  20.1 7.2 %collective-permute-done.refs_1_.refs_9_.refs_10_ = bf16[1152,256]{1,0:T(8,128)(2,1)S(1)} collective-permute-done((bf16[1152,256]{1,0:T(8,128)(2,1)}, bf16[1152,256]{1,0:T(8,128)(2,1)S(1)}, u32[]{:S(2)}, u32[]{:S(2)}) %collective-permute-start) | collective-permute-done | bytes 589856 | tf_op jit(solution)/shard_map/ppermute | solution.py:435
  27.3 3.8 %collective-permute-start.3 = (bf16[768,256]{1,0:T(8,128)(2,1)}, bf16[768,256]{1,0:T(8,128)(2,1)S(1)}, u32[]{:S(2)}, u32[]{:S(2)}) collective-permute-start(bf16[768,256]{1,0:T(8,128)(2,1)} %get-tuple-element.30), channel_id=1, source_target_pairs={{0,96},{32,0},{64,32},{96,64},{1,97},{33,1},{65,33},{97,65},{2,98}... | collective-permute-start | bytes 1179656 | tf_op jit(solution)/shard_map/ppermute | solution.py:435
  31.1 3.5 %collective-permute-start.8 = (bf16[768,256]{1,0:T(8,128)(2,1)}, bf16[768,256]{1,0:T(8,128)(2,1)}, u32[]{:S(2)}, u32[]{:S(2)}) collective-permute-start(bf16[768,256]{1,0:T(8,128)(2,1)} %bitcast.33), channel_id=1, source_target_pairs={{0,24},{8,0},{16,8},{24,16},{1,25},{9,1},{17,9},{25,17},{2,26},{10... | collective-permute-start | bytes 1179656 | tf_op jit(solution)/shard_map/ppermute | solution.py:435
  34.6 2.2 collective-permute-done.2.refs_4_.refs_1_.refs_5_
  37.3 4.2 %shard_map.154.refs_2_ = bf16[528,768]{1,0:T(8,128)(2,1)} custom-call(s32[2]{0:T(128)} %pad_add_fusion.place.refs_0_, bf16[768,256]{1,0:T(8,128)(2,1)} %bitcast.27, bf16[768,256]{1,0:T(8,128)(2,1)} %bitcast.34, bf16[1152,256]{1,0:T(8,128)(2,1)} %get-tuple-element.24.refs_3_.refs_1_.refs_4_), custom_call_target="tpu_custom_call" | custom-call | flops 1811939328 | bytes 786432 | tf_op jit(solution)/shard_map/pallas_call | solution.py:349
  41.5 3.7 %shard_map.155.refs_7_ = bf16[272,768]{1,0:T(8,128)(2,1)} custom-call(s32[2]{0:T(128)} %pad_add_fusion.place.refs_0_, bf16[1152,256]{1,0:T(8,128)(2,1)} %get-tuple-element.24.refs_3_.refs_1_.refs_4_, bf16[768,256]{1,0:T(8,128)(2,1)} %get-tuple-element.26.refs_2_.refs_3_), custom_call_target="tpu_custom_call" | custom-call | flops 905969664 | bytes 393216 | tf_op jit(solution)/shard_map/pallas_call | solution.py:349
  46.0 3.9 %shard_map.156 = bf16[272,768]{1,0:T(8,128)(2,1)} custom-call(s32[2]{0:T(128)} %pad_add_fusion.place.refs_0_, bf16[1152,256]{1,0:T(8,128)(2,1)} %copy-done.14, bf16[768,256]{1,0:T(8,128)(2,1)} %get-tuple-element.26.refs_2_.refs_3_, bf16[768,256]{1,0:T(8,128)(2,1)} %copy-done.19, bf16[768,256]{1,0:T(8,128)(2,1)} %copy-done.20, bf16[768,256]{1,0:T(8,128)(2,1)} %copy-done.21), custom_call_target="tpu_custom_call" | custom-call | flops 905969664 | bytes 1572864 | tf_op jit(solution)/shard_map/pallas_call | solution.py:349
  50.8 43.5 %shard_map.157 = bf16[528,768]{1,0:T(8,128)(2,1)} custom-call(s32[2]{0:T(128)} %pad_add_fusion.place.refs_0_, bf16[768,256]{1,0:T(8,128)(2,1)} %copy-done.20, bf16[768,256]{1,0:T(8,128)(2,1)} %bitcast.35, bf16[1152,256]{1,0:T(8,128)(2,1)} %get-tuple-element.24.refs_3_.refs_1_.refs_4_, bf16[768,256]{1,0:T(8,128)(2,1)} %copy-done.18, ...), custom_call_target="tpu_custom_call" | custom-call | flops 1811939328 | bytes 3145728 | tf_op jit(solution)/shard_map/pallas_call | solution.py:349
  94.3 2.2 collective-permute-start.10
  98.8 49.3 %shard_map.158 = (bf16[528,768]{1,0:T(8,128)(2,1)}, bf16[528,768]{1,0:T(8,128)(2,1)}) custom-call(s32[2]{0:T(128)} %pad_add_fusion.place.refs_0_, bf16[768,256]{1,0:T(8,128)(2,1)} %copy-done.21, bf16[768,256]{1,0:T(8,128)(2,1)} %copy-done.19, bf16[768,256]{1,0:T(8,128)(2,1)} %bitcast.36, bf16[1152,256]{1,0:T(8,128)(2,1)} %get-tuple-element.24.refs_3_.refs_1_.refs_4_, ...), custom_call_target="tpu_custom_call" | custom-call | flops 3623878656 | bytes 3145728 | tf_op jit(solution)/shard_map/pallas_call | solution.py:349
  151.5 5.4 %shard_map.159 = (bf16[272,768]{1,0:T(8,128)(2,1)}, bf16[272,768]{1,0:T(8,128)(2,1)}) custom-call(s32[2]{0:T(128)} %pad_add_fusion.place.refs_0_, bf16[1152,256]{1,0:T(8,128)(2,1)} %copy-done.15, bf16[384,256]{1,0:T(8,128)(2,1)} %copy-done.22, bf16[768,256]{1,0:T(8,128)(2,1)} %get-tuple-element.26.refs_2_.refs_3_, bf16[768,256]{1,0:T(8,128)(2,1)} %copy-done.19, ...), custom_call_target="tpu_custom_call" | custom-call | flops 1811939328 | bytes 1572864 | tf_op jit(solution)/shard_map/pallas_call | solution.py:349
  157.7 2.8 collective-permute-start.16
  163.6 2.8 collective-permute-done.15.refs_10_
  169.7 5.4 %merge_reads.1 = bf16[768,384]{1,0:T(8,128)(2,1)} custom-call(s32[2]{0:T(128)} %pad_add_fusion.place.refs_0_, f32[2,1]{1,0:T(2,128)} %copy.23.refs_1_, bf16[528,768]{1,0:T(8,128)(2,1)} %shard_map.154.refs_2_, bf16[528,768]{1,0:T(8,128)(2,1)} %shard_map.161.refs_3_, bf16[528,768]{1,0:T(8,128)(2,1)} %copy-done.11, bf16[528,768]{1,0:T(8,128)(2,1)} %copy-done.9, ...), custom_call_target="tpu_custom_call" | custom-call | tf_op jit(solution)/shard_map/merge_reads/pallas_call | solution.py:423
  175.2 10.1 %all-to-all-start = ((bf16[8,96,384]{2,1,0:T(8,128)(2,1)}), bf16[8,96,384]{2,1,0:T(8,128)(2,1)S(1)}, u32[]{:S(2)}, u32[]{:S(2)}) async-start(bf16[8,96,384]{2,1,0:T(8,128)(2,1)} %bitcast.24), calls=%async_computation | async-start | bytes 1179648 | tf_op jit(solution)/shard_map/all_to_all | solution.py:767
  185.8 9.5 %all-to-all-done.mine = bf16[8,96,384]{2,1,0:T(8,128)(2,1)S(1)} async-done(((bf16[8,96,384]{2,1,0:T(8,128)(2,1)}), bf16[8,96,384]{2,1,0:T(8,128)(2,1)S(1)}, u32[]{:S(2)}, u32[]{:S(2)}) %all-to-all-start) | async-done | bytes 589856 | tf_op jit(solution)/shard_map/all_to_all | solution.py:767
  198.2 6.9 %project.1 = (bf16[96,2048]{1,0:T(8,128)(2,1)S(1)}, bf16[384,16,128]{2,1,0:T(8,128)(2,1)S(1)}) custom-call(s32[384]{0:T(512)S(1)} %select_reduce_fusion.token_of, bf16[8,96,384]{2,1,0:T(8,128)(2,1)S(1)} %copy-done.4, bf16[2048,2048]{1,0:T(8,128)(2,1)} %all-gather.3.cloned.1.call-done.weight_wide, ...), custom_call_target="tpu_custom_call" | custom-call | tf_op jit(solution)/shard_map/project/pallas_call | solution.py:594
  205.1 34.9 %all_to_all.15 = bf16[128,48,128]{2,1,0:T(8,128)(2,1)S(1)} all-to-all(bf16[128,48,128]{2,1,0:T(8,128)(2,1)S(1)} %bitcast.22), channel_id=1, replica_groups=mesh['z'=4,'x'=4,'y'=4,'c'=2] {'z','x','y','c'}, dimensions={0} | all-to-all | bytes 3145728 | tf_op jit(solution)/shard_map/all_to_all | solution.py:776
  240.0 10.0 %experts.1 = bf16[384,16,128]{2,1,0:T(8,128)(2,1)} custom-call(bf16[384,16,128]{2,1,0:T(8,128)(2,1)S(1)} %bitcast.18, bf16[2048,1024]{1,0:T(8,128)(2,1)S(1)} %bitcast.19, bf16[2048,1024]{1,0:T(8,128)(2,1)S(1)} %bitcast.20, bf16[1024,2048]{1,0:T(8,128)(2,1)S(1)} %bitcast.21), custom_call_target="tpu_custom_call" | custom-call | tf_op jit(solution)/shard_map/experts/pallas_call | solution.py:673
  250.0 4.8 %all-to-all-start.2 = ((bf16[128,48,128]{2,1,0:T(8,128)(2,1)}), bf16[128,48,128]{2,1,0:T(8,128)(2,1)S(1)}, u32[]{:S(2)}, u32[]{:S(2)}) async-start(bf16[128,48,128]{2,1,0:T(8,128)(2,1)} %bitcast.15), calls=%async_computation.2 | async-start | bytes 3145728 | tf_op jit(solution)/shard_map/all_to_all | solution.py:776
  255.1 24.3 %all-to-all-done.2 = bf16[128,48,128]{2,1,0:T(8,128)(2,1)S(1)} async-done(((bf16[128,48,128]{2,1,0:T(8,128)(2,1)}), bf16[128,48,128]{2,1,0:T(8,128)(2,1)S(1)}, u32[]{:S(2)}, u32[]{:S(2)}) %all-to-all-start.2) | async-done | bytes 1572896 | tf_op jit(solution)/shard_map/all_to_all | solution.py:776
  (94 shorter events, 25.5 us)
Async XLA Ops:
  6.5 189.6 %all-gather.5.cloned.1.call-start = ((), (), s32[]{:S(2)}) async-start(), calls=%async_computation.4 | async-start | bytes 4718592 | tf_op jit(solution)/shard_map/all_gather | solution.py:766
  7.3 188.9 %all-gather.3.cloned.1.call-start = ((), (), s32[]{:S(2)}) async-start(), calls=%async_computation.3 | async-start | bytes 9437184 | tf_op jit(solution)/shard_map/all_gather | solution.py:765
  11.6 15.6 %collective-permute-start = (bf16[1152,256]{1,0:T(8,128)(2,1)}, bf16[1152,256]{1,0:T(8,128)(2,1)S(1)}, u32[]{:S(2)}, u32[]{:S(2)}) collective-permute-start(bf16[1152,256]{1,0:T(8,128)(2,1)} %get-tuple-element.24.refs_3_.refs_1_.refs_4_), channel_id=1, source_target_pairs={{0,24},{8,0},{16,8},{24,16},{1,25},{9,1},{17,9},{25,17},{2,26},{10... | collective-permute-start | bytes 1769480 | tf_op jit(solution)/shard_map/ppermute | solution.py:435
  14.9 16.1 %collective-permute-start.1 = (bf16[768,256]{1,0:T(8,128)(2,1)}, bf16[768,256]{1,0:T(8,128)(2,1)S(1)}, u32[]{:S(2)}, u32[]{:S(2)}) collective-permute-start(bf16[768,256]{1,0:T(8,128)(2,1)} %get-tuple-element.28), channel_id=1, source_target_pairs={{0,32},{32,64},{64,96},{96,0},{1,33},{33,65},{65,97},{97,1},{2,34}... | collective-permute-start | bytes 1179656 | tf_op jit(solution)/shard_map/ppermute | solution.py:435
  16.6 18.0 %collective-permute-start.4 = (bf16[768,256]{1,0:T(8,128)(2,1)}, bf16[768,256]{1,0:T(8,128)(2,1)S(1)}, u32[]{:S(2)}, u32[]{:S(2)}) collective-permute-start(bf16[768,256]{1,0:T(8,128)(2,1)} %bitcast.32), channel_id=1, source_target_pairs={{0,8},{8,16},{16,24},{24,0},{1,9},{9,17},{17,25},{25,1},{2,10},{10... | collective-permute-start | bytes 1179656 | tf_op jit(solution)/shard_map/ppermute | solution.py:435
  16.6 20.2 %collective-permute-start.2 = (bf16[768,256]{1,0:T(8,128)(2,1)}, bf16[768,256]{1,0:T(8,128)(2,1)S(1)}, u32[]{:S(2)}, u32[]{:S(2)}) collective-permute-start(bf16[768,256]{1,0:T(8,128)(2,1)} %get-tuple-element.29), channel_id=1, source_target_pairs={{0,64},{32,96},{64,0},{96,32},{1,65},{33,97},{65,1},{97,33},{2,66}... | collective-permute-start | bytes 1179656 | tf_op jit(solution)/shard_map/ppermute | solution.py:435
  19.9 30.1 %collective-permute-start.5 = (bf16[1152,256]{1,0:T(8,128)(2,1)}, bf16[1152,256]{1,0:T(8,128)(2,1)S(1)}, u32[]{:S(2)}, u32[]{:S(2)}) collective-permute-start(bf16[1152,256]{1,0:T(8,128)(2,1)} %get-tuple-element.24.refs_3_.refs_1_.refs_4_), channel_id=1, source_target_pairs={{0,8},{8,16},{16,24},{24,0},{1,9},{9,17},{17,25},{25,1},{2,10},{10... | collective-permute-start | bytes 1769480 | tf_op jit(solution)/shard_map/ppermute | solution.py:435
  27.3 18.0 %collective-permute-start.3 = (bf16[768,256]{1,0:T(8,128)(2,1)}, bf16[768,256]{1,0:T(8,128)(2,1)S(1)}, u32[]{:S(2)}, u32[]{:S(2)}) collective-permute-start(bf16[768,256]{1,0:T(8,128)(2,1)} %get-tuple-element.30), channel_id=1, source_target_pairs={{0,96},{32,0},{64,32},{96,64},{1,97},{33,1},{65,33},{97,65},{2,98}... | collective-permute-start | bytes 1179656 | tf_op jit(solution)/shard_map/ppermute | solution.py:435
  31.1 18.9 %collective-permute-start.8 = (bf16[768,256]{1,0:T(8,128)(2,1)}, bf16[768,256]{1,0:T(8,128)(2,1)}, u32[]{:S(2)}, u32[]{:S(2)}) collective-permute-start(bf16[768,256]{1,0:T(8,128)(2,1)} %bitcast.33), channel_id=1, source_target_pairs={{0,24},{8,0},{16,8},{24,16},{1,25},{9,1},{17,9},{25,17},{2,26},{10... | collective-permute-start | bytes 1179656 | tf_op jit(solution)/shard_map/ppermute | solution.py:435
  34.6 15.5 %collective-permute-start.6 = (bf16[768,256]{1,0:T(8,128)(2,1)S(1)}, bf16[768,256]{1,0:T(8,128)(2,1)}, u32[]{:S(2)}, u32[]{:S(2)}) collective-permute-start(bf16[768,256]{1,0:T(8,128)(2,1)S(1)} %collective-permute-done.4.refs_4_.refs_5_), channel_id=1, source_target_pairs={{0,8},{8,16},{16,24},{24,0},{1,9},{9,17},{17,25},{25,1},{2,10},{10... | collective-permute-start | bytes 1179656 | tf_op jit(solution)/shard_map/ppermute | solution.py:435
  36.8 13.3 %collective-permute-start.7 = (bf16[768,256]{1,0:T(8,128)(2,1)S(1)}, bf16[768,256]{1,0:T(8,128)(2,1)}, u32[]{:S(2)}, u32[]{:S(2)}) collective-permute-start(bf16[768,256]{1,0:T(8,128)(2,1)S(1)} %slice.8), channel_id=1, source_target_pairs={{0,24},{8,0},{16,8},{24,16},{1,25},{9,1},{17,9},{25,17},{2,26},{10... | collective-permute-start | bytes 1179656 | tf_op jit(solution)/shard_map/ppermute | solution.py:435
  94.3 62.6 %collective-permute-start.10 = (bf16[528,768]{1,0:T(8,128)(2,1)}, bf16[528,768]{1,0:T(8,128)(2,1)}, u32[]{:S(2)}, u32[]{:S(2)}) collective-permute-start(bf16[528,768]{1,0:T(8,128)(2,1)} %shard_map.157), channel_id=1, source_target_pairs={{0,96},{32,64},{1,97},{33,65},{2,98},{34,66},{3,99},{35,67},{4,100... | collective-permute-start | bytes 2433032 | tf_op jit(solution)/shard_map/ppermute | solution.py:514
  96.5 61.2 %collective-permute-start.14 = (bf16[272,768]{1,0:T(8,128)(2,1)}, bf16[272,768]{1,0:T(8,128)(2,1)S(1)}, u32[]{:S(2)}, u32[]{:S(2)}) collective-permute-start(bf16[272,768]{1,0:T(8,128)(2,1)} %shard_map.156), channel_id=1, source_target_pairs={{0,8},{8,16},{16,24},{24,0},{1,9},{9,17},{17,25},{25,1},{2,10},{10... | collective-permute-start | bytes 1253384 | tf_op jit(solution)/shard_map/ppermute | solution.py:435
  97.5 53.3 %collective-permute-start.9 = (bf16[384,256]{1,0:T(8,128)(2,1)S(1)}, bf16[384,256]{1,0:T(8,128)(2,1)S(1)}, u32[]{:S(2)}, u32[]{:S(2)}) collective-permute-start(bf16[384,256]{1,0:T(8,128)(2,1)S(1)} %slice.9), channel_id=1, source_target_pairs={{0,8},{8,16},{16,24},{24,0},{1,9},{9,17},{17,25},{25,1},{2,10},{10... | collective-permute-start | bytes 589832 | tf_op jit(solution)/shard_map/ppermute | solution.py:435
  148.1 19.6 %collective-permute-start.12 = (bf16[528,768]{1,0:T(8,128)(2,1)}, bf16[528,768]{1,0:T(8,128)(2,1)S(1)}, u32[]{:S(2)}, u32[]{:S(2)}) collective-permute-start(bf16[528,768]{1,0:T(8,128)(2,1)} %get-tuple-element.33), channel_id=1, source_target_pairs={{0,32},{32,64},{64,96},{1,33},{33,65},{65,97},{2,34},{34,66},{66,9... | collective-permute-start | bytes 2433032 | tf_op jit(solution)/shard_map/ppermute | solution.py:439
  149.5 18.2 %collective-permute-start.13 = (bf16[528,768]{1,0:T(8,128)(2,1)}, bf16[528,768]{1,0:T(8,128)(2,1)S(1)}, u32[]{:S(2)}, u32[]{:S(2)}) collective-permute-start(bf16[528,768]{1,0:T(8,128)(2,1)} %get-tuple-element.39), channel_id=1, source_target_pairs={{0,96},{1,97},{2,98},{3,99},{4,100},{5,101},{6,102},{7,103},{8,104... | collective-permute-start | bytes 2433032 | tf_op jit(solution)/shard_map/ppermute | solution.py:439
  156.9 10.8 %collective-permute-start.11 = (bf16[528,768]{1,0:T(8,128)(2,1)}, bf16[528,768]{1,0:T(8,128)(2,1)S(1)}, u32[]{:S(2)}, u32[]{:S(2)}) collective-permute-start(bf16[528,768]{1,0:T(8,128)(2,1)} %collective-permute-done.10), channel_id=1, source_target_pairs={{96,64},{64,96},{97,65},{65,97},{98,66},{66,98},{99,67},{67,99},{1... | collective-permute-start | bytes 2433032 | tf_op jit(solution)/shard_map/ppermute | solution.py:523
  157.6 8.7 %collective-permute-start.15 = (bf16[272,768]{1,0:T(8,128)(2,1)}, bf16[272,768]{1,0:T(8,128)(2,1)S(1)}, u32[]{:S(2)}, u32[]{:S(2)}) collective-permute-start(bf16[272,768]{1,0:T(8,128)(2,1)} %get-tuple-element.35), channel_id=1, source_target_pairs={{0,24},{8,0},{16,8},{24,16},{1,25},{9,1},{17,9},{25,17},{2,26},{10... | collective-permute-start | bytes 1253384 | tf_op jit(solution)/shard_map/ppermute | solution.py:435
  157.7 9.9 %collective-permute-start.16 = (bf16[272,768]{1,0:T(8,128)(2,1)}, bf16[272,768]{1,0:T(8,128)(2,1)}, u32[]{:S(2)}, u32[]{:S(2)}) collective-permute-start(bf16[272,768]{1,0:T(8,128)(2,1)} %get-tuple-element.40), channel_id=1, source_target_pairs={{0,16},{8,24},{16,0},{24,8},{1,17},{9,25},{17,1},{25,9},{2,18},{10... | collective-permute-start | bytes 1253384 | tf_op jit(solution)/shard_map/ppermute | solution.py:435
  175.2 20.1 %all-to-all-start = ((bf16[8,96,384]{2,1,0:T(8,128)(2,1)}), bf16[8,96,384]{2,1,0:T(8,128)(2,1)S(1)}, u32[]{:S(2)}, u32[]{:S(2)}) async-start(bf16[8,96,384]{2,1,0:T(8,128)(2,1)} %bitcast.24), calls=%async_computation | async-start | bytes 1179648 | tf_op jit(solution)/shard_map/all_to_all | solution.py:767
  198.2 41.8 %copy-start.1 = (bf16[1,2048,1024]{2,1,0:T(8,128)(2,1)S(1)}, bf16[1,2048,1024]{2,1,0:T(8,128)(2,1)}, u32[]{:S(2)}) copy-start(bf16[1,2048,1024]{2,1,0:T(8,128)(2,1)} %param.30) | copy-start | bytes 12582916
  198.2 41.8 %copy-start.2 = (bf16[1,1024,2048]{2,1,0:T(8,128)(2,1)S(1)}, bf16[1,1024,2048]{2,1,0:T(8,128)(2,1)}, u32[]{:S(2)}) copy-start(bf16[1,1024,2048]{2,1,0:T(8,128)(2,1)} %param.31) | copy-start | bytes 12582916
  205.1 44.9 %copy-start.6 = (bf16[96,2048]{1,0:T(8,128)(2,1)}, bf16[96,2048]{1,0:T(8,128)(2,1)S(1)}, u32[]{:S(2)}) copy-start(bf16[96,2048]{1,0:T(8,128)(2,1)S(1)} %get-tuple-element.42.stream) | copy-start | bytes 1179652
  250.0 29.4 %all-to-all-start.2 = ((bf16[128,48,128]{2,1,0:T(8,128)(2,1)}), bf16[128,48,128]{2,1,0:T(8,128)(2,1)S(1)}, u32[]{:S(2)}, u32[]{:S(2)}) async-start(bf16[128,48,128]{2,1,0:T(8,128)(2,1)} %bitcast.15), calls=%async_computation.2 | async-start | bytes 3145728 | tf_op jit(solution)/shard_map/all_to_all | solution.py:776
  (21 other events, 189.6 us)
Sparse Core Ops, SparseCore 0:
  9.0 35.6 all-gather.4
  46.5 49.6 all-gather.2

commit v3 on v2

--- a/solution.py
+++ b/solution.py
@@ -22,9 +22,9 @@
 
 
 def pack_kernel(
-    place, q_wide, v_wide, q_narrow, k_narrow, v_narrow, v_out, kv_out, plus_out, minus_out, two_out
+    q_wide, v_wide, q_narrow, k_narrow, v_narrow, v_out, kv_out, plus_out, minus_out, two_out
 ):
-    z = place[0]
+    z = lax.axis_index("z")
     chunk, width = v_wide.shape
     half = chunk // 2
     width_narrow = v_narrow.shape[1]
@@ -54,7 +54,7 @@
             out[...] = kv_out[...]
 
 
-def pack(place, q_wide, v_wide, q_narrow, k_narrow, v_narrow):
+def pack(q_wide, v_wide, q_narrow, k_narrow, v_narrow):
     chunk, width = v_wide.shape
     half = chunk // 2
     both = jax.ShapeDtypeStruct(q_wide.shape, jnp.bfloat16)
@@ -68,10 +68,8 @@
             both,
             both,
         ),
-        in_specs=[pl.BlockSpec(memory_space=pltpu.SMEM)]
-        + [pl.BlockSpec(memory_space=pltpu.VMEM)] * 5,
         name="pack",
-    )(place, q_wide, v_wide, q_narrow, k_narrow, v_narrow)
+    )(q_wide, v_wide, q_narrow, k_narrow, v_narrow)
 
 
 def attend_kernel(place, *refs, plans, slots, pieces, wide, diagonal, fill, size, width, chunk):
@@ -459,7 +457,7 @@
     xk_near = around(key_wide, "x", 1)
     xk_back = around(key_wide, "x", -1)
     values, kv_narrow, plus, minus, two = pack(
-        place, query_wide, value_wide, query_narrow, key_narrow, value_narrow
+        query_wide, value_wide, query_narrow, key_narrow, value_narrow
     )
     xv_back = around(values, "x", -1)
     xv_near = around(values, "x", 1)
@@ -520,11 +518,11 @@
     )
     for d in (1, 3):
         sent[d] = onward(sent[d], "z", d)
-    sent[2] = lax.ppermute(after(relayed, side[1]), "z", [(3, 2), (2, 3)])
     rest_narrow = narrow(side[1], (narrow_rest_plan,), [values], narrow_sources, False)[0]
+    sent[2] = lax.ppermute(after(relayed, rest_narrow), "z", [(3, 2), (2, 3)])
     rest_wide = wide(rest_narrow, (wide_rest_plan,), [query_wide], wide_sources, False)[0]
     side = {s: around(side[s], "x", -s) for s in NARROW_ORDER}
-    return merge(
+    made = merge(
         place,
         mix_lambda,
         (
@@ -533,6 +531,7 @@
         ),
         (width_wide, width_narrow),
     )
+    return made, values
 
 
 def project_kernel(
@@ -614,7 +613,7 @@
             pltpu.VMEM((tokens, tiles, LANES), jnp.bfloat16),
             pltpu.SemaphoreType.DMA((parts,)),
         ],
-        compiler_params=pltpu.CompilerParams(vmem_limit_bytes=49 * 1024 * 1024),
+        compiler_params=pltpu.CompilerParams(vmem_limit_bytes=48 * 1024 * 1024),
         name="project",
     )(token_of, mine, weight_wide, weight_narrow, residual, gain)
 
@@ -748,7 +747,7 @@
     up_weight,
     down_weight,
 ):
-    heads = attention(
+    heads, packed = attention(
         query_wide[:, 0],
         key_wide[:, 0],
         value_wide[:, 0],
@@ -762,6 +761,7 @@
     experts_all = lax.axis_size(SP_TP)
     capacity = max(2, 4 * local_rows // experts_all)
     slot_of, token_of = slot_tables(expert_ids, experts_all, capacity)
+    out_wide, out_narrow, _ = lax.optimization_barrier((out_wide, out_narrow, packed))
     whole_wide = lax.all_gather(out_wide, TP, axis=0, tiled=True)
     whole_narrow = lax.all_gather(out_narrow, TP, axis=0, tiled=True)
     mine = lax.all_to_all(

time: 290 us -> 292 us (level)
  blocking collectives: 34.9 us -> 39.2 us
  local copies, waits for them, and re-layouts: 10.3 us -> 6.54 us
  waiting for transfers between devices: 48.6 us -> 52.3 us
    all_to_all x1, blocking collectives: 34.9 us -> 39.2 us  [exchanged(): lax.all_to_all(rows.reshape(experts_all, -1, LANES), SP_TP, split_axis=0,...]
    unnamed x51 -> x45, local copies, waits for them, and re-layouts: 9.06 us -> 5.31 us
  transfers between devices with their start and end apart: 21 -> 21, of which waited for: 6 -> 7; matrix products, arithmetic and copies ran while one was open for 1% -> 1% of each run, Pallas kernels for 42% -> 40%
where the time goes in v3:
time: 292 us; the launch traced here: 291 us
  Pallas kernels  140 us (48%)
  waiting for transfers between devices  52.3 us (18%)
  blocking collectives  39.2 us (13%)
  starting transfers between devices  38.7 us (13%)
  between operations  13.8 us (5%)
  local copies, waits for them, and re-layouts  6.54 us (2%)
    pallas_call x8, Pallas kernels, attend(): pl.pallas_call(body, out_shape=[out] * chunks, in_specs=[pl.BlockSpec(mem...  112 us
    all_to_all x1, blocking collectives, exchanged(): lax.all_to_all(rows.reshape(experts_all, -1, LANES), SP_TP, split_axis=0,...  39.2 us
    all_to_all x1, waiting for transfers between devices, exchanged(): lax.all_to_all(rows.reshape(experts_all, -1, LANES), SP_TP, split_axis=0,...  24.3 us
    ppermute x13, starting transfers between devices, around(): lax.ppermute(array, axis, [(k, (k + by) % RING) for k in range(RING)])  20.5 us
    ppermute x13, waiting for transfers between devices, around(): lax.ppermute(array, axis, [(k, (k + by) % RING) for k in range(RING)])  15.3 us
    pallas_call x1, Pallas kernels, experts(): pl.pallas_call(expert_kernel, out_shape=jax.ShapeDtypeStruct(arrived.shap...  9.94 us
    all_to_all x1, waiting for transfers between devices, shards(): lax.all_to_all(heads.reshape(tp_size, local_rows, -1), TP, split_axis=0,...  9.46 us
    all_to_all x1, starting transfers between devices, shards(): lax.all_to_all(heads.reshape(tp_size, local_rows, -1), TP, split_axis=0,...  7.7 us
  transfers between devices with their start and end apart: 21, of which 7 were waited for; matrix products, arithmetic and copies ran while one was open for 1% of the time, Pallas kernels for 40%

profile of v3, /device:TPU:1, one launch (start us, length us, event | category | flops | bytes accessed | tf_op | source)
XLA Modules:
  0.0 291.0 jit_solution(13463134912409666380)
XLA Ops:
  6.5 3.0 %pack.1 = (bf16[1152,256]{1,0:T(8,128)(2,1)}, bf16[768,256]{1,0:T(8,128)(2,1)}, bf16[768,256]{1,0:T(8,128)(2,1)}, bf16[768,256]{1,0:T(8,128)(2,1)}, bf16[768,256]{1,0:T(8,128)(2,1)}) custom-call(bf16[768,256]{1,0:T(8,128)(2,1)} %bitcast.26, bf16[768,256]{1,0:T(8,128)(2,1)} %bitcast.25, bf16[768,128]{1,0:T(8,128)(2,1)} %bitcast.29, ...), custom_call_target="tpu_custom_call" | custom-call | tf_op jit(solution)/shard_map/pack/pallas_call | solution.py:62
  10.3 3.4 %collective-permute-start = (bf16[1152,256]{1,0:T(8,128)(2,1)}, bf16[1152,256]{1,0:T(8,128)(2,1)S(1)}, u32[]{:S(2)}, u32[]{:S(2)}) collective-permute-start(bf16[1152,256]{1,0:T(8,128)(2,1)} %get-tuple-element.26.refs_3_.refs_1_.refs_4_), channel_id=1, source_target_pairs={{0,24},{8,0},{16,8},{24,16},{1,25},{9,1},{17,9},{25,17},{2,26},{10... | collective-permute-start | bytes 1769480 | tf_op jit(solution)/shard_map/ppermute | solution.py:433
  15.4 3.3 %collective-permute-start.2 = (bf16[768,256]{1,0:T(8,128)(2,1)}, bf16[768,256]{1,0:T(8,128)(2,1)S(1)}, u32[]{:S(2)}, u32[]{:S(2)}) collective-permute-start(bf16[768,256]{1,0:T(8,128)(2,1)} %get-tuple-element.31), channel_id=1, source_target_pairs={{0,64},{32,96},{64,0},{96,32},{1,65},{33,97},{65,1},{97,33},{2,66}... | collective-permute-start | bytes 1179656 | tf_op jit(solution)/shard_map/ppermute | solution.py:433
  18.8 7.2 %collective-permute-done.refs_1_.refs_9_.refs_10_ = bf16[1152,256]{1,0:T(8,128)(2,1)S(1)} collective-permute-done((bf16[1152,256]{1,0:T(8,128)(2,1)}, bf16[1152,256]{1,0:T(8,128)(2,1)S(1)}, u32[]{:S(2)}, u32[]{:S(2)}) %collective-permute-start) | collective-permute-done | bytes 589856 | tf_op jit(solution)/shard_map/ppermute | solution.py:433
  26.0 3.7 %collective-permute-start.3 = (bf16[768,256]{1,0:T(8,128)(2,1)}, bf16[768,256]{1,0:T(8,128)(2,1)}, u32[]{:S(2)}, u32[]{:S(2)}) collective-permute-start(bf16[768,256]{1,0:T(8,128)(2,1)} %get-tuple-element.32), channel_id=1, source_target_pairs={{0,96},{32,0},{64,32},{96,64},{1,97},{33,1},{65,33},{97,65},{2,98}... | collective-permute-start | bytes 1179656 | tf_op jit(solution)/shard_map/ppermute | solution.py:433
  29.8 3.5 %collective-permute-start.8 = (bf16[768,256]{1,0:T(8,128)(2,1)}, bf16[768,256]{1,0:T(8,128)(2,1)S(1)}, u32[]{:S(2)}, u32[]{:S(2)}) collective-permute-start(bf16[768,256]{1,0:T(8,128)(2,1)} %bitcast.33), channel_id=1, source_target_pairs={{0,24},{8,0},{16,8},{24,16},{1,25},{9,1},{17,9},{25,17},{2,26},{10... | collective-permute-start | bytes 1179656 | tf_op jit(solution)/shard_map/ppermute | solution.py:433
  33.3 2.2 collective-permute-done.2.refs_4_.refs_1_.refs_5_
  36.7 4.2 %shard_map.154.refs_2_ = bf16[528,768]{1,0:T(8,128)(2,1)} custom-call(s32[2]{0:T(128)} %pad_add_fusion.refs_0_, bf16[768,256]{1,0:T(8,128)(2,1)} %bitcast.27, bf16[768,256]{1,0:T(8,128)(2,1)} %bitcast.34, bf16[1152,256]{1,0:T(8,128)(2,1)} %get-tuple-element.26.refs_3_.refs_1_.refs_4_), custom_call_target="tpu_custom_call" | custom-call | flops 1811939328 | bytes 786432 | tf_op jit(solution)/shard_map/pallas_call | solution.py:347
  40.9 3.7 %shard_map.155.refs_7_ = bf16[272,768]{1,0:T(8,128)(2,1)} custom-call(s32[2]{0:T(128)} %pad_add_fusion.refs_0_, bf16[1152,256]{1,0:T(8,128)(2,1)} %get-tuple-element.26.refs_3_.refs_1_.refs_4_, bf16[768,256]{1,0:T(8,128)(2,1)} %get-tuple-element.28.refs_2_.refs_3_), custom_call_target="tpu_custom_call" | custom-call | flops 905969664 | bytes 393216 | tf_op jit(solution)/shard_map/pallas_call | solution.py:347
  44.7 3.9 %shard_map.156 = bf16[272,768]{1,0:T(8,128)(2,1)} custom-call(s32[2]{0:T(128)} %pad_add_fusion.refs_0_, bf16[1152,256]{1,0:T(8,128)(2,1)} %copy-done.11, bf16[768,256]{1,0:T(8,128)(2,1)} %get-tuple-element.28.refs_2_.refs_3_, bf16[768,256]{1,0:T(8,128)(2,1)} %copy-done.16, bf16[768,256]{1,0:T(8,128)(2,1)} %copy-done.17, ...), custom_call_target="tpu_custom_call" | custom-call | flops 905969664 | bytes 1572864 | tf_op jit(solution)/shard_map/pallas_call | solution.py:347
  49.6 43.5 %shard_map.157 = bf16[528,768]{1,0:T(8,128)(2,1)} custom-call(s32[2]{0:T(128)} %pad_add_fusion.refs_0_, bf16[768,256]{1,0:T(8,128)(2,1)} %copy-done.17, bf16[768,256]{1,0:T(8,128)(2,1)} %bitcast.35, bf16[1152,256]{1,0:T(8,128)(2,1)} %get-tuple-element.26.refs_3_.refs_1_.refs_4_, bf16[768,256]{1,0:T(8,128)(2,1)} %copy-done.15, bf16[1152,256]{1,0:T(8,128)(2,1)} %copy-done.12, ...), custom_call_target="tpu_custom_call" | custom-call | flops 1811939328 | bytes 3145728 | tf_op jit(solution)/shard_map/pallas_call | solution.py:347
  97.6 49.3 %shard_map.158 = (bf16[528,768]{1,0:T(8,128)(2,1)}, bf16[528,768]{1,0:T(8,128)(2,1)}) custom-call(s32[2]{0:T(128)} %pad_add_fusion.refs_0_, bf16[768,256]{1,0:T(8,128)(2,1)} %collective-permute-done.3.refs_5_.refs_1_.refs_6_, bf16[768,256]{1,0:T(8,128)(2,1)} %copy-done.16, bf16[768,256]{1,0:T(8,128)(2,1)} %bitcast.36, ...), custom_call_target="tpu_custom_call" | custom-call | flops 3623878656 | bytes 3145728 | tf_op jit(solution)/shard_map/pallas_call | solution.py:347
  148.9 5.4 %shard_map.159 = (bf16[272,768]{1,0:T(8,128)(2,1)}, bf16[272,768]{1,0:T(8,128)(2,1)}) custom-call(s32[2]{0:T(128)} %pad_add_fusion.refs_0_, bf16[1152,256]{1,0:T(8,128)(2,1)} %copy-done.12, bf16[384,256]{1,0:T(8,128)(2,1)} %copy-done.19, bf16[768,256]{1,0:T(8,128)(2,1)} %get-tuple-element.28.refs_2_.refs_3_, bf16[768,256]{1,0:T(8,128)(2,1)} %copy-done.16, ...), custom_call_target="tpu_custom_call" | custom-call | flops 1811939328 | bytes 1572864 | tf_op jit(solution)/shard_map/pallas_call | solution.py:347
  158.0 2.8 collective-permute-start.16
  162.3 4.3 %collective-permute-done.15.refs_10_ = bf16[272,768]{1,0:T(8,128)(2,1)} collective-permute-done((bf16[272,768]{1,0:T(8,128)(2,1)}, bf16[272,768]{1,0:T(8,128)(2,1)}, u32[]{:S(2)}, u32[]{:S(2)}) %collective-permute-start.15) | collective-permute-done | bytes 417824 | tf_op jit(solution)/shard_map/ppermute | solution.py:433
  168.2 2.6 collective-permute-done.13.refs_6_
  172.6 5.4 %merge_reads.1 = bf16[768,384]{1,0:T(8,128)(2,1)} custom-call(s32[2]{0:T(128)} %pad_add_fusion.refs_0_, f32[2,1]{1,0:T(2,128)} %copy.23.refs_1_, bf16[528,768]{1,0:T(8,128)(2,1)} %shard_map.154.refs_2_, bf16[528,768]{1,0:T(8,128)(2,1)} %shard_map.161.refs_3_, bf16[528,768]{1,0:T(8,128)(2,1)} %copy-done.9, bf16[528,768]{1,0:T(8,128)(2,1)} %copy-done.7, ...), custom_call_target="tpu_custom_call" | custom-call | tf_op jit(solution)/shard_map/merge_reads/pallas_call | solution.py:421
  178.0 7.7 %all-to-all-start = ((bf16[8,96,384]{2,1,0:T(8,128)(2,1)}), bf16[8,96,384]{2,1,0:T(8,128)(2,1)S(1)}, u32[]{:S(2)}, u32[]{:S(2)}) async-start(bf16[8,96,384]{2,1,0:T(8,128)(2,1)} %bitcast.24), calls=%async_computation | async-start | bytes 1179648 | tf_op jit(solution)/shard_map/all_to_all | solution.py:767
  186.3 9.5 %all-to-all-done.mine = bf16[8,96,384]{2,1,0:T(8,128)(2,1)S(1)} async-done(((bf16[8,96,384]{2,1,0:T(8,128)(2,1)}), bf16[8,96,384]{2,1,0:T(8,128)(2,1)S(1)}, u32[]{:S(2)}, u32[]{:S(2)}) %all-to-all-start) | async-done | bytes 589856 | tf_op jit(solution)/shard_map/all_to_all | solution.py:767
  195.8 6.9 %project.1 = (bf16[96,2048]{1,0:T(8,128)(2,1)S(1)}, bf16[384,16,128]{2,1,0:T(8,128)(2,1)S(1)}) custom-call(s32[384]{0:T(512)S(1)} %select_reduce_fusion.token_of, bf16[8,96,384]{2,1,0:T(8,128)(2,1)S(1)} %all-to-all-done.mine, bf16[2048,2048]{1,0:T(8,128)(2,1)} %all-gather.3.cloned.1.call-done.weight_wide, ...), custom_call_target="tpu_custom_call" | custom-call | tf_op jit(solution)/shard_map/project/pallas_call | solution.py:593
  202.8 39.2 %all_to_all.15 = bf16[128,48,128]{2,1,0:T(8,128)(2,1)S(1)} all-to-all(bf16[128,48,128]{2,1,0:T(8,128)(2,1)S(1)} %bitcast.22), channel_id=1, replica_groups=mesh['z'=4,'x'=4,'y'=4,'c'=2] {'z','x','y','c'}, dimensions={0} | all-to-all | bytes 3145728 | tf_op jit(solution)/shard_map/all_to_all | solution.py:776
  241.9 9.9 %experts.1 = bf16[384,16,128]{2,1,0:T(8,128)(2,1)} custom-call(bf16[384,16,128]{2,1,0:T(8,128)(2,1)S(1)} %bitcast.18, bf16[2048,1024]{1,0:T(8,128)(2,1)S(1)} %bitcast.19, bf16[2048,1024]{1,0:T(8,128)(2,1)S(1)} %bitcast.20, bf16[1024,2048]{1,0:T(8,128)(2,1)S(1)} %bitcast.21), custom_call_target="tpu_custom_call" | custom-call | tf_op jit(solution)/shard_map/experts/pallas_call | solution.py:672
  251.9 4.8 %all-to-all-start.2 = ((bf16[128,48,128]{2,1,0:T(8,128)(2,1)}), bf16[128,48,128]{2,1,0:T(8,128)(2,1)S(1)}, u32[]{:S(2)}, u32[]{:S(2)}) async-start(bf16[128,48,128]{2,1,0:T(8,128)(2,1)} %bitcast.15), calls=%async_computation.2 | async-start | bytes 3145728 | tf_op jit(solution)/shard_map/all_to_all | solution.py:776
  257.0 24.3 %all-to-all-done.2 = bf16[128,48,128]{2,1,0:T(8,128)(2,1)S(1)} async-done(((bf16[128,48,128]{2,1,0:T(8,128)(2,1)}), bf16[128,48,128]{2,1,0:T(8,128)(2,1)S(1)}, u32[]{:S(2)}, u32[]{:S(2)}) %all-to-all-start.2) | async-done | bytes 1572896 | tf_op jit(solution)/shard_map/all_to_all | solution.py:776
  (88 shorter events, 23.4 us)
Async XLA Ops:
  6.5 189.2 %all-gather.5.cloned.1.call-start = ((), (), s32[]{:S(2)}) async-start(), calls=%async_computation.4 | async-start | bytes 4718592 | tf_op jit(solution)/shard_map/all_gather | solution.py:766
  9.6 186.2 %all-gather.3.cloned.1.call-start = ((), (), s32[]{:S(2)}) async-start(), calls=%async_computation.3 | async-start | bytes 9437184 | tf_op jit(solution)/shard_map/all_gather | solution.py:765
  10.3 15.7 %collective-permute-start = (bf16[1152,256]{1,0:T(8,128)(2,1)}, bf16[1152,256]{1,0:T(8,128)(2,1)S(1)}, u32[]{:S(2)}, u32[]{:S(2)}) collective-permute-start(bf16[1152,256]{1,0:T(8,128)(2,1)} %get-tuple-element.26.refs_3_.refs_1_.refs_4_), channel_id=1, source_target_pairs={{0,24},{8,0},{16,8},{24,16},{1,25},{9,1},{17,9},{25,17},{2,26},{10... | collective-permute-start | bytes 1769480 | tf_op jit(solution)/shard_map/ppermute | solution.py:433
  13.7 16.1 %collective-permute-start.1 = (bf16[768,256]{1,0:T(8,128)(2,1)}, bf16[768,256]{1,0:T(8,128)(2,1)S(1)}, u32[]{:S(2)}, u32[]{:S(2)}) collective-permute-start(bf16[768,256]{1,0:T(8,128)(2,1)} %get-tuple-element.30), channel_id=1, source_target_pairs={{0,32},{32,64},{64,96},{96,0},{1,33},{33,65},{65,97},{97,1},{2,34}... | collective-permute-start | bytes 1179656 | tf_op jit(solution)/shard_map/ppermute | solution.py:433
  15.4 18.0 %collective-permute-start.4 = (bf16[768,256]{1,0:T(8,128)(2,1)}, bf16[768,256]{1,0:T(8,128)(2,1)S(1)}, u32[]{:S(2)}, u32[]{:S(2)}) collective-permute-start(bf16[768,256]{1,0:T(8,128)(2,1)} %bitcast.32), channel_id=1, source_target_pairs={{0,8},{8,16},{16,24},{24,0},{1,9},{9,17},{17,25},{25,1},{2,10},{10... | collective-permute-start | bytes 1179656 | tf_op jit(solution)/shard_map/ppermute | solution.py:433
  15.4 20.2 %collective-permute-start.2 = (bf16[768,256]{1,0:T(8,128)(2,1)}, bf16[768,256]{1,0:T(8,128)(2,1)S(1)}, u32[]{:S(2)}, u32[]{:S(2)}) collective-permute-start(bf16[768,256]{1,0:T(8,128)(2,1)} %get-tuple-element.31), channel_id=1, source_target_pairs={{0,64},{32,96},{64,0},{96,32},{1,65},{33,97},{65,1},{97,33},{2,66}... | collective-permute-start | bytes 1179656 | tf_op jit(solution)/shard_map/ppermute | solution.py:433
  18.6 30.0 %collective-permute-start.5 = (bf16[1152,256]{1,0:T(8,128)(2,1)}, bf16[1152,256]{1,0:T(8,128)(2,1)S(1)}, u32[]{:S(2)}, u32[]{:S(2)}) collective-permute-start(bf16[1152,256]{1,0:T(8,128)(2,1)} %get-tuple-element.26.refs_3_.refs_1_.refs_4_), channel_id=1, source_target_pairs={{0,8},{8,16},{16,24},{24,0},{1,9},{9,17},{17,25},{25,1},{2,10},{10... | collective-permute-start | bytes 1769480 | tf_op jit(solution)/shard_map/ppermute | solution.py:433
  26.0 18.7 %collective-permute-start.3 = (bf16[768,256]{1,0:T(8,128)(2,1)}, bf16[768,256]{1,0:T(8,128)(2,1)}, u32[]{:S(2)}, u32[]{:S(2)}) collective-permute-start(bf16[768,256]{1,0:T(8,128)(2,1)} %get-tuple-element.32), channel_id=1, source_target_pairs={{0,96},{32,0},{64,32},{96,64},{1,97},{33,1},{65,33},{97,65},{2,98}... | collective-permute-start | bytes 1179656 | tf_op jit(solution)/shard_map/ppermute | solution.py:433
  29.8 18.8 %collective-permute-start.8 = (bf16[768,256]{1,0:T(8,128)(2,1)}, bf16[768,256]{1,0:T(8,128)(2,1)S(1)}, u32[]{:S(2)}, u32[]{:S(2)}) collective-permute-start(bf16[768,256]{1,0:T(8,128)(2,1)} %bitcast.33), channel_id=1, source_target_pairs={{0,24},{8,0},{16,8},{24,16},{1,25},{9,1},{17,9},{25,17},{2,26},{10... | collective-permute-start | bytes 1179656 | tf_op jit(solution)/shard_map/ppermute | solution.py:433
  33.3 15.4 %collective-permute-start.6 = (bf16[768,256]{1,0:T(8,128)(2,1)S(1)}, bf16[768,256]{1,0:T(8,128)(2,1)}, u32[]{:S(2)}, u32[]{:S(2)}) collective-permute-start(bf16[768,256]{1,0:T(8,128)(2,1)S(1)} %collective-permute-done.4.refs_4_.refs_5_), channel_id=1, source_target_pairs={{0,8},{8,16},{16,24},{24,0},{1,9},{9,17},{17,25},{25,1},{2,10},{10... | collective-permute-start | bytes 1179656 | tf_op jit(solution)/shard_map/ppermute | solution.py:433
  35.5 13.2 %collective-permute-start.7 = (bf16[768,256]{1,0:T(8,128)(2,1)S(1)}, bf16[768,256]{1,0:T(8,128)(2,1)}, u32[]{:S(2)}, u32[]{:S(2)}) collective-permute-start(bf16[768,256]{1,0:T(8,128)(2,1)S(1)} %slice.8), channel_id=1, source_target_pairs={{0,24},{8,0},{16,8},{24,16},{1,25},{9,1},{17,9},{25,17},{2,26},{10... | collective-permute-start | bytes 1179656 | tf_op jit(solution)/shard_map/ppermute | solution.py:433
  93.1 64.1 %collective-permute-start.10 = (bf16[528,768]{1,0:T(8,128)(2,1)}, bf16[528,768]{1,0:T(8,128)(2,1)}, u32[]{:S(2)}, u32[]{:S(2)}) collective-permute-start(bf16[528,768]{1,0:T(8,128)(2,1)} %shard_map.157), channel_id=1, source_target_pairs={{0,96},{32,64},{1,97},{33,65},{2,98},{34,66},{3,99},{35,67},{4,100... | collective-permute-start | bytes 2433032 | tf_op jit(solution)/shard_map/ppermute | solution.py:512
  95.3 62.7 %collective-permute-start.14 = (bf16[272,768]{1,0:T(8,128)(2,1)}, bf16[272,768]{1,0:T(8,128)(2,1)S(1)}, u32[]{:S(2)}, u32[]{:S(2)}) collective-permute-start(bf16[272,768]{1,0:T(8,128)(2,1)} %shard_map.156), channel_id=1, source_target_pairs={{0,8},{8,16},{16,24},{24,0},{1,9},{9,17},{17,25},{25,1},{2,10},{10... | collective-permute-start | bytes 1253384 | tf_op jit(solution)/shard_map/ppermute | solution.py:433
  96.3 52.0 %collective-permute-start.9 = (bf16[384,256]{1,0:T(8,128)(2,1)S(1)}, bf16[384,256]{1,0:T(8,128)(2,1)S(1)}, u32[]{:S(2)}, u32[]{:S(2)}) collective-permute-start(bf16[384,256]{1,0:T(8,128)(2,1)S(1)} %slice.9), channel_id=1, source_target_pairs={{0,8},{8,16},{16,24},{24,0},{1,9},{9,17},{17,25},{25,1},{2,10},{10... | collective-permute-start | bytes 589832 | tf_op jit(solution)/shard_map/ppermute | solution.py:433
  146.9 21.3 %collective-permute-start.12 = (bf16[528,768]{1,0:T(8,128)(2,1)}, bf16[528,768]{1,0:T(8,128)(2,1)S(1)}, u32[]{:S(2)}, u32[]{:S(2)}) collective-permute-start(bf16[528,768]{1,0:T(8,128)(2,1)} %get-tuple-element.35), channel_id=1, source_target_pairs={{0,32},{32,64},{64,96},{1,33},{33,65},{65,97},{2,34},{34,66},{66,9... | collective-permute-start | bytes 2433032 | tf_op jit(solution)/shard_map/ppermute | solution.py:437
  154.3 16.5 %collective-permute-start.13 = (bf16[528,768]{1,0:T(8,128)(2,1)}, bf16[528,768]{1,0:T(8,128)(2,1)S(1)}, u32[]{:S(2)}, u32[]{:S(2)}) collective-permute-start(bf16[528,768]{1,0:T(8,128)(2,1)} %get-tuple-element.41), channel_id=1, source_target_pairs={{0,96},{1,97},{2,98},{3,99},{4,100},{5,101},{6,102},{7,103},{8,104... | collective-permute-start | bytes 2433032 | tf_op jit(solution)/shard_map/ppermute | solution.py:437
  157.2 13.6 %collective-permute-start.11 = (bf16[528,768]{1,0:T(8,128)(2,1)}, bf16[528,768]{1,0:T(8,128)(2,1)S(1)}, u32[]{:S(2)}, u32[]{:S(2)}) collective-permute-start(bf16[528,768]{1,0:T(8,128)(2,1)} %collective-permute-done.10), channel_id=1, source_target_pairs={{96,64},{64,96},{97,65},{65,97},{98,66},{66,98},{99,67},{67,99},{1... | collective-permute-start | bytes 2433032 | tf_op jit(solution)/shard_map/ppermute | solution.py:522
  157.9 8.7 %collective-permute-start.15 = (bf16[272,768]{1,0:T(8,128)(2,1)}, bf16[272,768]{1,0:T(8,128)(2,1)}, u32[]{:S(2)}, u32[]{:S(2)}) collective-permute-start(bf16[272,768]{1,0:T(8,128)(2,1)} %get-tuple-element.37), channel_id=1, source_target_pairs={{0,24},{8,0},{16,8},{24,16},{1,25},{9,1},{17,9},{25,17},{2,26},{10... | collective-permute-start | bytes 1253384 | tf_op jit(solution)/shard_map/ppermute | solution.py:433
  158.0 10.2 %collective-permute-start.16 = (bf16[272,768]{1,0:T(8,128)(2,1)}, bf16[272,768]{1,0:T(8,128)(2,1)}, u32[]{:S(2)}, u32[]{:S(2)}) collective-permute-start(bf16[272,768]{1,0:T(8,128)(2,1)} %get-tuple-element.42), channel_id=1, source_target_pairs={{0,16},{8,24},{16,0},{24,8},{1,17},{9,25},{17,1},{25,9},{2,18},{10... | collective-permute-start | bytes 1253384 | tf_op jit(solution)/shard_map/ppermute | solution.py:433
  178.0 17.8 %all-to-all-start = ((bf16[8,96,384]{2,1,0:T(8,128)(2,1)}), bf16[8,96,384]{2,1,0:T(8,128)(2,1)S(1)}, u32[]{:S(2)}, u32[]{:S(2)}) async-start(bf16[8,96,384]{2,1,0:T(8,128)(2,1)} %bitcast.24), calls=%async_computation | async-start | bytes 1179648 | tf_op jit(solution)/shard_map/all_to_all | solution.py:767
  195.8 46.1 %copy-start = (bf16[1,2048,1024]{2,1,0:T(8,128)(2,1)S(1)}, bf16[1,2048,1024]{2,1,0:T(8,128)(2,1)}, u32[]{:S(2)}) copy-start(bf16[1,2048,1024]{2,1,0:T(8,128)(2,1)} %param.29) | copy-start | bytes 12582916
  195.8 46.1 %copy-start.1 = (bf16[1,2048,1024]{2,1,0:T(8,128)(2,1)S(1)}, bf16[1,2048,1024]{2,1,0:T(8,128)(2,1)}, u32[]{:S(2)}) copy-start(bf16[1,2048,1024]{2,1,0:T(8,128)(2,1)} %param.30) | copy-start | bytes 12582916
  202.7 49.1 %copy-start.4 = (bf16[96,2048]{1,0:T(8,128)(2,1)}, bf16[96,2048]{1,0:T(8,128)(2,1)S(1)}, u32[]{:S(2)}) copy-start(bf16[96,2048]{1,0:T(8,128)(2,1)S(1)} %get-tuple-element.46.stream) | copy-start | bytes 1179652
  251.9 29.4 %all-to-all-start.2 = ((bf16[128,48,128]{2,1,0:T(8,128)(2,1)}), bf16[128,48,128]{2,1,0:T(8,128)(2,1)S(1)}, u32[]{:S(2)}, u32[]{:S(2)}) async-start(bf16[128,48,128]{2,1,0:T(8,128)(2,1)} %bitcast.15), calls=%async_computation.2 | async-start | bytes 3145728 | tf_op jit(solution)/shard_map/all_to_all | solution.py:776
  (18 other events, 232.4 us)
Sparse Core Ops, SparseCore 0:
  9.7 35.6 all-gather.4
  47.1 49.6 all-gather.2

commit v4 on v3

--- a/solution.py
+++ b/solution.py
@@ -415,16 +415,17 @@
 
 def merge(place, lam, groups, widths):
     chunk = groups[0][0].shape[1]
+    block = chunk // 2
     counts = [len(parts) for parts in groups]
     flat = [part for parts in groups for part in parts]
     body = lambda *refs: merge_kernel(*refs, widths=widths, counts=counts)
     return pl.pallas_call(
         body,
-        grid=(chunk // BLOCK,),
+        grid=(chunk // block,),
         out_shape=jax.ShapeDtypeStruct((chunk, sum(widths)), jnp.bfloat16),
         in_specs=[pl.BlockSpec(memory_space=pltpu.SMEM)] * 2
-        + [pl.BlockSpec((part.shape[0], BLOCK), lambda i: (0, i)) for part in flat],
-        out_specs=pl.BlockSpec((BLOCK, sum(widths)), lambda i: (i, 0)),
+        + [pl.BlockSpec((part.shape[0], block), lambda i: (0, i)) for part in flat],
+        out_specs=pl.BlockSpec((block, sum(widths)), lambda i: (i, 0)),
         name="merge_reads",
     )(place, lam, *flat)
 
@@ -518,8 +519,8 @@
     )
     for d in (1, 3):
         sent[d] = onward(sent[d], "z", d)
+    sent[2] = lax.ppermute(after(relayed, side[1]), "z", [(3, 2), (2, 3)])
     rest_narrow = narrow(side[1], (narrow_rest_plan,), [values], narrow_sources, False)[0]
-    sent[2] = lax.ppermute(after(relayed, rest_narrow), "z", [(3, 2), (2, 3)])
     rest_wide = wide(rest_narrow, (wide_rest_plan,), [query_wide], wide_sources, False)[0]
     side = {s: around(side[s], "x", -s) for s in NARROW_ORDER}
     made = merge(
@@ -620,9 +621,6 @@
 
 def expert_kernel(arrived, gate, up, down, out, flat, rows, hidden):
     count, tiles, _ = arrived.shape
-    model, inner = gate.shape
-    steps = inner // BLOCK
-    columns = model // steps
 
     def spread(k, _):
         some = arrived[pl.ds(k * SOME, SOME)].astype(jnp.float32)
@@ -642,27 +640,12 @@
             jnp.bfloat16
         )
 
-    def widen(k, _):
-        part = pl.ds(pl.multiple_of(k * BLOCK, BLOCK), BLOCK)
-        gate_part = jnp.dot(rows[...], gate[:, part], preferred_element_type=jnp.float32)
-        up_part = jnp.dot(rows[...], up[:, part], preferred_element_type=jnp.float32)
-        hidden[:, part] = (gate_part * jax.nn.sigmoid(gate_part) * up_part).astype(jnp.bfloat16)
-        return 0
-
-    def narrow(k, _):
-        result = jnp.dot(
-            hidden[...],
-            down[:, pl.ds(pl.multiple_of(k * columns, columns), columns)],
-            preferred_element_type=jnp.float32,
-        )
-        for j in range(columns // LANES):
-            flat[pl.ds(k * (columns // LANES) + j, count, stride=tiles), :] = result[
-                :, j * LANES : (j + 1) * LANES
-            ]
-        return 0
-
-    lax.fori_loop(0, steps, widen, 0)
-    lax.fori_loop(0, steps, narrow, 0)
+    gate_part = jnp.dot(rows[...], gate[...], preferred_element_type=jnp.float32)
+    up_part = jnp.dot(rows[...], up[...], preferred_element_type=jnp.float32)
+    hidden[...] = (gate_part * jax.nn.sigmoid(gate_part) * up_part).astype(jnp.bfloat16)
+    result = jnp.dot(hidden[...], down[...], preferred_element_type=jnp.float32)
+    for j in range(tiles):
+        flat[pl.ds(j, count, stride=tiles), :] = result[:, j * LANES : (j + 1) * LANES]
     lax.fori_loop(0, count // SOME, gathered, 0)
 
 

time: 292 us -> 283 us (0.969)
  blocking collectives: 39.2 us -> 34.9 us
  waiting for transfers between devices: 52.3 us -> 48.2 us
  Pallas kernels: 140 us -> 137 us
    all_to_all x1, blocking collectives: 39.2 us -> 34.9 us  [exchanged(): lax.all_to_all(rows.reshape(experts_all, -1, LANES), SP_TP, split_axis=0,...]
    unnamed x45 -> x49, local copies, waits for them, and re-layouts: 5.31 us -> 7.24 us
  transfers between devices with their start and end apart: 21 -> 21, of which waited for: 7 -> 6; matrix products, arithmetic and copies ran while one was open for 1% -> 1% of each run, Pallas kernels for 40% -> 42%
where the time goes in v4:
time: 283 us
  Pallas kernels  137 us (48%)
  waiting for transfers between devices  48.2 us (17%)
  starting transfers between devices  39.3 us (14%)
  blocking collectives  34.9 us (12%)
  between operations  13.8 us (5%)
  local copies, waits for them, and re-layouts  8.47 us (3%)
    pallas_call x8, Pallas kernels, attend(): pl.pallas_call(body, out_shape=[out] * chunks, in_specs=[pl.BlockSpec(mem...  112 us
    all_to_all x1, blocking collectives, exchanged(): lax.all_to_all(rows.reshape(experts_all, -1, LANES), SP_TP, split_axis=0,...  34.9 us
    all_to_all x1, waiting for transfers between devices, exchanged(): lax.all_to_all(rows.reshape(experts_all, -1, LANES), SP_TP, split_axis=0,...  24.3 us
    ppermute x13, starting transfers between devices, around(): lax.ppermute(array, axis, [(k, (k + by) % RING) for k in range(RING)])  19.9 us
    ppermute x13, waiting for transfers between devices, around(): lax.ppermute(array, axis, [(k, (k + by) % RING) for k in range(RING)])  13.8 us
    all_to_all x1, starting transfers between devices, shards(): lax.all_to_all(heads.reshape(tp_size, local_rows, -1), TP, split_axis=0,...  9.81 us
    all_to_all x1, waiting for transfers between devices, shards(): lax.all_to_all(heads.reshape(tp_size, local_rows, -1), TP, split_axis=0,...  9.46 us
    pallas_call x1, Pallas kernels, experts(): pl.pallas_call(expert_kernel, out_shape=jax.ShapeDtypeStruct(arrived.shap...  7.78 us
  transfers between devices with their start and end apart: 21, of which 6 were waited for; matrix products, arithmetic and copies ran while one was open for 1% of the time, Pallas kernels for 42%

profile of v4, /device:TPU:1, one launch (start us, length us, event | category | flops | bytes accessed | tf_op | source)
XLA Modules:
  0.0 282.6 jit_solution(13981729526013729716)
XLA Ops:
  6.5 3.0 %pack.1 = (bf16[1152,256]{1,0:T(8,128)(2,1)}, bf16[768,256]{1,0:T(8,128)(2,1)}, bf16[768,256]{1,0:T(8,128)(2,1)}, bf16[768,256]{1,0:T(8,128)(2,1)}, bf16[768,256]{1,0:T(8,128)(2,1)}) custom-call(bf16[768,256]{1,0:T(8,128)(2,1)} %bitcast.26, bf16[768,256]{1,0:T(8,128)(2,1)} %bitcast.25, bf16[768,128]{1,0:T(8,128)(2,1)} %bitcast.29, ...), custom_call_target="tpu_custom_call" | custom-call | tf_op jit(solution)/shard_map/pack/pallas_call | solution.py:62
  10.3 3.4 %collective-permute-start = (bf16[1152,256]{1,0:T(8,128)(2,1)}, bf16[1152,256]{1,0:T(8,128)(2,1)S(1)}, u32[]{:S(2)}, u32[]{:S(2)}) collective-permute-start(bf16[1152,256]{1,0:T(8,128)(2,1)} %get-tuple-element.26.refs_3_.refs_1_.refs_4_), channel_id=1, source_target_pairs={{0,24},{8,0},{16,8},{24,16},{1,25},{9,1},{17,9},{25,17},{2,26},{10... | collective-permute-start | bytes 1769480 | tf_op jit(solution)/shard_map/ppermute | solution.py:434
  15.3 3.3 %collective-permute-start.2 = (bf16[768,256]{1,0:T(8,128)(2,1)}, bf16[768,256]{1,0:T(8,128)(2,1)S(1)}, u32[]{:S(2)}, u32[]{:S(2)}) collective-permute-start(bf16[768,256]{1,0:T(8,128)(2,1)} %get-tuple-element.31), channel_id=1, source_target_pairs={{0,64},{32,96},{64,0},{96,32},{1,65},{33,97},{65,1},{97,33},{2,66}... | collective-permute-start | bytes 1179656 | tf_op jit(solution)/shard_map/ppermute | solution.py:434
  18.8 7.2 %collective-permute-done.refs_1_.refs_9_.refs_10_ = bf16[1152,256]{1,0:T(8,128)(2,1)S(1)} collective-permute-done((bf16[1152,256]{1,0:T(8,128)(2,1)}, bf16[1152,256]{1,0:T(8,128)(2,1)S(1)}, u32[]{:S(2)}, u32[]{:S(2)}) %collective-permute-start) | collective-permute-done | bytes 589856 | tf_op jit(solution)/shard_map/ppermute | solution.py:434
  26.0 3.7 %collective-permute-start.3 = (bf16[768,256]{1,0:T(8,128)(2,1)}, bf16[768,256]{1,0:T(8,128)(2,1)S(1)}, u32[]{:S(2)}, u32[]{:S(2)}) collective-permute-start(bf16[768,256]{1,0:T(8,128)(2,1)} %get-tuple-element.32), channel_id=1, source_target_pairs={{0,96},{32,0},{64,32},{96,64},{1,97},{33,1},{65,33},{97,65},{2,98}... | collective-permute-start | bytes 1179656 | tf_op jit(solution)/shard_map/ppermute | solution.py:434
  29.8 3.5 %collective-permute-start.8 = (bf16[768,256]{1,0:T(8,128)(2,1)}, bf16[768,256]{1,0:T(8,128)(2,1)S(1)}, u32[]{:S(2)}, u32[]{:S(2)}) collective-permute-start(bf16[768,256]{1,0:T(8,128)(2,1)} %bitcast.33), channel_id=1, source_target_pairs={{0,24},{8,0},{16,8},{24,16},{1,25},{9,1},{17,9},{25,17},{2,26},{10... | collective-permute-start | bytes 1179656 | tf_op jit(solution)/shard_map/ppermute | solution.py:434
  33.3 2.2 collective-permute-done.2.refs_4_.refs_1_.refs_5_
  36.6 4.2 %shard_map.154.refs_2_ = bf16[528,768]{1,0:T(8,128)(2,1)} custom-call(s32[2]{0:T(128)} %pad_add_fusion.refs_0_, bf16[768,256]{1,0:T(8,128)(2,1)} %bitcast.27, bf16[768,256]{1,0:T(8,128)(2,1)} %bitcast.34, bf16[1152,256]{1,0:T(8,128)(2,1)} %get-tuple-element.26.refs_3_.refs_1_.refs_4_), custom_call_target="tpu_custom_call" | custom-call | flops 1811939328 | bytes 786432 | tf_op jit(solution)/shard_map/pallas_call | solution.py:347
  40.9 3.7 %shard_map.155.refs_7_ = bf16[272,768]{1,0:T(8,128)(2,1)} custom-call(s32[2]{0:T(128)} %pad_add_fusion.refs_0_, bf16[1152,256]{1,0:T(8,128)(2,1)} %get-tuple-element.26.refs_3_.refs_1_.refs_4_, bf16[768,256]{1,0:T(8,128)(2,1)} %get-tuple-element.28.refs_2_.refs_3_), custom_call_target="tpu_custom_call" | custom-call | flops 905969664 | bytes 393216 | tf_op jit(solution)/shard_map/pallas_call | solution.py:347
  45.4 3.9 %shard_map.156 = bf16[272,768]{1,0:T(8,128)(2,1)} custom-call(s32[2]{0:T(128)} %pad_add_fusion.refs_0_, bf16[1152,256]{1,0:T(8,128)(2,1)} %copy-done.11, bf16[768,256]{1,0:T(8,128)(2,1)} %get-tuple-element.28.refs_2_.refs_3_, bf16[768,256]{1,0:T(8,128)(2,1)} %copy-done.17, bf16[768,256]{1,0:T(8,128)(2,1)} %copy-done.18, bf16[768,256]{1,0:T(8,128)(2,1)} %copy-done.19), custom_call_target="tpu_custom_call" | custom-call | flops 905969664 | bytes 1572864 | tf_op jit(solution)/shard_map/pallas_call | solution.py:347
  50.3 43.5 %shard_map.157 = bf16[528,768]{1,0:T(8,128)(2,1)} custom-call(s32[2]{0:T(128)} %pad_add_fusion.refs_0_, bf16[768,256]{1,0:T(8,128)(2,1)} %copy-done.18, bf16[768,256]{1,0:T(8,128)(2,1)} %bitcast.35, bf16[1152,256]{1,0:T(8,128)(2,1)} %get-tuple-element.26.refs_3_.refs_1_.refs_4_, bf16[768,256]{1,0:T(8,128)(2,1)} %copy-done.16, bf16[1152,256]{1,0:T(8,128)(2,1)} %copy-done.12, ...), custom_call_target="tpu_custom_call" | custom-call | flops 1811939328 | bytes 3145728 | tf_op jit(solution)/shard_map/pallas_call | solution.py:347
  96.8 49.3 %shard_map.158 = (bf16[528,768]{1,0:T(8,128)(2,1)}, bf16[528,768]{1,0:T(8,128)(2,1)}) custom-call(s32[2]{0:T(128)} %pad_add_fusion.refs_0_, bf16[768,256]{1,0:T(8,128)(2,1)} %copy-done.19, bf16[768,256]{1,0:T(8,128)(2,1)} %copy-done.17, bf16[768,256]{1,0:T(8,128)(2,1)} %bitcast.36, bf16[1152,256]{1,0:T(8,128)(2,1)} %get-tuple-element.26.refs_3_.refs_1_.refs_4_, ...), custom_call_target="tpu_custom_call" | custom-call | flops 3623878656 | bytes 3145728 | tf_op jit(solution)/shard_map/pallas_call | solution.py:347
  149.5 5.4 %shard_map.159 = (bf16[272,768]{1,0:T(8,128)(2,1)}, bf16[272,768]{1,0:T(8,128)(2,1)}) custom-call(s32[2]{0:T(128)} %pad_add_fusion.refs_0_, bf16[1152,256]{1,0:T(8,128)(2,1)} %copy-done.12, bf16[384,256]{1,0:T(8,128)(2,1)} %copy-done.21, bf16[768,256]{1,0:T(8,128)(2,1)} %get-tuple-element.28.refs_2_.refs_3_, bf16[768,256]{1,0:T(8,128)(2,1)} %copy-done.17, ...), custom_call_target="tpu_custom_call" | custom-call | flops 1811939328 | bytes 1572864 | tf_op jit(solution)/shard_map/pallas_call | solution.py:347
  156.6 2.8 %collective-permute-start.16 = (bf16[272,768]{1,0:T(8,128)(2,1)}, bf16[272,768]{1,0:T(8,128)(2,1)}, u32[]{:S(2)}, u32[]{:S(2)}) collective-permute-start(bf16[272,768]{1,0:T(8,128)(2,1)} %get-tuple-element.42), channel_id=1, source_target_pairs={{0,16},{8,24},{16,0},{24,8},{1,17},{9,25},{17,1},{25,9},{2,18},{10... | collective-permute-start | bytes 1253384 | tf_op jit(solution)/shard_map/ppermute | solution.py:434
  162.5 2.8 collective-permute-done.15.refs_10_
  168.9 5.0 %merge_reads.1 = bf16[768,384]{1,0:T(8,128)(2,1)} custom-call(s32[2]{0:T(128)} %pad_add_fusion.refs_0_, f32[2,1]{1,0:T(2,128)} %copy.23.refs_1_, bf16[528,768]{1,0:T(8,128)(2,1)} %shard_map.154.refs_2_, bf16[528,768]{1,0:T(8,128)(2,1)} %shard_map.161.refs_3_, bf16[528,768]{1,0:T(8,128)(2,1)} %copy-done.9, bf16[528,768]{1,0:T(8,128)(2,1)} %copy-done.7, ...), custom_call_target="tpu_custom_call" | custom-call | tf_op jit(solution)/shard_map/merge_reads/pallas_call | solution.py:422
  173.9 9.8 %all-to-all-start = ((bf16[8,96,384]{2,1,0:T(8,128)(2,1)}), bf16[8,96,384]{2,1,0:T(8,128)(2,1)S(1)}, u32[]{:S(2)}, u32[]{:S(2)}) async-start(bf16[8,96,384]{2,1,0:T(8,128)(2,1)} %bitcast.24), calls=%async_computation | async-start | bytes 1179648 | tf_op jit(solution)/shard_map/all_to_all | solution.py:750
  184.3 9.5 %all-to-all-done.mine = bf16[8,96,384]{2,1,0:T(8,128)(2,1)S(1)} async-done(((bf16[8,96,384]{2,1,0:T(8,128)(2,1)}), bf16[8,96,384]{2,1,0:T(8,128)(2,1)S(1)}, u32[]{:S(2)}, u32[]{:S(2)}) %all-to-all-start) | async-done | bytes 589856 | tf_op jit(solution)/shard_map/all_to_all | solution.py:750
  193.8 6.9 %project.1 = (bf16[96,2048]{1,0:T(8,128)(2,1)S(1)}, bf16[384,16,128]{2,1,0:T(8,128)(2,1)S(1)}) custom-call(s32[384]{0:T(512)S(1)} %select_reduce_fusion.token_of, bf16[8,96,384]{2,1,0:T(8,128)(2,1)S(1)} %all-to-all-done.mine, bf16[2048,2048]{1,0:T(8,128)(2,1)} %all-gather.3.cloned.1.call-done.weight_wide, ...), custom_call_target="tpu_custom_call" | custom-call | tf_op jit(solution)/shard_map/project/pallas_call | solution.py:594
  200.8 34.9 %all_to_all.15 = bf16[128,48,128]{2,1,0:T(8,128)(2,1)S(1)} all-to-all(bf16[128,48,128]{2,1,0:T(8,128)(2,1)S(1)} %bitcast.22), channel_id=1, replica_groups=mesh['z'=4,'x'=4,'y'=4,'c'=2] {'z','x','y','c'}, dimensions={0} | all-to-all | bytes 3145728 | tf_op jit(solution)/shard_map/all_to_all | solution.py:759
  235.7 7.8 %experts.1 = bf16[384,16,128]{2,1,0:T(8,128)(2,1)} custom-call(bf16[384,16,128]{2,1,0:T(8,128)(2,1)S(1)} %bitcast.18, bf16[2048,1024]{1,0:T(8,128)(2,1)S(1)} %bitcast.19, bf16[2048,1024]{1,0:T(8,128)(2,1)S(1)} %bitcast.20, bf16[1024,2048]{1,0:T(8,128)(2,1)S(1)} %bitcast.21), custom_call_target="tpu_custom_call" | custom-call | tf_op jit(solution)/shard_map/experts/pallas_call | solution.py:655
  243.4 4.8 %all-to-all-start.2 = ((bf16[128,48,128]{2,1,0:T(8,128)(2,1)}), bf16[128,48,128]{2,1,0:T(8,128)(2,1)S(1)}, u32[]{:S(2)}, u32[]{:S(2)}) async-start(bf16[128,48,128]{2,1,0:T(8,128)(2,1)} %bitcast.15), calls=%async_computation.2 | async-start | bytes 3145728 | tf_op jit(solution)/shard_map/all_to_all | solution.py:759
  248.5 24.3 %all-to-all-done.2 = bf16[128,48,128]{2,1,0:T(8,128)(2,1)S(1)} async-done(((bf16[128,48,128]{2,1,0:T(8,128)(2,1)}), bf16[128,48,128]{2,1,0:T(8,128)(2,1)S(1)}, u32[]{:S(2)}, u32[]{:S(2)}) %all-to-all-start.2) | async-done | bytes 1572896 | tf_op jit(solution)/shard_map/all_to_all | solution.py:759
  273.8 1.9 combine.1
  (92 shorter events, 21.9 us)
Async XLA Ops:
  6.5 187.2 %all-gather.5.cloned.1.call-start = ((), (), s32[]{:S(2)}) async-start(), calls=%async_computation.4 | async-start | bytes 4718592 | tf_op jit(solution)/shard_map/all_gather | solution.py:749
  9.6 184.2 %all-gather.3.cloned.1.call-start = ((), (), s32[]{:S(2)}) async-start(), calls=%async_computation.3 | async-start | bytes 9437184 | tf_op jit(solution)/shard_map/all_gather | solution.py:748
  10.3 15.7 %collective-permute-start = (bf16[1152,256]{1,0:T(8,128)(2,1)}, bf16[1152,256]{1,0:T(8,128)(2,1)S(1)}, u32[]{:S(2)}, u32[]{:S(2)}) collective-permute-start(bf16[1152,256]{1,0:T(8,128)(2,1)} %get-tuple-element.26.refs_3_.refs_1_.refs_4_), channel_id=1, source_target_pairs={{0,24},{8,0},{16,8},{24,16},{1,25},{9,1},{17,9},{25,17},{2,26},{10... | collective-permute-start | bytes 1769480 | tf_op jit(solution)/shard_map/ppermute | solution.py:434
  13.7 16.1 %collective-permute-start.1 = (bf16[768,256]{1,0:T(8,128)(2,1)}, bf16[768,256]{1,0:T(8,128)(2,1)S(1)}, u32[]{:S(2)}, u32[]{:S(2)}) collective-permute-start(bf16[768,256]{1,0:T(8,128)(2,1)} %get-tuple-element.30), channel_id=1, source_target_pairs={{0,32},{32,64},{64,96},{96,0},{1,33},{33,65},{65,97},{97,1},{2,34}... | collective-permute-start | bytes 1179656 | tf_op jit(solution)/shard_map/ppermute | solution.py:434
  15.3 18.0 %collective-permute-start.4 = (bf16[768,256]{1,0:T(8,128)(2,1)}, bf16[768,256]{1,0:T(8,128)(2,1)S(1)}, u32[]{:S(2)}, u32[]{:S(2)}) collective-permute-start(bf16[768,256]{1,0:T(8,128)(2,1)} %bitcast.32), channel_id=1, source_target_pairs={{0,8},{8,16},{16,24},{24,0},{1,9},{9,17},{17,25},{25,1},{2,10},{10... | collective-permute-start | bytes 1179656 | tf_op jit(solution)/shard_map/ppermute | solution.py:434
  15.3 20.2 %collective-permute-start.2 = (bf16[768,256]{1,0:T(8,128)(2,1)}, bf16[768,256]{1,0:T(8,128)(2,1)S(1)}, u32[]{:S(2)}, u32[]{:S(2)}) collective-permute-start(bf16[768,256]{1,0:T(8,128)(2,1)} %get-tuple-element.31), channel_id=1, source_target_pairs={{0,64},{32,96},{64,0},{96,32},{1,65},{33,97},{65,1},{97,33},{2,66}... | collective-permute-start | bytes 1179656 | tf_op jit(solution)/shard_map/ppermute | solution.py:434
  18.6 30.7 %collective-permute-start.5 = (bf16[1152,256]{1,0:T(8,128)(2,1)}, bf16[1152,256]{1,0:T(8,128)(2,1)S(1)}, u32[]{:S(2)}, u32[]{:S(2)}) collective-permute-start(bf16[1152,256]{1,0:T(8,128)(2,1)} %get-tuple-element.26.refs_3_.refs_1_.refs_4_), channel_id=1, source_target_pairs={{0,8},{8,16},{16,24},{24,0},{1,9},{9,17},{17,25},{25,1},{2,10},{10... | collective-permute-start | bytes 1769480 | tf_op jit(solution)/shard_map/ppermute | solution.py:434
  26.0 18.6 %collective-permute-start.3 = (bf16[768,256]{1,0:T(8,128)(2,1)}, bf16[768,256]{1,0:T(8,128)(2,1)S(1)}, u32[]{:S(2)}, u32[]{:S(2)}) collective-permute-start(bf16[768,256]{1,0:T(8,128)(2,1)} %get-tuple-element.32), channel_id=1, source_target_pairs={{0,96},{32,0},{64,32},{96,64},{1,97},{33,1},{65,33},{97,65},{2,98}... | collective-permute-start | bytes 1179656 | tf_op jit(solution)/shard_map/ppermute | solution.py:434
  29.8 19.5 %collective-permute-start.8 = (bf16[768,256]{1,0:T(8,128)(2,1)}, bf16[768,256]{1,0:T(8,128)(2,1)S(1)}, u32[]{:S(2)}, u32[]{:S(2)}) collective-permute-start(bf16[768,256]{1,0:T(8,128)(2,1)} %bitcast.33), channel_id=1, source_target_pairs={{0,24},{8,0},{16,8},{24,16},{1,25},{9,1},{17,9},{25,17},{2,26},{10... | collective-permute-start | bytes 1179656 | tf_op jit(solution)/shard_map/ppermute | solution.py:434
  33.3 16.1 %collective-permute-start.6 = (bf16[768,256]{1,0:T(8,128)(2,1)S(1)}, bf16[768,256]{1,0:T(8,128)(2,1)}, u32[]{:S(2)}, u32[]{:S(2)}) collective-permute-start(bf16[768,256]{1,0:T(8,128)(2,1)S(1)} %collective-permute-done.4.refs_4_.refs_5_), channel_id=1, source_target_pairs={{0,8},{8,16},{16,24},{24,0},{1,9},{9,17},{17,25},{25,1},{2,10},{10... | collective-permute-start | bytes 1179656 | tf_op jit(solution)/shard_map/ppermute | solution.py:434
  35.5 13.9 %collective-permute-start.7 = (bf16[768,256]{1,0:T(8,128)(2,1)S(1)}, bf16[768,256]{1,0:T(8,128)(2,1)}, u32[]{:S(2)}, u32[]{:S(2)}) collective-permute-start(bf16[768,256]{1,0:T(8,128)(2,1)S(1)} %slice.8), channel_id=1, source_target_pairs={{0,24},{8,0},{16,8},{24,16},{1,25},{9,1},{17,9},{25,17},{2,26},{10... | collective-permute-start | bytes 1179656 | tf_op jit(solution)/shard_map/ppermute | solution.py:434
  93.8 61.1 %collective-permute-start.10 = (bf16[528,768]{1,0:T(8,128)(2,1)}, bf16[528,768]{1,0:T(8,128)(2,1)S(1)}, u32[]{:S(2)}, u32[]{:S(2)}) collective-permute-start(bf16[528,768]{1,0:T(8,128)(2,1)} %shard_map.157), channel_id=1, source_target_pairs={{0,96},{32,64},{1,97},{33,65},{2,98},{34,66},{3,99},{35,67},{4,100... | collective-permute-start | bytes 2433032 | tf_op jit(solution)/shard_map/ppermute | solution.py:513
  95.2 61.4 %collective-permute-start.14 = (bf16[272,768]{1,0:T(8,128)(2,1)}, bf16[272,768]{1,0:T(8,128)(2,1)S(1)}, u32[]{:S(2)}, u32[]{:S(2)}) collective-permute-start(bf16[272,768]{1,0:T(8,128)(2,1)} %shard_map.156), channel_id=1, source_target_pairs={{0,8},{8,16},{16,24},{24,0},{1,9},{9,17},{17,25},{25,1},{2,10},{10... | collective-permute-start | bytes 1253384 | tf_op jit(solution)/shard_map/ppermute | solution.py:434
  96.2 52.6 %collective-permute-start.9 = (bf16[384,256]{1,0:T(8,128)(2,1)S(1)}, bf16[384,256]{1,0:T(8,128)(2,1)S(1)}, u32[]{:S(2)}, u32[]{:S(2)}) collective-permute-start(bf16[384,256]{1,0:T(8,128)(2,1)S(1)} %slice.9), channel_id=1, source_target_pairs={{0,8},{8,16},{16,24},{24,0},{1,9},{9,17},{17,25},{25,1},{2,10},{10... | collective-permute-start | bytes 589832 | tf_op jit(solution)/shard_map/ppermute | solution.py:434
  146.1 20.7 %collective-permute-start.12 = (bf16[528,768]{1,0:T(8,128)(2,1)}, bf16[528,768]{1,0:T(8,128)(2,1)S(1)}, u32[]{:S(2)}, u32[]{:S(2)}) collective-permute-start(bf16[528,768]{1,0:T(8,128)(2,1)} %get-tuple-element.35), channel_id=1, source_target_pairs={{0,32},{32,64},{64,96},{1,33},{33,65},{65,97},{2,34},{34,66},{66,9... | collective-permute-start | bytes 2433032 | tf_op jit(solution)/shard_map/ppermute | solution.py:438
  147.5 19.3 %collective-permute-start.13 = (bf16[528,768]{1,0:T(8,128)(2,1)}, bf16[528,768]{1,0:T(8,128)(2,1)S(1)}, u32[]{:S(2)}, u32[]{:S(2)}) collective-permute-start(bf16[528,768]{1,0:T(8,128)(2,1)} %get-tuple-element.41), channel_id=1, source_target_pairs={{0,96},{1,97},{2,98},{3,99},{4,100},{5,101},{6,102},{7,103},{8,104... | collective-permute-start | bytes 2433032 | tf_op jit(solution)/shard_map/ppermute | solution.py:438
  155.8 11.0 %collective-permute-start.11 = (bf16[528,768]{1,0:T(8,128)(2,1)}, bf16[528,768]{1,0:T(8,128)(2,1)S(1)}, u32[]{:S(2)}, u32[]{:S(2)}) collective-permute-start(bf16[528,768]{1,0:T(8,128)(2,1)} %copy-done.15), channel_id=1, source_target_pairs={{96,64},{64,96},{97,65},{65,97},{98,66},{66,98},{99,67},{67,99},{1... | collective-permute-start | bytes 2433032 | tf_op jit(solution)/shard_map/ppermute | solution.py:522
  156.5 8.7 %collective-permute-start.15 = (bf16[272,768]{1,0:T(8,128)(2,1)}, bf16[272,768]{1,0:T(8,128)(2,1)}, u32[]{:S(2)}, u32[]{:S(2)}) collective-permute-start(bf16[272,768]{1,0:T(8,128)(2,1)} %get-tuple-element.37), channel_id=1, source_target_pairs={{0,24},{8,0},{16,8},{24,16},{1,25},{9,1},{17,9},{25,17},{2,26},{10... | collective-permute-start | bytes 1253384 | tf_op jit(solution)/shard_map/ppermute | solution.py:434
  156.6 10.2 %collective-permute-start.16 = (bf16[272,768]{1,0:T(8,128)(2,1)}, bf16[272,768]{1,0:T(8,128)(2,1)}, u32[]{:S(2)}, u32[]{:S(2)}) collective-permute-start(bf16[272,768]{1,0:T(8,128)(2,1)} %get-tuple-element.42), channel_id=1, source_target_pairs={{0,16},{8,24},{16,0},{24,8},{1,17},{9,25},{17,1},{25,9},{2,18},{10... | collective-permute-start | bytes 1253384 | tf_op jit(solution)/shard_map/ppermute | solution.py:434
  173.9 19.9 %all-to-all-start = ((bf16[8,96,384]{2,1,0:T(8,128)(2,1)}), bf16[8,96,384]{2,1,0:T(8,128)(2,1)S(1)}, u32[]{:S(2)}, u32[]{:S(2)}) async-start(bf16[8,96,384]{2,1,0:T(8,128)(2,1)} %bitcast.24), calls=%async_computation | async-start | bytes 1179648 | tf_op jit(solution)/shard_map/all_to_all | solution.py:750
  193.8 41.8 %copy-start = (bf16[1,2048,1024]{2,1,0:T(8,128)(2,1)S(1)}, bf16[1,2048,1024]{2,1,0:T(8,128)(2,1)}, u32[]{:S(2)}) copy-start(bf16[1,2048,1024]{2,1,0:T(8,128)(2,1)} %param.29) | copy-start | bytes 12582916
  193.8 41.8 %copy-start.1 = (bf16[1,2048,1024]{2,1,0:T(8,128)(2,1)S(1)}, bf16[1,2048,1024]{2,1,0:T(8,128)(2,1)}, u32[]{:S(2)}) copy-start(bf16[1,2048,1024]{2,1,0:T(8,128)(2,1)} %param.30) | copy-start | bytes 12582916
  200.7 42.7 %copy-start.4 = (bf16[96,2048]{1,0:T(8,128)(2,1)}, bf16[96,2048]{1,0:T(8,128)(2,1)S(1)}, u32[]{:S(2)}) copy-start(bf16[96,2048]{1,0:T(8,128)(2,1)S(1)} %get-tuple-element.46.stream) | copy-start | bytes 1179652
  243.4 29.4 %all-to-all-start.2 = ((bf16[128,48,128]{2,1,0:T(8,128)(2,1)}), bf16[128,48,128]{2,1,0:T(8,128)(2,1)S(1)}, u32[]{:S(2)}, u32[]{:S(2)}) async-start(bf16[128,48,128]{2,1,0:T(8,128)(2,1)} %bitcast.15), calls=%async_computation.2 | async-start | bytes 3145728 | tf_op jit(solution)/shard_map/all_to_all | solution.py:759
  (20 other events, 218.1 us)
Sparse Core Ops, SparseCore 0:
  9.7 35.6 all-gather.4
  47.1 49.6 all-gather.2

commit v5 on v4

--- a/solution.py
+++ b/solution.py
@@ -510,16 +510,16 @@
     side, sent = {}, {}
     side[3] = narrow(diag_narrow, (narrow_plan(3),), [q_side[3]], narrow_sources, False)[0]
     sent[2] = wide(side[3], (wide_plan(2),), [q_later[2]], wide_sources, False)[0]
-    relayed = lax.ppermute(sent[2], "z", [(0, 3), (1, 2)])
+    first_sent = sent[2]
+    sent[2] = onward(sent[2], "z", 2)
     sent[1], sent[3] = wide(
-        sent[2], (wide_plan(1), wide_plan(3)), [q_later[1], q_later[3]], wide_sources, False,
+        first_sent, (wide_plan(1), wide_plan(3)), [q_later[1], q_later[3]], wide_sources, False,
     )
     side[1], side[2] = narrow(
         sent[1], (narrow_plan(1), narrow_plan(2)), [q_side[1], q_side[2]], narrow_sources, False,
     )
     for d in (1, 3):
         sent[d] = onward(sent[d], "z", d)
-    sent[2] = lax.ppermute(after(relayed, side[1]), "z", [(3, 2), (2, 3)])
     rest_narrow = narrow(side[1], (narrow_rest_plan,), [values], narrow_sources, False)[0]
     rest_wide = wide(rest_narrow, (wide_rest_plan,), [query_wide], wide_sources, False)[0]
     side = {s: around(side[s], "x", -s) for s in NARROW_ORDER}

time: 283 us -> 288 us (1.018)
  waiting for transfers between devices: 48.2 us -> 63.7 us
  starting transfers between devices: 39.3 us -> 34 us
  blocking collectives: 34.9 us -> 32 us
    ppermute x2 -> x3, waiting for transfers between devices: 0.01 us -> 7.75 us  [onward(): lax.ppermute(array, axis, [(k, k + by) for k in range(RING) if 0 <= k + b...]
    ppermute x13, waiting for transfers between devices: 13.8 us -> 21.5 us  [around(): lax.ppermute(array, axis, [(k, (k + by) % RING) for k in range(RING)])]
    all_to_all x1, blocking collectives: 34.9 us -> 32 us  [exchanged(): lax.all_to_all(rows.reshape(experts_all, -1, LANES), SP_TP, split_axis=0,...]
    unnamed x49 -> x47, local copies, waits for them, and re-layouts: 7.24 us -> 5.23 us
  transfers between devices with their start and end apart: 21 -> 20, of which waited for: 6 -> 8; matrix products, arithmetic and copies ran while one was open for 1% -> 1% of each run, Pallas kernels for 42% -> 41%
where the time goes in v5:
time: 288 us
  Pallas kernels  137 us (48%)
  waiting for transfers between devices  63.7 us (22%)
  starting transfers between devices  34 us (12%)
  blocking collectives  32 us (11%)
  between operations  13.8 us (5%)
  local copies, waits for them, and re-layouts  6.47 us (2%)
    pallas_call x8, Pallas kernels, attend(): pl.pallas_call(body, out_shape=[out] * chunks, in_specs=[pl.BlockSpec(mem...  112 us
    all_to_all x1, blocking collectives, exchanged(): lax.all_to_all(rows.reshape(experts_all, -1, LANES), SP_TP, split_axis=0,...  32 us
    all_to_all x1, waiting for transfers between devices, exchanged(): lax.all_to_all(rows.reshape(experts_all, -1, LANES), SP_TP, split_axis=0,...  24.3 us
    ppermute x13, waiting for transfers between devices, around(): lax.ppermute(array, axis, [(k, (k + by) % RING) for k in range(RING)])  21.5 us
    ppermute x13, starting transfers between devices, around(): lax.ppermute(array, axis, [(k, (k + by) % RING) for k in range(RING)])  17.5 us
    all_to_all x1, waiting for transfers between devices, shards(): lax.all_to_all(heads.reshape(tp_size, local_rows, -1), TP, split_axis=0,...  9.46 us
    pallas_call x1, Pallas kernels, experts(): pl.pallas_call(expert_kernel, out_shape=jax.ShapeDtypeStruct(arrived.shap...  7.79 us
    ppermute x3, waiting for transfers between devices, onward(): lax.ppermute(array, axis, [(k, k + by) for k in range(RING) if 0 <= k + b...  7.75 us
  transfers between devices with their start and end apart: 20, of which 8 were waited for; matrix products, arithmetic and copies ran while one was open for 1% of the time, Pallas kernels for 41%

profile of v5, /device:TPU:1, one launch (start us, length us, event | category | flops | bytes accessed | tf_op | source)
XLA Modules:
  0.0 287.7 jit_solution(9771173967939519138)
XLA Ops:
  6.5 3.0 %pack.1 = (bf16[1152,256]{1,0:T(8,128)(2,1)}, bf16[768,256]{1,0:T(8,128)(2,1)}, bf16[768,256]{1,0:T(8,128)(2,1)}, bf16[768,256]{1,0:T(8,128)(2,1)}, bf16[768,256]{1,0:T(8,128)(2,1)}) custom-call(bf16[768,256]{1,0:T(8,128)(2,1)} %bitcast.26, bf16[768,256]{1,0:T(8,128)(2,1)} %bitcast.25, bf16[768,128]{1,0:T(8,128)(2,1)} %bitcast.29, ...), custom_call_target="tpu_custom_call" | custom-call | tf_op jit(solution)/shard_map/pack/pallas_call | solution.py:62
  10.3 3.4 %collective-permute-start = (bf16[1152,256]{1,0:T(8,128)(2,1)}, bf16[1152,256]{1,0:T(8,128)(2,1)S(1)}, u32[]{:S(2)}, u32[]{:S(2)}) collective-permute-start(bf16[1152,256]{1,0:T(8,128)(2,1)} %get-tuple-element.25.refs_3_.refs_1_.refs_4_), channel_id=1, source_target_pairs={{0,24},{8,0},{16,8},{24,16},{1,25},{9,1},{17,9},{25,17},{2,26},{10... | collective-permute-start | bytes 1769480 | tf_op jit(solution)/shard_map/ppermute | solution.py:434
  15.3 3.3 %collective-permute-start.2 = (bf16[768,256]{1,0:T(8,128)(2,1)}, bf16[768,256]{1,0:T(8,128)(2,1)S(1)}, u32[]{:S(2)}, u32[]{:S(2)}) collective-permute-start(bf16[768,256]{1,0:T(8,128)(2,1)} %get-tuple-element.30), channel_id=1, source_target_pairs={{0,64},{32,96},{64,0},{96,32},{1,65},{33,97},{65,1},{97,33},{2,66}... | collective-permute-start | bytes 1179656 | tf_op jit(solution)/shard_map/ppermute | solution.py:434
  18.8 7.2 %collective-permute-done.refs_1_.refs_9_.refs_10_ = bf16[1152,256]{1,0:T(8,128)(2,1)S(1)} collective-permute-done((bf16[1152,256]{1,0:T(8,128)(2,1)}, bf16[1152,256]{1,0:T(8,128)(2,1)S(1)}, u32[]{:S(2)}, u32[]{:S(2)}) %collective-permute-start) | collective-permute-done | bytes 589856 | tf_op jit(solution)/shard_map/ppermute | solution.py:434
  26.0 3.7 %collective-permute-start.3 = (bf16[768,256]{1,0:T(8,128)(2,1)}, bf16[768,256]{1,0:T(8,128)(2,1)S(1)}, u32[]{:S(2)}, u32[]{:S(2)}) collective-permute-start(bf16[768,256]{1,0:T(8,128)(2,1)} %get-tuple-element.31), channel_id=1, source_target_pairs={{0,96},{32,0},{64,32},{96,64},{1,97},{33,1},{65,33},{97,65},{2,98}... | collective-permute-start | bytes 1179656 | tf_op jit(solution)/shard_map/ppermute | solution.py:434
  29.8 3.5 %collective-permute-start.8 = (bf16[768,256]{1,0:T(8,128)(2,1)}, bf16[768,256]{1,0:T(8,128)(2,1)S(1)}, u32[]{:S(2)}, u32[]{:S(2)}) collective-permute-start(bf16[768,256]{1,0:T(8,128)(2,1)} %bitcast.33), channel_id=1, source_target_pairs={{0,24},{8,0},{16,8},{24,16},{1,25},{9,1},{17,9},{25,17},{2,26},{10... | collective-permute-start | bytes 1179656 | tf_op jit(solution)/shard_map/ppermute | solution.py:434
  33.3 2.2 collective-permute-done.2.refs_4_.refs_1_.refs_5_
  36.7 4.2 %shard_map.154.refs_2_ = bf16[528,768]{1,0:T(8,128)(2,1)} custom-call(s32[2]{0:T(128)} %pad_add_fusion.refs_0_, bf16[768,256]{1,0:T(8,128)(2,1)} %bitcast.27, bf16[768,256]{1,0:T(8,128)(2,1)} %bitcast.34, bf16[1152,256]{1,0:T(8,128)(2,1)} %get-tuple-element.25.refs_3_.refs_1_.refs_4_), custom_call_target="tpu_custom_call" | custom-call | flops 1811939328 | bytes 786432 | tf_op jit(solution)/shard_map/pallas_call | solution.py:347
  41.0 3.7 %shard_map.155.refs_7_ = bf16[272,768]{1,0:T(8,128)(2,1)} custom-call(s32[2]{0:T(128)} %pad_add_fusion.refs_0_, bf16[1152,256]{1,0:T(8,128)(2,1)} %get-tuple-element.25.refs_3_.refs_1_.refs_4_, bf16[768,256]{1,0:T(8,128)(2,1)} %get-tuple-element.27.refs_2_.refs_3_), custom_call_target="tpu_custom_call" | custom-call | flops 905969664 | bytes 393216 | tf_op jit(solution)/shard_map/pallas_call | solution.py:347
  45.5 3.9 %shard_map.156 = bf16[272,768]{1,0:T(8,128)(2,1)} custom-call(s32[2]{0:T(128)} %pad_add_fusion.refs_0_, bf16[1152,256]{1,0:T(8,128)(2,1)} %copy-done.11, bf16[768,256]{1,0:T(8,128)(2,1)} %get-tuple-element.27.refs_2_.refs_3_, bf16[768,256]{1,0:T(8,128)(2,1)} %copy-done.16, bf16[768,256]{1,0:T(8,128)(2,1)} %copy-done.17, bf16[768,256]{1,0:T(8,128)(2,1)} %copy-done.18), custom_call_target="tpu_custom_call" | custom-call | flops 905969664 | bytes 1572864 | tf_op jit(solution)/shard_map/pallas_call | solution.py:347
  51.4 43.5 %shard_map.157 = bf16[528,768]{1,0:T(8,128)(2,1)} custom-call(s32[2]{0:T(128)} %pad_add_fusion.refs_0_, bf16[768,256]{1,0:T(8,128)(2,1)} %copy-done.17, bf16[768,256]{1,0:T(8,128)(2,1)} %bitcast.35, bf16[1152,256]{1,0:T(8,128)(2,1)} %get-tuple-element.25.refs_3_.refs_1_.refs_4_, bf16[768,256]{1,0:T(8,128)(2,1)} %copy-done.15, bf16[1152,256]{1,0:T(8,128)(2,1)} %copy-done.12, ...), custom_call_target="tpu_custom_call" | custom-call | flops 1811939328 | bytes 3145728 | tf_op jit(solution)/shard_map/pallas_call | solution.py:347
  94.9 49.3 %shard_map.158 = (bf16[528,768]{1,0:T(8,128)(2,1)}, bf16[528,768]{1,0:T(8,128)(2,1)}) custom-call(s32[2]{0:T(128)} %pad_add_fusion.refs_0_, bf16[768,256]{1,0:T(8,128)(2,1)} %copy-done.18, bf16[768,256]{1,0:T(8,128)(2,1)} %copy-done.16, bf16[768,256]{1,0:T(8,128)(2,1)} %bitcast.36, bf16[1152,256]{1,0:T(8,128)(2,1)} %get-tuple-element.25.refs_3_.refs_1_.refs_4_, ...), custom_call_target="tpu_custom_call" | custom-call | flops 3623878656 | bytes 3145728 | tf_op jit(solution)/shard_map/pallas_call | solution.py:347
  149.2 5.7 %collective-permute-done.9.refs_2_ = bf16[384,256]{1,0:T(8,128)(2,1)S(1)} collective-permute-done((bf16[384,256]{1,0:T(8,128)(2,1)S(1)}, bf16[384,256]{1,0:T(8,128)(2,1)S(1)}, u32[]{:S(2)}, u32[]{:S(2)}) %collective-permute-start.9) | collective-permute-done | bytes 196640 | tf_op jit(solution)/shard_map/ppermute | solution.py:434
  155.6 5.4 %shard_map.159 = (bf16[272,768]{1,0:T(8,128)(2,1)}, bf16[272,768]{1,0:T(8,128)(2,1)}) custom-call(s32[2]{0:T(128)} %pad_add_fusion.refs_0_, bf16[1152,256]{1,0:T(8,128)(2,1)} %copy-done.12, bf16[384,256]{1,0:T(8,128)(2,1)} %copy-done.20, bf16[768,256]{1,0:T(8,128)(2,1)} %get-tuple-element.27.refs_2_.refs_3_, bf16[768,256]{1,0:T(8,128)(2,1)} %copy-done.16, ...), custom_call_target="tpu_custom_call" | custom-call | flops 1811939328 | bytes 1572864 | tf_op jit(solution)/shard_map/pallas_call | solution.py:347
  164.2 4.7 %collective-permute-done.14.refs_10_ = bf16[272,768]{1,0:T(8,128)(2,1)} collective-permute-done((bf16[272,768]{1,0:T(8,128)(2,1)}, bf16[272,768]{1,0:T(8,128)(2,1)}, u32[]{:S(2)}, u32[]{:S(2)}) %collective-permute-start.14) | collective-permute-done | bytes 417824 | tf_op jit(solution)/shard_map/ppermute | solution.py:434
  170.6 7.7 %collective-permute-done.10.refs_4_ = bf16[528,768]{1,0:T(8,128)(2,1)S(1)} collective-permute-done((bf16[528,768]{1,0:T(8,128)(2,1)}, bf16[528,768]{1,0:T(8,128)(2,1)S(1)}, u32[]{:S(2)}, u32[]{:S(2)}) %collective-permute-start.10) | collective-permute-done | bytes 811040 | tf_op jit(solution)/shard_map/ppermute | solution.py:438
  179.2 5.0 %merge_reads.1 = bf16[768,384]{1,0:T(8,128)(2,1)} custom-call(s32[2]{0:T(128)} %pad_add_fusion.refs_0_, f32[2,1]{1,0:T(2,128)} %copy.23.refs_1_, bf16[528,768]{1,0:T(8,128)(2,1)} %shard_map.154.refs_2_, bf16[528,768]{1,0:T(8,128)(2,1)} %shard_map.161.refs_3_, bf16[528,768]{1,0:T(8,128)(2,1)} %copy-done.9, bf16[528,768]{1,0:T(8,128)(2,1)} %copy-done.7, ...), custom_call_target="tpu_custom_call" | custom-call | tf_op jit(solution)/shard_map/merge_reads/pallas_call | solution.py:422
  184.2 7.6 %all-to-all-start = ((bf16[8,96,384]{2,1,0:T(8,128)(2,1)}), bf16[8,96,384]{2,1,0:T(8,128)(2,1)S(1)}, u32[]{:S(2)}, u32[]{:S(2)}) async-start(bf16[8,96,384]{2,1,0:T(8,128)(2,1)} %bitcast.24), calls=%async_computation | async-start | bytes 1179648 | tf_op jit(solution)/shard_map/all_to_all | solution.py:750
  192.4 9.5 %all-to-all-done.mine = bf16[8,96,384]{2,1,0:T(8,128)(2,1)S(1)} async-done(((bf16[8,96,384]{2,1,0:T(8,128)(2,1)}), bf16[8,96,384]{2,1,0:T(8,128)(2,1)S(1)}, u32[]{:S(2)}, u32[]{:S(2)}) %all-to-all-start) | async-done | bytes 589856 | tf_op jit(solution)/shard_map/all_to_all | solution.py:750
  201.9 6.9 %project.1 = (bf16[96,2048]{1,0:T(8,128)(2,1)S(1)}, bf16[384,16,128]{2,1,0:T(8,128)(2,1)S(1)}) custom-call(s32[384]{0:T(512)S(1)} %select_reduce_fusion.token_of, bf16[8,96,384]{2,1,0:T(8,128)(2,1)S(1)} %all-to-all-done.mine, bf16[2048,2048]{1,0:T(8,128)(2,1)} %all-gather.3.cloned.1.call-done.weight_wide, ...), custom_call_target="tpu_custom_call" | custom-call | tf_op jit(solution)/shard_map/project/pallas_call | solution.py:594
  208.8 32.0 %all_to_all.15 = bf16[128,48,128]{2,1,0:T(8,128)(2,1)S(1)} all-to-all(bf16[128,48,128]{2,1,0:T(8,128)(2,1)S(1)} %bitcast.22), channel_id=1, replica_groups=mesh['z'=4,'x'=4,'y'=4,'c'=2] {'z','x','y','c'}, dimensions={0} | all-to-all | bytes 3145728 | tf_op jit(solution)/shard_map/all_to_all | solution.py:759
  240.8 7.8 %experts.1 = bf16[384,16,128]{2,1,0:T(8,128)(2,1)} custom-call(bf16[384,16,128]{2,1,0:T(8,128)(2,1)S(1)} %bitcast.18, bf16[2048,1024]{1,0:T(8,128)(2,1)S(1)} %bitcast.19, bf16[2048,1024]{1,0:T(8,128)(2,1)S(1)} %bitcast.20, bf16[1024,2048]{1,0:T(8,128)(2,1)S(1)} %bitcast.21), custom_call_target="tpu_custom_call" | custom-call | tf_op jit(solution)/shard_map/experts/pallas_call | solution.py:655
  248.6 4.8 %all-to-all-start.2 = ((bf16[128,48,128]{2,1,0:T(8,128)(2,1)}), bf16[128,48,128]{2,1,0:T(8,128)(2,1)S(1)}, u32[]{:S(2)}, u32[]{:S(2)}) async-start(bf16[128,48,128]{2,1,0:T(8,128)(2,1)} %bitcast.15), calls=%async_computation.2 | async-start | bytes 3145728 | tf_op jit(solution)/shard_map/all_to_all | solution.py:759
  253.7 24.3 %all-to-all-done.2 = bf16[128,48,128]{2,1,0:T(8,128)(2,1)S(1)} async-done(((bf16[128,48,128]{2,1,0:T(8,128)(2,1)}), bf16[128,48,128]{2,1,0:T(8,128)(2,1)S(1)}, u32[]{:S(2)}, u32[]{:S(2)}) %all-to-all-start.2) | async-done | bytes 1572896 | tf_op jit(solution)/shard_map/all_to_all | solution.py:759
  (88 shorter events, 21.7 us)
Async XLA Ops:
  6.5 195.3 %all-gather.5.cloned.1.call-start = ((), (), s32[]{:S(2)}) async-start(), calls=%async_computation.4 | async-start | bytes 4718592 | tf_op jit(solution)/shard_map/all_gather | solution.py:749
  9.6 192.3 %all-gather.3.cloned.1.call-start = ((), (), s32[]{:S(2)}) async-start(), calls=%async_computation.3 | async-start | bytes 9437184 | tf_op jit(solution)/shard_map/all_gather | solution.py:748
  10.3 15.7 %collective-permute-start = (bf16[1152,256]{1,0:T(8,128)(2,1)}, bf16[1152,256]{1,0:T(8,128)(2,1)S(1)}, u32[]{:S(2)}, u32[]{:S(2)}) collective-permute-start(bf16[1152,256]{1,0:T(8,128)(2,1)} %get-tuple-element.25.refs_3_.refs_1_.refs_4_), channel_id=1, source_target_pairs={{0,24},{8,0},{16,8},{24,16},{1,25},{9,1},{17,9},{25,17},{2,26},{10... | collective-permute-start | bytes 1769480 | tf_op jit(solution)/shard_map/ppermute | solution.py:434
  13.7 16.1 %collective-permute-start.1 = (bf16[768,256]{1,0:T(8,128)(2,1)}, bf16[768,256]{1,0:T(8,128)(2,1)S(1)}, u32[]{:S(2)}, u32[]{:S(2)}) collective-permute-start(bf16[768,256]{1,0:T(8,128)(2,1)} %get-tuple-element.29), channel_id=1, source_target_pairs={{0,32},{32,64},{64,96},{96,0},{1,33},{33,65},{65,97},{97,1},{2,34}... | collective-permute-start | bytes 1179656 | tf_op jit(solution)/shard_map/ppermute | solution.py:434
  15.3 18.0 %collective-permute-start.4 = (bf16[768,256]{1,0:T(8,128)(2,1)}, bf16[768,256]{1,0:T(8,128)(2,1)S(1)}, u32[]{:S(2)}, u32[]{:S(2)}) collective-permute-start(bf16[768,256]{1,0:T(8,128)(2,1)} %bitcast.32), channel_id=1, source_target_pairs={{0,8},{8,16},{16,24},{24,0},{1,9},{9,17},{17,25},{25,1},{2,10},{10... | collective-permute-start | bytes 1179656 | tf_op jit(solution)/shard_map/ppermute | solution.py:434
  15.3 20.2 %collective-permute-start.2 = (bf16[768,256]{1,0:T(8,128)(2,1)}, bf16[768,256]{1,0:T(8,128)(2,1)S(1)}, u32[]{:S(2)}, u32[]{:S(2)}) collective-permute-start(bf16[768,256]{1,0:T(8,128)(2,1)} %get-tuple-element.30), channel_id=1, source_target_pairs={{0,64},{32,96},{64,0},{96,32},{1,65},{33,97},{65,1},{97,33},{2,66}... | collective-permute-start | bytes 1179656 | tf_op jit(solution)/shard_map/ppermute | solution.py:434
  18.6 31.8 %collective-permute-start.5 = (bf16[1152,256]{1,0:T(8,128)(2,1)}, bf16[1152,256]{1,0:T(8,128)(2,1)S(1)}, u32[]{:S(2)}, u32[]{:S(2)}) collective-permute-start(bf16[1152,256]{1,0:T(8,128)(2,1)} %get-tuple-element.25.refs_3_.refs_1_.refs_4_), channel_id=1, source_target_pairs={{0,8},{8,16},{16,24},{24,0},{1,9},{9,17},{17,25},{25,1},{2,10},{10... | collective-permute-start | bytes 1769480 | tf_op jit(solution)/shard_map/ppermute | solution.py:434
  26.0 18.7 %collective-permute-start.3 = (bf16[768,256]{1,0:T(8,128)(2,1)}, bf16[768,256]{1,0:T(8,128)(2,1)S(1)}, u32[]{:S(2)}, u32[]{:S(2)}) collective-permute-start(bf16[768,256]{1,0:T(8,128)(2,1)} %get-tuple-element.31), channel_id=1, source_target_pairs={{0,96},{32,0},{64,32},{96,64},{1,97},{33,1},{65,33},{97,65},{2,98}... | collective-permute-start | bytes 1179656 | tf_op jit(solution)/shard_map/ppermute | solution.py:434
  29.8 20.6 %collective-permute-start.8 = (bf16[768,256]{1,0:T(8,128)(2,1)}, bf16[768,256]{1,0:T(8,128)(2,1)S(1)}, u32[]{:S(2)}, u32[]{:S(2)}) collective-permute-start(bf16[768,256]{1,0:T(8,128)(2,1)} %bitcast.33), channel_id=1, source_target_pairs={{0,24},{8,0},{16,8},{24,16},{1,25},{9,1},{17,9},{25,17},{2,26},{10... | collective-permute-start | bytes 1179656 | tf_op jit(solution)/shard_map/ppermute | solution.py:434
  33.3 17.1 %collective-permute-start.6 = (bf16[768,256]{1,0:T(8,128)(2,1)S(1)}, bf16[768,256]{1,0:T(8,128)(2,1)}, u32[]{:S(2)}, u32[]{:S(2)}) collective-permute-start(bf16[768,256]{1,0:T(8,128)(2,1)S(1)} %collective-permute-done.4.refs_4_.refs_5_), channel_id=1, source_target_pairs={{0,8},{8,16},{16,24},{24,0},{1,9},{9,17},{17,25},{25,1},{2,10},{10... | collective-permute-start | bytes 1179656 | tf_op jit(solution)/shard_map/ppermute | solution.py:434
  35.5 14.9 %collective-permute-start.7 = (bf16[768,256]{1,0:T(8,128)(2,1)S(1)}, bf16[768,256]{1,0:T(8,128)(2,1)}, u32[]{:S(2)}, u32[]{:S(2)}) collective-permute-start(bf16[768,256]{1,0:T(8,128)(2,1)S(1)} %slice.8), channel_id=1, source_target_pairs={{0,24},{8,0},{16,8},{24,16},{1,25},{9,1},{17,9},{25,17},{2,26},{10... | collective-permute-start | bytes 1179656 | tf_op jit(solution)/shard_map/ppermute | solution.py:434
  49.4 111.7 %collective-permute-start.13 = (bf16[272,768]{1,0:T(8,128)(2,1)}, bf16[272,768]{1,0:T(8,128)(2,1)S(1)}, u32[]{:S(2)}, u32[]{:S(2)}) collective-permute-start(bf16[272,768]{1,0:T(8,128)(2,1)} %shard_map.156), channel_id=1, source_target_pairs={{0,8},{8,16},{16,24},{24,0},{1,9},{9,17},{17,25},{25,1},{2,10},{10... | collective-permute-start | bytes 1253384 | tf_op jit(solution)/shard_map/ppermute | solution.py:434
  144.2 26.4 %collective-permute-start.11 = (bf16[528,768]{1,0:T(8,128)(2,1)}, bf16[528,768]{1,0:T(8,128)(2,1)S(1)}, u32[]{:S(2)}, u32[]{:S(2)}) collective-permute-start(bf16[528,768]{1,0:T(8,128)(2,1)} %get-tuple-element.34), channel_id=1, source_target_pairs={{0,32},{32,64},{64,96},{1,33},{33,65},{65,97},{2,34},{34,66},{66,9... | collective-permute-start | bytes 2433032 | tf_op jit(solution)/shard_map/ppermute | solution.py:438
  145.5 25.0 %collective-permute-start.12 = (bf16[528,768]{1,0:T(8,128)(2,1)}, bf16[528,768]{1,0:T(8,128)(2,1)S(1)}, u32[]{:S(2)}, u32[]{:S(2)}) collective-permute-start(bf16[528,768]{1,0:T(8,128)(2,1)} %get-tuple-element.39), channel_id=1, source_target_pairs={{0,96},{1,97},{2,98},{3,99},{4,100},{5,101},{6,102},{7,103},{8,104... | collective-permute-start | bytes 2433032 | tf_op jit(solution)/shard_map/ppermute | solution.py:438
  146.9 31.5 %collective-permute-start.10 = (bf16[528,768]{1,0:T(8,128)(2,1)}, bf16[528,768]{1,0:T(8,128)(2,1)S(1)}, u32[]{:S(2)}, u32[]{:S(2)}) collective-permute-start(bf16[528,768]{1,0:T(8,128)(2,1)} %shard_map.157), channel_id=1, source_target_pairs={{0,64},{32,96},{1,65},{33,97},{2,66},{34,98},{3,67},{35,99},{4,68}... | collective-permute-start | bytes 2433032 | tf_op jit(solution)/shard_map/ppermute | solution.py:438
  149.2 5.8 %collective-permute-start.9 = (bf16[384,256]{1,0:T(8,128)(2,1)S(1)}, bf16[384,256]{1,0:T(8,128)(2,1)S(1)}, u32[]{:S(2)}, u32[]{:S(2)}) collective-permute-start(bf16[384,256]{1,0:T(8,128)(2,1)S(1)} %slice.9), channel_id=1, source_target_pairs={{0,8},{8,16},{16,24},{24,0},{1,9},{9,17},{17,25},{25,1},{2,10},{10... | collective-permute-start | bytes 589832 | tf_op jit(solution)/shard_map/ppermute | solution.py:434
  161.0 7.9 %collective-permute-start.14 = (bf16[272,768]{1,0:T(8,128)(2,1)}, bf16[272,768]{1,0:T(8,128)(2,1)}, u32[]{:S(2)}, u32[]{:S(2)}) collective-permute-start(bf16[272,768]{1,0:T(8,128)(2,1)} %get-tuple-element.36), channel_id=1, source_target_pairs={{0,24},{8,0},{16,8},{24,16},{1,25},{9,1},{17,9},{25,17},{2,26},{10... | collective-permute-start | bytes 1253384 | tf_op jit(solution)/shard_map/ppermute | solution.py:434
  161.1 9.4 %collective-permute-start.15 = (bf16[272,768]{1,0:T(8,128)(2,1)}, bf16[272,768]{1,0:T(8,128)(2,1)}, u32[]{:S(2)}, u32[]{:S(2)}) collective-permute-start(bf16[272,768]{1,0:T(8,128)(2,1)} %get-tuple-element.40), channel_id=1, source_target_pairs={{0,16},{8,24},{16,0},{24,8},{1,17},{9,25},{17,1},{25,9},{2,18},{10... | collective-permute-start | bytes 1253384 | tf_op jit(solution)/shard_map/ppermute | solution.py:434
  184.2 17.6 %all-to-all-start = ((bf16[8,96,384]{2,1,0:T(8,128)(2,1)}), bf16[8,96,384]{2,1,0:T(8,128)(2,1)S(1)}, u32[]{:S(2)}, u32[]{:S(2)}) async-start(bf16[8,96,384]{2,1,0:T(8,128)(2,1)} %bitcast.24), calls=%async_computation | async-start | bytes 1179648 | tf_op jit(solution)/shard_map/all_to_all | solution.py:750
  201.8 38.9 %copy-start = (bf16[1,2048,1024]{2,1,0:T(8,128)(2,1)S(1)}, bf16[1,2048,1024]{2,1,0:T(8,128)(2,1)}, u32[]{:S(2)}) copy-start(bf16[1,2048,1024]{2,1,0:T(8,128)(2,1)} %param.29) | copy-start | bytes 12582916
  201.9 38.9 %copy-start.1 = (bf16[1,2048,1024]{2,1,0:T(8,128)(2,1)S(1)}, bf16[1,2048,1024]{2,1,0:T(8,128)(2,1)}, u32[]{:S(2)}) copy-start(bf16[1,2048,1024]{2,1,0:T(8,128)(2,1)} %param.30) | copy-start | bytes 12582916
  201.9 38.9 %copy-start.2 = (bf16[1,1024,2048]{2,1,0:T(8,128)(2,1)S(1)}, bf16[1,1024,2048]{2,1,0:T(8,128)(2,1)}, u32[]{:S(2)}) copy-start(bf16[1,1024,2048]{2,1,0:T(8,128)(2,1)} %param.31) | copy-start | bytes 12582916
  208.8 39.8 %copy-start.4 = (bf16[96,2048]{1,0:T(8,128)(2,1)}, bf16[96,2048]{1,0:T(8,128)(2,1)S(1)}, u32[]{:S(2)}) copy-start(bf16[96,2048]{1,0:T(8,128)(2,1)S(1)} %get-tuple-element.44.stream) | copy-start | bytes 1179652
  248.6 29.4 %all-to-all-start.2 = ((bf16[128,48,128]{2,1,0:T(8,128)(2,1)}), bf16[128,48,128]{2,1,0:T(8,128)(2,1)S(1)}, u32[]{:S(2)}, u32[]{:S(2)}) async-start(bf16[128,48,128]{2,1,0:T(8,128)(2,1)} %bitcast.15), calls=%async_computation.2 | async-start | bytes 3145728 | tf_op jit(solution)/shard_map/all_to_all | solution.py:759
  (18 other events, 205.3 us)
Sparse Core Ops, SparseCore 0:
  9.7 35.6 all-gather.4
  47.1 49.6 all-gather.2

commit v6 on v5

--- a/solution.py
+++ b/solution.py
@@ -375,6 +375,18 @@
     ]
     valid = (wide_valid, narrow_valid)
     out_ref = refs[-1]
+    lax.fori_loop(
+        0,
+        out_ref.shape[0] // BLOCK,
+        lambda k, _: merge_block(
+            pl.ds(pl.multiple_of(k * BLOCK, BLOCK), BLOCK), valid, lam, refs, widths, counts
+        ),
+        0,
+    )
+
+
+def merge_block(block, valid, lam, refs, widths, counts):
+    out_ref = refs[-1]
     guarded = (1, None)
     begin = 0
     column = 0
@@ -385,7 +397,7 @@
         for m in range(2):
             levels = []
             for k, part in enumerate(parts):
-                stats = part[2 * width :, :].astype(jnp.float32)
+                stats = part[2 * width :, block].astype(jnp.float32)
                 level = stats[8 * m : 8 * m + 1] + stats[8 * m + 1 : 8 * m + 2] + stats[
                     8 * m + 2 : 8 * m + 3
                 ]
@@ -399,7 +411,7 @@
                 whole = whole + share
             read = None
             for k, (share, part) in enumerate(zip(shares, parts)):
-                term = part[m * width : (m + 1) * width, :].astype(jnp.float32) * (share / whole)
+                term = part[m * width : (m + 1) * width, block].astype(jnp.float32) * (share / whole)
                 if read is None:
                     read = term
                 elif guarded[group] == k:
@@ -409,23 +421,23 @@
             reads.append(read)
         mixed = reads[0] - lam[group, 0] * reads[1]
         normed = mixed * lax.rsqrt(jnp.mean(mixed * mixed, axis=0, keepdims=True) + 1e-06)
-        out_ref[:, column : column + width] = normed.T.astype(jnp.bfloat16)
+        out_ref[block, column : column + width] = normed.T.astype(jnp.bfloat16)
         column += width
+    return 0
 
 
 def merge(place, lam, groups, widths):
     chunk = groups[0][0].shape[1]
-    block = chunk // 2
     counts = [len(parts) for parts in groups]
     flat = [part for parts in groups for part in parts]
     body = lambda *refs: merge_kernel(*refs, widths=widths, counts=counts)
     return pl.pallas_call(
         body,
-        grid=(chunk // block,),
         out_shape=jax.ShapeDtypeStruct((chunk, sum(widths)), jnp.bfloat16),
         in_specs=[pl.BlockSpec(memory_space=pltpu.SMEM)] * 2
-        + [pl.BlockSpec((part.shape[0], block), lambda i: (0, i)) for part in flat],
-        out_specs=pl.BlockSpec((block, sum(widths)), lambda i: (i, 0)),
+        + [pl.BlockSpec(memory_space=pltpu.VMEM)] * len(flat),
+        out_specs=pl.BlockSpec(memory_space=pltpu.VMEM),
+        compiler_params=pltpu.CompilerParams(vmem_limit_bytes=16 * 1024 * 1024),
         name="merge_reads",
     )(place, lam, *flat)
 

time: 288 us -> 291 us (1.010)
  local copies, waits for them, and re-layouts: 6.47 us -> 9.76 us
    unnamed x47, local copies, waits for them, and re-layouts: 5.23 us -> 8.52 us
  transfers between devices with their start and end apart: 20 -> 20, of which waited for: 8 -> 8; matrix products, arithmetic and copies ran while one was open for 1% -> 1% of each run, Pallas kernels for 41% -> 40%
where the time goes in v6:
time: 291 us; the launch traced here: 290 us
  Pallas kernels  137 us (47%)
  waiting for transfers between devices  63.4 us (22%)
  starting transfers between devices  33.8 us (12%)
  blocking collectives  32 us (11%)
  between operations  13.7 us (5%)
  local copies, waits for them, and re-layouts  9.76 us (3%)
    pallas_call x8, Pallas kernels, attend(): pl.pallas_call(body, out_shape=[out] * chunks, in_specs=[pl.BlockSpec(mem...  112 us
    all_to_all x1, blocking collectives, exchanged(): lax.all_to_all(rows.reshape(experts_all, -1, LANES), SP_TP, split_axis=0,...  32 us
    all_to_all x1, waiting for transfers between devices, exchanged(): lax.all_to_all(rows.reshape(experts_all, -1, LANES), SP_TP, split_axis=0,...  24.3 us
    ppermute x13, waiting for transfers between devices, around(): lax.ppermute(array, axis, [(k, (k + by) % RING) for k in range(RING)])  21.9 us
    ppermute x13, starting transfers between devices, around(): lax.ppermute(array, axis, [(k, (k + by) % RING) for k in range(RING)])  17.4 us
    all_to_all x1, waiting for transfers between devices, shards(): lax.all_to_all(heads.reshape(tp_size, local_rows, -1), TP, split_axis=0,...  9.46 us
    unnamed x47, local copies, waits for them, and re-layouts  8.52 us
    pallas_call x1, Pallas kernels, experts(): pl.pallas_call(expert_kernel, out_shape=jax.ShapeDtypeStruct(arrived.shap...  7.8 us
  transfers between devices with their start and end apart: 20, of which 8 were waited for; matrix products, arithmetic and copies ran while one was open for 1% of the time, Pallas kernels for 40%

profile of v6, /device:TPU:1, one launch (start us, length us, event | category | flops | bytes accessed | tf_op | source)
XLA Modules:
  0.0 290.3 jit_solution(9277919872155956306)
XLA Ops:
  6.5 3.0 %pack.1 = (bf16[1152,256]{1,0:T(8,128)(2,1)}, bf16[768,256]{1,0:T(8,128)(2,1)}, bf16[768,256]{1,0:T(8,128)(2,1)}, bf16[768,256]{1,0:T(8,128)(2,1)}, bf16[768,256]{1,0:T(8,128)(2,1)}) custom-call(bf16[768,256]{1,0:T(8,128)(2,1)} %bitcast.25, bf16[768,256]{1,0:T(8,128)(2,1)} %bitcast.24, bf16[768,128]{1,0:T(8,128)(2,1)} %bitcast.28, ...), custom_call_target="tpu_custom_call" | custom-call | tf_op jit(solution)/shard_map/pack/pallas_call | solution.py:62
  10.3 3.4 %collective-permute-start = (bf16[1152,256]{1,0:T(8,128)(2,1)}, bf16[1152,256]{1,0:T(8,128)(2,1)S(1)}, u32[]{:S(2)}, u32[]{:S(2)}) collective-permute-start(bf16[1152,256]{1,0:T(8,128)(2,1)} %get-tuple-element.25.refs_3_.refs_1_.refs_4_), channel_id=1, source_target_pairs={{0,24},{8,0},{16,8},{24,16},{1,25},{9,1},{17,9},{25,17},{2,26},{10... | collective-permute-start | bytes 1769480 | tf_op jit(solution)/shard_map/ppermute | solution.py:446
  15.3 3.3 %collective-permute-start.2 = (bf16[768,256]{1,0:T(8,128)(2,1)}, bf16[768,256]{1,0:T(8,128)(2,1)S(1)}, u32[]{:S(2)}, u32[]{:S(2)}) collective-permute-start(bf16[768,256]{1,0:T(8,128)(2,1)} %get-tuple-element.30), channel_id=1, source_target_pairs={{0,64},{32,96},{64,0},{96,32},{1,65},{33,97},{65,1},{97,33},{2,66}... | collective-permute-start | bytes 1179656 | tf_op jit(solution)/shard_map/ppermute | solution.py:446
  18.8 7.2 %collective-permute-done.refs_1_.refs_9_.refs_10_ = bf16[1152,256]{1,0:T(8,128)(2,1)S(1)} collective-permute-done((bf16[1152,256]{1,0:T(8,128)(2,1)}, bf16[1152,256]{1,0:T(8,128)(2,1)S(1)}, u32[]{:S(2)}, u32[]{:S(2)}) %collective-permute-start) | collective-permute-done | bytes 589856 | tf_op jit(solution)/shard_map/ppermute | solution.py:446
  26.0 3.7 %collective-permute-start.3 = (bf16[768,256]{1,0:T(8,128)(2,1)}, bf16[768,256]{1,0:T(8,128)(2,1)S(1)}, u32[]{:S(2)}, u32[]{:S(2)}) collective-permute-start(bf16[768,256]{1,0:T(8,128)(2,1)} %get-tuple-element.31), channel_id=1, source_target_pairs={{0,96},{32,0},{64,32},{96,64},{1,97},{33,1},{65,33},{97,65},{2,98}... | collective-permute-start | bytes 1179656 | tf_op jit(solution)/shard_map/ppermute | solution.py:446
  29.8 3.5 %collective-permute-start.8 = (bf16[768,256]{1,0:T(8,128)(2,1)}, bf16[768,256]{1,0:T(8,128)(2,1)}, u32[]{:S(2)}, u32[]{:S(2)}) collective-permute-start(bf16[768,256]{1,0:T(8,128)(2,1)} %bitcast.32), channel_id=1, source_target_pairs={{0,24},{8,0},{16,8},{24,16},{1,25},{9,1},{17,9},{25,17},{2,26},{10... | collective-permute-start | bytes 1179656 | tf_op jit(solution)/shard_map/ppermute | solution.py:446
  36.7 4.2 %shard_map.154.refs_2_ = bf16[528,768]{1,0:T(8,128)(2,1)} custom-call(s32[2]{0:T(128)} %pad_add_fusion.refs_0_, bf16[768,256]{1,0:T(8,128)(2,1)} %bitcast.26, bf16[768,256]{1,0:T(8,128)(2,1)} %bitcast.33, bf16[1152,256]{1,0:T(8,128)(2,1)} %get-tuple-element.25.refs_3_.refs_1_.refs_4_), custom_call_target="tpu_custom_call" | custom-call | flops 1811939328 | bytes 786432 | tf_op jit(solution)/shard_map/pallas_call | solution.py:347
  40.9 3.7 %shard_map.155.refs_7_ = bf16[272,768]{1,0:T(8,128)(2,1)} custom-call(s32[2]{0:T(128)} %pad_add_fusion.refs_0_, bf16[1152,256]{1,0:T(8,128)(2,1)} %get-tuple-element.25.refs_3_.refs_1_.refs_4_, bf16[768,256]{1,0:T(8,128)(2,1)} %get-tuple-element.27.refs_2_.refs_3_), custom_call_target="tpu_custom_call" | custom-call | flops 905969664 | bytes 393216 | tf_op jit(solution)/shard_map/pallas_call | solution.py:347
  45.4 3.9 %shard_map.156 = bf16[272,768]{1,0:T(8,128)(2,1)} custom-call(s32[2]{0:T(128)} %pad_add_fusion.refs_0_, bf16[1152,256]{1,0:T(8,128)(2,1)} %copy-done.12, bf16[768,256]{1,0:T(8,128)(2,1)} %get-tuple-element.27.refs_2_.refs_3_, bf16[768,256]{1,0:T(8,128)(2,1)} %copy-done.17, bf16[768,256]{1,0:T(8,128)(2,1)} %copy-done.18, bf16[768,256]{1,0:T(8,128)(2,1)} %copy-done.19), custom_call_target="tpu_custom_call" | custom-call | flops 905969664 | bytes 1572864 | tf_op jit(solution)/shard_map/pallas_call | solution.py:347
  51.2 43.5 %shard_map.157 = bf16[528,768]{1,0:T(8,128)(2,1)} custom-call(s32[2]{0:T(128)} %pad_add_fusion.refs_0_, bf16[768,256]{1,0:T(8,128)(2,1)} %copy-done.18, bf16[768,256]{1,0:T(8,128)(2,1)} %bitcast.34, bf16[1152,256]{1,0:T(8,128)(2,1)} %get-tuple-element.25.refs_3_.refs_1_.refs_4_, bf16[768,256]{1,0:T(8,128)(2,1)} %copy-done.16, bf16[1152,256]{1,0:T(8,128)(2,1)} %copy-done.13, ...), custom_call_target="tpu_custom_call" | custom-call | flops 1811939328 | bytes 3145728 | tf_op jit(solution)/shard_map/pallas_call | solution.py:347
  94.7 49.3 %shard_map.158 = (bf16[528,768]{1,0:T(8,128)(2,1)}, bf16[528,768]{1,0:T(8,128)(2,1)}) custom-call(s32[2]{0:T(128)} %pad_add_fusion.refs_0_, bf16[768,256]{1,0:T(8,128)(2,1)} %copy-done.19, bf16[768,256]{1,0:T(8,128)(2,1)} %copy-done.17, bf16[768,256]{1,0:T(8,128)(2,1)} %bitcast.35, bf16[1152,256]{1,0:T(8,128)(2,1)} %get-tuple-element.25.refs_3_.refs_1_.refs_4_, ...), custom_call_target="tpu_custom_call" | custom-call | flops 3623878656 | bytes 3145728 | tf_op jit(solution)/shard_map/pallas_call | solution.py:347
  149.1 5.7 %collective-permute-done.9.refs_2_ = bf16[384,256]{1,0:T(8,128)(2,1)S(1)} collective-permute-done((bf16[384,256]{1,0:T(8,128)(2,1)S(1)}, bf16[384,256]{1,0:T(8,128)(2,1)S(1)}, u32[]{:S(2)}, u32[]{:S(2)}) %collective-permute-start.9) | collective-permute-done | bytes 196640 | tf_op jit(solution)/shard_map/ppermute | solution.py:446
  155.5 5.4 %shard_map.159 = (bf16[272,768]{1,0:T(8,128)(2,1)}, bf16[272,768]{1,0:T(8,128)(2,1)}) custom-call(s32[2]{0:T(128)} %pad_add_fusion.refs_0_, bf16[1152,256]{1,0:T(8,128)(2,1)} %copy-done.13, bf16[384,256]{1,0:T(8,128)(2,1)} %copy-done.20, bf16[768,256]{1,0:T(8,128)(2,1)} %get-tuple-element.27.refs_2_.refs_3_, bf16[768,256]{1,0:T(8,128)(2,1)} %copy-done.17, ...), custom_call_target="tpu_custom_call" | custom-call | flops 1811939328 | bytes 1572864 | tf_op jit(solution)/shard_map/pallas_call | solution.py:347
  164.3 4.5 %collective-permute-done.14.refs_10_ = bf16[272,768]{1,0:T(8,128)(2,1)} collective-permute-done((bf16[272,768]{1,0:T(8,128)(2,1)}, bf16[272,768]{1,0:T(8,128)(2,1)}, u32[]{:S(2)}, u32[]{:S(2)}) %collective-permute-start.14) | collective-permute-done | bytes 417824 | tf_op jit(solution)/shard_map/ppermute | solution.py:446
  168.8 2.3 collective-permute-done.15.refs_11_
  171.1 7.1 %collective-permute-done.10.refs_4_ = bf16[528,768]{1,0:T(8,128)(2,1)S(1)} collective-permute-done((bf16[528,768]{1,0:T(8,128)(2,1)}, bf16[528,768]{1,0:T(8,128)(2,1)S(1)}, u32[]{:S(2)}, u32[]{:S(2)}) %collective-permute-start.10) | collective-permute-done | bytes 811040 | tf_op jit(solution)/shard_map/ppermute | solution.py:450
  182.3 4.5 %merge_reads.1 = bf16[768,384]{1,0:T(8,128)(2,1)} custom-call(s32[2]{0:T(128)S(1)} %copy-done.11, f32[2,1]{1,0:T(2,128)S(1)} %copy.23.refs_1_, bf16[528,768]{1,0:T(8,128)(2,1)S(1)} %copy-done.3, bf16[528,768]{1,0:T(8,128)(2,1)S(1)} %copy-done.4, bf16[528,768]{1,0:T(8,128)(2,1)S(1)} %collective-permute-done.10.refs_4_, ...), custom_call_target="tpu_custom_call" | custom-call | tf_op jit(solution)/shard_map/merge_reads/pallas_call | solution.py:434
  186.8 7.5 %all-to-all-start = ((bf16[8,96,384]{2,1,0:T(8,128)(2,1)}), bf16[8,96,384]{2,1,0:T(8,128)(2,1)S(1)}, u32[]{:S(2)}, u32[]{:S(2)}) async-start(bf16[8,96,384]{2,1,0:T(8,128)(2,1)} %bitcast.8), calls=%async_computation | async-start | bytes 1179648 | tf_op jit(solution)/shard_map/all_to_all | solution.py:762
  194.9 9.5 %all-to-all-done.mine = bf16[8,96,384]{2,1,0:T(8,128)(2,1)S(1)} async-done(((bf16[8,96,384]{2,1,0:T(8,128)(2,1)}), bf16[8,96,384]{2,1,0:T(8,128)(2,1)S(1)}, u32[]{:S(2)}, u32[]{:S(2)}) %all-to-all-start) | async-done | bytes 589856 | tf_op jit(solution)/shard_map/all_to_all | solution.py:762
  205.4 6.9 %project.1 = (bf16[96,2048]{1,0:T(8,128)(2,1)S(1)}, bf16[384,16,128]{2,1,0:T(8,128)(2,1)S(1)}) custom-call(s32[384]{0:T(512)S(1)} %select_reduce_fusion.token_of, bf16[8,96,384]{2,1,0:T(8,128)(2,1)S(1)} %all-to-all-done.mine, bf16[2048,2048]{1,0:T(8,128)(2,1)} %all-gather.3.cloned.1.call-done.weight_wide, ...), custom_call_target="tpu_custom_call" | custom-call | tf_op jit(solution)/shard_map/project/pallas_call | solution.py:606
  212.3 32.0 %all_to_all.15 = bf16[128,48,128]{2,1,0:T(8,128)(2,1)S(1)} all-to-all(bf16[128,48,128]{2,1,0:T(8,128)(2,1)S(1)} %bitcast.22), channel_id=1, replica_groups=mesh['z'=4,'x'=4,'y'=4,'c'=2] {'z','x','y','c'}, dimensions={0} | all-to-all | bytes 3145728 | tf_op jit(solution)/shard_map/all_to_all | solution.py:771
  244.3 7.8 %experts.1 = bf16[384,16,128]{2,1,0:T(8,128)(2,1)} custom-call(bf16[384,16,128]{2,1,0:T(8,128)(2,1)S(1)} %bitcast.18, bf16[2048,1024]{1,0:T(8,128)(2,1)S(1)} %bitcast.19, bf16[2048,1024]{1,0:T(8,128)(2,1)S(1)} %bitcast.20, bf16[1024,2048]{1,0:T(8,128)(2,1)S(1)} %bitcast.21), custom_call_target="tpu_custom_call" | custom-call | tf_op jit(solution)/shard_map/experts/pallas_call | solution.py:667
  252.1 4.8 %all-to-all-start.2 = ((bf16[128,48,128]{2,1,0:T(8,128)(2,1)}), bf16[128,48,128]{2,1,0:T(8,128)(2,1)S(1)}, u32[]{:S(2)}, u32[]{:S(2)}) async-start(bf16[128,48,128]{2,1,0:T(8,128)(2,1)} %bitcast.15), calls=%async_computation.2 | async-start | bytes 3145728 | tf_op jit(solution)/shard_map/all_to_all | solution.py:771
  257.2 24.3 %all-to-all-done.2 = bf16[128,48,128]{2,1,0:T(8,128)(2,1)S(1)} async-done(((bf16[128,48,128]{2,1,0:T(8,128)(2,1)}), bf16[128,48,128]{2,1,0:T(8,128)(2,1)S(1)}, u32[]{:S(2)}, u32[]{:S(2)}) %all-to-all-start.2) | async-done | bytes 1572896 | tf_op jit(solution)/shard_map/all_to_all | solution.py:771
  (88 shorter events, 25.6 us)
Async XLA Ops:
  6.5 197.8 %all-gather.5.cloned.1.call-start = ((), (), s32[]{:S(2)}) async-start(), calls=%async_computation.4 | async-start | bytes 4718592 | tf_op jit(solution)/shard_map/all_gather | solution.py:761
  9.6 194.8 %all-gather.3.cloned.1.call-start = ((), (), s32[]{:S(2)}) async-start(), calls=%async_computation.3 | async-start | bytes 9437184 | tf_op jit(solution)/shard_map/all_gather | solution.py:760
  10.3 15.7 %collective-permute-start = (bf16[1152,256]{1,0:T(8,128)(2,1)}, bf16[1152,256]{1,0:T(8,128)(2,1)S(1)}, u32[]{:S(2)}, u32[]{:S(2)}) collective-permute-start(bf16[1152,256]{1,0:T(8,128)(2,1)} %get-tuple-element.25.refs_3_.refs_1_.refs_4_), channel_id=1, source_target_pairs={{0,24},{8,0},{16,8},{24,16},{1,25},{9,1},{17,9},{25,17},{2,26},{10... | collective-permute-start | bytes 1769480 | tf_op jit(solution)/shard_map/ppermute | solution.py:446
  13.7 16.1 %collective-permute-start.1 = (bf16[768,256]{1,0:T(8,128)(2,1)}, bf16[768,256]{1,0:T(8,128)(2,1)S(1)}, u32[]{:S(2)}, u32[]{:S(2)}) collective-permute-start(bf16[768,256]{1,0:T(8,128)(2,1)} %get-tuple-element.29), channel_id=1, source_target_pairs={{0,32},{32,64},{64,96},{96,0},{1,33},{33,65},{65,97},{97,1},{2,34}... | collective-permute-start | bytes 1179656 | tf_op jit(solution)/shard_map/ppermute | solution.py:446
  15.3 18.0 %collective-permute-start.4 = (bf16[768,256]{1,0:T(8,128)(2,1)}, bf16[768,256]{1,0:T(8,128)(2,1)S(1)}, u32[]{:S(2)}, u32[]{:S(2)}) collective-permute-start(bf16[768,256]{1,0:T(8,128)(2,1)} %bitcast.31), channel_id=1, source_target_pairs={{0,8},{8,16},{16,24},{24,0},{1,9},{9,17},{17,25},{25,1},{2,10},{10... | collective-permute-start | bytes 1179656 | tf_op jit(solution)/shard_map/ppermute | solution.py:446
  15.3 20.2 %collective-permute-start.2 = (bf16[768,256]{1,0:T(8,128)(2,1)}, bf16[768,256]{1,0:T(8,128)(2,1)S(1)}, u32[]{:S(2)}, u32[]{:S(2)}) collective-permute-start(bf16[768,256]{1,0:T(8,128)(2,1)} %get-tuple-element.30), channel_id=1, source_target_pairs={{0,64},{32,96},{64,0},{96,32},{1,65},{33,97},{65,1},{97,33},{2,66}... | collective-permute-start | bytes 1179656 | tf_op jit(solution)/shard_map/ppermute | solution.py:446
  18.6 31.8 %collective-permute-start.5 = (bf16[1152,256]{1,0:T(8,128)(2,1)}, bf16[1152,256]{1,0:T(8,128)(2,1)S(1)}, u32[]{:S(2)}, u32[]{:S(2)}) collective-permute-start(bf16[1152,256]{1,0:T(8,128)(2,1)} %get-tuple-element.25.refs_3_.refs_1_.refs_4_), channel_id=1, source_target_pairs={{0,8},{8,16},{16,24},{24,0},{1,9},{9,17},{17,25},{25,1},{2,10},{10... | collective-permute-start | bytes 1769480 | tf_op jit(solution)/shard_map/ppermute | solution.py:446
  26.0 18.7 %collective-permute-start.3 = (bf16[768,256]{1,0:T(8,128)(2,1)}, bf16[768,256]{1,0:T(8,128)(2,1)S(1)}, u32[]{:S(2)}, u32[]{:S(2)}) collective-permute-start(bf16[768,256]{1,0:T(8,128)(2,1)} %get-tuple-element.31), channel_id=1, source_target_pairs={{0,96},{32,0},{64,32},{96,64},{1,97},{33,1},{65,33},{97,65},{2,98}... | collective-permute-start | bytes 1179656 | tf_op jit(solution)/shard_map/ppermute | solution.py:446
  29.8 20.6 %collective-permute-start.8 = (bf16[768,256]{1,0:T(8,128)(2,1)}, bf16[768,256]{1,0:T(8,128)(2,1)}, u32[]{:S(2)}, u32[]{:S(2)}) collective-permute-start(bf16[768,256]{1,0:T(8,128)(2,1)} %bitcast.32), channel_id=1, source_target_pairs={{0,24},{8,0},{16,8},{24,16},{1,25},{9,1},{17,9},{25,17},{2,26},{10... | collective-permute-start | bytes 1179656 | tf_op jit(solution)/shard_map/ppermute | solution.py:446
  33.3 17.1 %collective-permute-start.6 = (bf16[768,256]{1,0:T(8,128)(2,1)S(1)}, bf16[768,256]{1,0:T(8,128)(2,1)}, u32[]{:S(2)}, u32[]{:S(2)}) collective-permute-start(bf16[768,256]{1,0:T(8,128)(2,1)S(1)} %collective-permute-done.4.refs_4_.refs_5_), channel_id=1, source_target_pairs={{0,8},{8,16},{16,24},{24,0},{1,9},{9,17},{17,25},{25,1},{2,10},{10... | collective-permute-start | bytes 1179656 | tf_op jit(solution)/shard_map/ppermute | solution.py:446
  35.5 14.9 %collective-permute-start.7 = (bf16[768,256]{1,0:T(8,128)(2,1)S(1)}, bf16[768,256]{1,0:T(8,128)(2,1)}, u32[]{:S(2)}, u32[]{:S(2)}) collective-permute-start(bf16[768,256]{1,0:T(8,128)(2,1)S(1)} %slice.8), channel_id=1, source_target_pairs={{0,24},{8,0},{16,8},{24,16},{1,25},{9,1},{17,9},{25,17},{2,26},{10... | collective-permute-start | bytes 1179656 | tf_op jit(solution)/shard_map/ppermute | solution.py:446
  49.4 111.6 %collective-permute-start.13 = (bf16[272,768]{1,0:T(8,128)(2,1)}, bf16[272,768]{1,0:T(8,128)(2,1)S(1)}, u32[]{:S(2)}, u32[]{:S(2)}) collective-permute-start(bf16[272,768]{1,0:T(8,128)(2,1)} %shard_map.156), channel_id=1, source_target_pairs={{0,8},{8,16},{16,24},{24,0},{1,9},{9,17},{17,25},{25,1},{2,10},{10... | collective-permute-start | bytes 1253384 | tf_op jit(solution)/shard_map/ppermute | solution.py:446
  144.0 27.1 %collective-permute-start.11 = (bf16[528,768]{1,0:T(8,128)(2,1)}, bf16[528,768]{1,0:T(8,128)(2,1)S(1)}, u32[]{:S(2)}, u32[]{:S(2)}) collective-permute-start(bf16[528,768]{1,0:T(8,128)(2,1)} %get-tuple-element.34), channel_id=1, source_target_pairs={{0,32},{32,64},{64,96},{1,33},{33,65},{65,97},{2,34},{34,66},{66,9... | collective-permute-start | bytes 2433032 | tf_op jit(solution)/shard_map/ppermute | solution.py:450
  145.3 25.7 %collective-permute-start.12 = (bf16[528,768]{1,0:T(8,128)(2,1)}, bf16[528,768]{1,0:T(8,128)(2,1)S(1)}, u32[]{:S(2)}, u32[]{:S(2)}) collective-permute-start(bf16[528,768]{1,0:T(8,128)(2,1)} %get-tuple-element.39), channel_id=1, source_target_pairs={{0,96},{1,97},{2,98},{3,99},{4,100},{5,101},{6,102},{7,103},{8,104... | collective-permute-start | bytes 2433032 | tf_op jit(solution)/shard_map/ppermute | solution.py:450
  146.7 31.5 %collective-permute-start.10 = (bf16[528,768]{1,0:T(8,128)(2,1)}, bf16[528,768]{1,0:T(8,128)(2,1)S(1)}, u32[]{:S(2)}, u32[]{:S(2)}) collective-permute-start(bf16[528,768]{1,0:T(8,128)(2,1)} %shard_map.157), channel_id=1, source_target_pairs={{0,64},{32,96},{1,65},{33,97},{2,66},{34,98},{3,67},{35,99},{4,68}... | collective-permute-start | bytes 2433032 | tf_op jit(solution)/shard_map/ppermute | solution.py:450
  149.0 5.8 %collective-permute-start.9 = (bf16[384,256]{1,0:T(8,128)(2,1)S(1)}, bf16[384,256]{1,0:T(8,128)(2,1)S(1)}, u32[]{:S(2)}, u32[]{:S(2)}) collective-permute-start(bf16[384,256]{1,0:T(8,128)(2,1)S(1)} %slice.9), channel_id=1, source_target_pairs={{0,8},{8,16},{16,24},{24,0},{1,9},{9,17},{17,25},{25,1},{2,10},{10... | collective-permute-start | bytes 589832 | tf_op jit(solution)/shard_map/ppermute | solution.py:446
  160.9 7.9 %collective-permute-start.14 = (bf16[272,768]{1,0:T(8,128)(2,1)}, bf16[272,768]{1,0:T(8,128)(2,1)}, u32[]{:S(2)}, u32[]{:S(2)}) collective-permute-start(bf16[272,768]{1,0:T(8,128)(2,1)} %get-tuple-element.36), channel_id=1, source_target_pairs={{0,24},{8,0},{16,8},{24,16},{1,25},{9,1},{17,9},{25,17},{2,26},{10... | collective-permute-start | bytes 1253384 | tf_op jit(solution)/shard_map/ppermute | solution.py:446
  161.7 9.3 %collective-permute-start.15 = (bf16[272,768]{1,0:T(8,128)(2,1)}, bf16[272,768]{1,0:T(8,128)(2,1)}, u32[]{:S(2)}, u32[]{:S(2)}) collective-permute-start(bf16[272,768]{1,0:T(8,128)(2,1)} %get-tuple-element.40), channel_id=1, source_target_pairs={{0,16},{8,24},{16,0},{24,8},{1,17},{9,25},{17,1},{25,9},{2,18},{10... | collective-permute-start | bytes 1253384 | tf_op jit(solution)/shard_map/ppermute | solution.py:446
  163.4 41.0 %copy-start.10 = (f32[2048]{0:T(1024)S(1)}, f32[2048]{0:T(1024)}, u32[]{:S(2)}) copy-start(f32[2048]{0:T(1024)} %param.26) | copy-start | bytes 24580
  186.8 17.6 %all-to-all-start = ((bf16[8,96,384]{2,1,0:T(8,128)(2,1)}), bf16[8,96,384]{2,1,0:T(8,128)(2,1)S(1)}, u32[]{:S(2)}, u32[]{:S(2)}) async-start(bf16[8,96,384]{2,1,0:T(8,128)(2,1)} %bitcast.8), calls=%async_computation | async-start | bytes 1179648 | tf_op jit(solution)/shard_map/all_to_all | solution.py:762
  205.4 38.9 %copy-start = (bf16[1,2048,1024]{2,1,0:T(8,128)(2,1)S(1)}, bf16[1,2048,1024]{2,1,0:T(8,128)(2,1)}, u32[]{:S(2)}) copy-start(bf16[1,2048,1024]{2,1,0:T(8,128)(2,1)} %param.29) | copy-start | bytes 12582916
  205.4 38.9 %copy-start.1 = (bf16[1,2048,1024]{2,1,0:T(8,128)(2,1)S(1)}, bf16[1,2048,1024]{2,1,0:T(8,128)(2,1)}, u32[]{:S(2)}) copy-start(bf16[1,2048,1024]{2,1,0:T(8,128)(2,1)} %param.30) | copy-start | bytes 12582916
  205.4 38.9 %copy-start.2 = (bf16[1,1024,2048]{2,1,0:T(8,128)(2,1)S(1)}, bf16[1,1024,2048]{2,1,0:T(8,128)(2,1)}, u32[]{:S(2)}) copy-start(bf16[1,1024,2048]{2,1,0:T(8,128)(2,1)} %param.31) | copy-start | bytes 12582916
  252.1 29.3 %all-to-all-start.2 = ((bf16[128,48,128]{2,1,0:T(8,128)(2,1)}), bf16[128,48,128]{2,1,0:T(8,128)(2,1)S(1)}, u32[]{:S(2)}, u32[]{:S(2)}) async-start(bf16[128,48,128]{2,1,0:T(8,128)(2,1)} %bitcast.15), calls=%async_computation.2 | async-start | bytes 3145728 | tf_op jit(solution)/shard_map/all_to_all | solution.py:771
  (18 other events, 148.1 us)
Sparse Core Ops, SparseCore 0:
  9.7 35.6 all-gather.4
  47.1 49.6 all-gather.2
